TPU v7x, 512 devices: a whole 4x8x8 slice. The times are simulated.
512 devices in a mesh: sp: 32 (over z, x), tp: 16 (over y, core).
Axes of the slice: x: 4, y: 8, z: 8, core: 2. Of those that a mesh axis runs over, the one named last changes fastest.
Arguments:
- conv_value: bfloat16 [8192, 1024], P('sp', 'tp'), may hold values from -15 to 15
- conv_gate: bfloat16 [8192, 1024], P('sp', 'tp'), may hold values from -8 to 8
- conv_taps: bfloat16 [31, 1024], P(None, 'tp'), may hold values from -1 to 1
- conv_gain: float32 [1024], P('tp'), may hold values from 0.1 to 1.9
- out_weight: bfloat16 [1024, 2048], P('tp'), may hold values from -0.1875 to 0.1875
- residual: bfloat16 [8192, 2048], P('sp'), may hold values from -6 to 6
- route_ids: int32 [8192, 2], P('sp'), may hold values from 0 to 31, all different within a row; in each aligned block of 256 rows (0 to 255, 256 to 511, ...) at most 32 rows name the same one
- route_weight: float32 [8192, 2], P('sp'), may hold values from 0.3 to 1.5
- expert_gate: bfloat16 [32, 2048, 4096], P('sp', None, 'tp'), may hold values from -0.125 to 0.125
- expert_up: bfloat16 [32, 2048, 4096], P('sp', None, 'tp'), may hold values from -0.125 to 0.125
- expert_down: bfloat16 [32, 4096, 2048], P('sp', 'tp'), may hold values from -0.09375 to 0.09375
Outputs:
- layer_out: bfloat16 [8192, 2048], P('sp', 'tp')
Inputs may be any that keep to these rules, and one draw needn't show every extreme that they name: `route_ids`: in each aligned block of 256 rows no expert is named by more than 32 rows; some expert is named by exactly 32 rows in some blocks.
All inputs are finite; a program needn't handle non-finite values.
Results may differ from a plain program's by a relative error of at most 0.017.
Values may be sent and summed in bfloat16 or wider, within the bound.
No kernel may reach another device: no remote copies, remote signals or barrier semaphores. Data moves between devices by JAX's collectives and lax.ppermute only.
A program may use at most 64 MiB of HBM per device.

v0:
```python
import jax
import jax.numpy as jnp
from jax import lax
from jax.sharding import Mesh
from jax.sharding import PartitionSpec as P

TP = ("tp_0", "tp_1")


def passed_along(value, axis, steps):
    count = lax.axis_size(axis)
    initial, last = (max(0, -steps), min(count, count - steps))
    return lax.ppermute(value, axis, [(source, source + steps) for source in range(initial, last)])


def sent_to_all(value, axis):
    size = lax.axis_size(axis)
    return lax.all_to_all(
        jnp.broadcast_to(value[None], (size, *value.shape)), axis, 0, 0, tiled=True
    )


def over_copies(value, axis):
    everything = sent_to_all(value, axis)
    return jnp.sum(everything, axis=0)


def packed_total(arrays, axis):
    ends = [0]
    for a in arrays:
        ends.append(ends[-1] + a.size)
    so_far = over_copies(jnp.concatenate([a.ravel() for a in arrays]), axis)
    return tuple((so_far[b:e].reshape(a.shape) for a, b, e in zip(arrays, ends, ends[1:])))


def filled_up(lines, size):
    spare = -len(lines) % size
    return jnp.pad(lines, [(0, spare)] + [(0, 0)] * (lines.ndim - 1))


def laid_out(blocks, dim):
    blocks = jnp.moveaxis(blocks, 0, dim)
    shape = blocks.shape
    return blocks.reshape(*shape[:dim], shape[dim] * shape[dim + 1], *shape[dim + 2 :])


def gather_axes(value, axes, dim):
    far, near = axes
    initial = sent_to_all(value, far)
    blocks = jnp.swapaxes(sent_to_all(initial, near), 0, 1)
    return laid_out(blocks.reshape(-1, *value.shape), dim)


def split_up(value, dim, size):
    shape = value.shape
    blocks = value.reshape(*shape[:dim], size, shape[dim] // size, *shape[dim + 1 :])
    return jnp.moveaxis(blocks, dim, 0)


def summed_on_arrival(value, axis, dim):
    size = lax.axis_size(axis)
    blocks = lax.all_to_all(split_up(value, dim, size), axis, 0, 0, tiled=True)
    return jnp.sum(blocks.astype(jnp.float32), axis=0)


def sum_in_two_steps(value, axes, dim):
    far, near = axes
    blocks = split_up(value, dim, lax.axis_size(far))
    nearer = summed_on_arrival(blocks, near, dim + 1)
    arrived = lax.all_to_all(
        nearer.astype(jnp.bfloat16), far, split_axis=0, concat_axis=0, tiled=True
    )
    return arrived.astype(jnp.float32).sum(axis=0)


def sum_by_parts(value, axes):
    lines = value.reshape(-1, value.shape[-1])
    padded = filled_up(lines, lax.axis_size(axes[0]) * lax.axis_size(axes[1]))
    whole = gather_axes(sum_in_two_steps(padded, axes, 0).astype(jnp.bfloat16), axes, 0)
    return lax.slice_in_dim(whole, 0, len(lines)).reshape(value.shape).astype(jnp.float32)


def slot_plan(block_ids, experts, capacity):
    assigned = block_ids.reshape(-1)
    pair_count = assigned.shape[0]
    onehot = (assigned[:, None] == jnp.arange(experts, dtype=jnp.int32)[None, :]).astype(jnp.int32)
    earlier = jnp.cumsum(onehot, axis=0) - onehot
    ranking = jnp.sum(earlier * onehot, axis=1)
    target = assigned * capacity + ranking
    owners = jnp.arange(pair_count, dtype=jnp.int32) // block_ids.shape[1]
    matches = target[None, :] == jnp.arange(experts * capacity, dtype=jnp.int32)[:, None]
    holder = jnp.sum(jnp.where(matches, owners[None, :] + 1, 0), axis=1) - 1
    holder = jnp.where(holder < 0, block_ids.shape[0], holder)
    return (target, holder)


def local(
    conv_value,
    conv_gate,
    conv_taps,
    conv_gain,
    out_weight,
    residual,
    route_ids,
    route_weight,
    expert_gate,
    expert_up,
    expert_down,
):
    taps_count = conv_taps.shape[0]
    token_rows = conv_value.shape[0]
    tails = passed_along(
        (conv_value[token_rows - taps_count + 1 :], conv_gate[token_rows - taps_count + 1 :]),
        "sp",
        1,
    )
    values_ext = jnp.concatenate([tails[0], conv_value], axis=0)
    gates_ext = jnp.concatenate([tails[1], conv_gate], axis=0)
    gated = values_ext.astype(jnp.float32) * jax.nn.sigmoid(gates_ext.astype(jnp.float32))
    filtered = jnp.zeros(conv_value.shape, jnp.float32)
    for offset in range(taps_count):
        filtered = (
            filtered + conv_taps[offset].astype(jnp.float32) * gated[offset : offset + token_rows]
        )
    channels = conv_value.shape[1] * lax.axis_size(TP)
    totals = packed_total((jnp.sum(filtered, axis=1), jnp.sum(filtered * filtered, axis=1)), TP)
    average = totals[0] / channels
    variance = totals[1] / channels - average * average
    normed = (filtered - average[:, None]) * lax.rsqrt(variance + 1e-05)[:, None] * conv_gain
    activated = jax.nn.silu(normed).astype(jnp.bfloat16)
    mixed = sum_by_parts(
        jnp.dot(activated, out_weight, preferred_element_type=jnp.float32).astype(jnp.bfloat16),
        ("tp_0", "tp_1"),
    )
    updated = residual.astype(jnp.float32) + mixed
    width = updated.shape[1]
    normal_rows = (
        updated * lax.rsqrt(jnp.mean(updated * updated, axis=1, keepdims=True) + 1e-06)
    ).astype(jnp.bfloat16)
    experts = lax.axis_size("sp")
    top_count = route_ids.shape[1]
    capacity = 2 * token_rows * top_count // experts
    targets, holders = slot_plan(route_ids, experts, capacity)
    padded_rows = jnp.concatenate([normal_rows, jnp.zeros((1, width), jnp.bfloat16)], axis=0)
    buffer = padded_rows[holders].reshape(experts, capacity, width)
    w_gate = expert_gate[0]
    w_up = expert_up[0]
    w_down = expert_down[0]
    share = capacity // lax.axis_size(TP)
    mine = lax.dynamic_slice_in_dim(buffer, lax.axis_index(TP) * share, share, 1)
    arrived = lax.all_to_all(mine, "sp", split_axis=0, concat_axis=0, tiled=True)
    block = lax.all_gather(arrived, TP, axis=1, tiled=True)
    flat = block.reshape(-1, width)
    gate_act = jnp.dot(flat, w_gate, preferred_element_type=jnp.float32)
    up_act = jnp.dot(flat, w_up, preferred_element_type=jnp.float32)
    hidden = (jax.nn.silu(gate_act) * up_act).astype(jnp.bfloat16)
    result = jnp.dot(hidden, w_down, preferred_element_type=jnp.float32)
    partials = result.reshape(block.shape[0], block.shape[1], width)
    summed = sum_in_two_steps(partials.astype(jnp.bfloat16), ("tp_0", "tp_1"), 2).astype(
        jnp.bfloat16
    )
    back = lax.all_to_all(summed, "sp", split_axis=0, concat_axis=0, tiled=True)
    columns = back.shape[2]
    picked = back.reshape(experts * capacity, columns)[targets].reshape(
        token_rows, top_count, columns
    )
    combined = jnp.sum(picked.astype(jnp.float32) * route_weight[:, :, None], axis=1)
    own_cols = lax.dynamic_slice_in_dim(updated, lax.axis_index(TP) * columns, columns, 1)
    return (own_cols + combined).astype(jnp.bfloat16)


def solution(mesh):
    torus = Mesh(mesh.devices.reshape(mesh.shape["sp"], 8, 2), ("sp", "tp_0", "tp_1"))
    placed = (
        P("sp", TP),
        P("sp", TP),
        P(None, TP),
        P(TP),
        P(TP, None),
        P("sp", None),
        P("sp", None),
        P("sp", None),
        P("sp", None, TP),
        P("sp", None, TP),
        P("sp", TP, None),
    )
    return jax.shard_map(local, mesh=torus, in_specs=placed, out_specs=P("sp", TP), check_vma=False)
```

profile of v0, /device:TPU:1, one launch (start us, length us, event | category | flops | bytes accessed | tf_op | source)
XLA Modules:
  0.0 284.7 jit_solution(16322086723981687801)
XLA Ops:
  7.4 3.9 %collective-permute-start = (bf16[30,64]{0,1:T(8,128)(2,1)S(1)}, bf16[30,64]{0,1:T(8,128)(2,1)S(1)}, u32[]{:S(2)}, u32[]{:S(2)}) collective-permute-start(bf16[30,64]{0,1:T(8,128)(2,1)S(1)} %slice.205), channel_id=1, source_target_pairs={{0,16},{16,32},{32,48},{48,64},{64,80},{80,96},{96,112},{112,128},... | collective-permute-start | bytes 11528 | tf_op jit(solution)/shard_map/ppermute | solution.py:13
  12.2 3.1 %collective-permute-start.1 = (bf16[30,64]{0,1:T(8,128)(2,1)S(1)}, bf16[30,64]{0,1:T(8,128)(2,1)S(1)}, u32[]{:S(2)}, u32[]{:S(2)}) collective-permute-start(bf16[30,64]{0,1:T(8,128)(2,1)S(1)} %slice.206), channel_id=1, source_target_pairs={{0,16},{16,32},{32,48},{48,64},{64,80},{80,96},{96,112},{112,128},... | collective-permute-start | bytes 11528 | tf_op jit(solution)/shard_map/ppermute | solution.py:13
  19.1 15.5 %all_to_all.46 = f32[16,1,512]{2,1,0:T(1,128)S(1)} all-to-all(f32[16,1,512]{2,1,0:T(1,128)S(1)} %broadcast_in_dim.17), channel_id=1, replica_groups=mesh['sp'=32,'tp_0'=8,'tp_1'=2] {'tp_0','tp_1'}, dimensions={0} | all-to-all | bytes 65536 | tf_op jit(solution)/shard_map/all_to_all | solution.py:18
  35.3 4.6 %all_to_all.47 = bf16[2,8,16,2048]{3,2,1,0:T(8,128)(2,1)S(1)} all-to-all(bf16[2,8,16,2048]{3,2,1,0:T(8,128)(2,1)S(1)} %bitcast.163), channel_id=1, replica_groups=mesh['sp'=32,'tp_0'=8,'tp_1'=2] {'tp_1'}, dimensions={0} | all-to-all | bytes 2097152 | tf_op jit(solution)/shard_map/all_to_all | solution.py:62
  41.0 3.5 %all-to-all-start.2 = ((bf16[8,16,2048]{2,1,0:T(8,128)(2,1)}), bf16[8,16,2048]{2,1,0:T(8,128)(2,1)S(1)}, u32[]{:S(2)}, u32[]{:S(2)}) async-start(bf16[8,16,2048]{2,1,0:T(8,128)(2,1)} %reduce_sum.116), calls=%async_computation.2 | async-start | bytes 1048576 | tf_op jit(solution)/shard_map/all_to_all | solution.py:70
  46.5 15.9 %all-to-all-done.2 = bf16[8,16,2048]{2,1,0:T(8,128)(2,1)S(1)} async-done(((bf16[8,16,2048]{2,1,0:T(8,128)(2,1)}), bf16[8,16,2048]{2,1,0:T(8,128)(2,1)S(1)}, u32[]{:S(2)}, u32[]{:S(2)}) %all-to-all-start.2) | async-done | bytes 524320 | tf_op jit(solution)/shard_map/all_to_all | solution.py:70
  63.4 3.5 %all-to-all-start.3 = ((bf16[8,16,2048]{2,1,0:T(8,128)(2,1)}), bf16[8,16,2048]{2,1,0:T(8,128)(2,1)S(1)}, u32[]{:S(2)}, u32[]{:S(2)}) async-start(bf16[8,16,2048]{2,1,0:T(8,128)(2,1)} %broadcast_in_dim.18), calls=%async_computation.3 | async-start | bytes 1048576 | tf_op jit(solution)/shard_map/all_to_all | solution.py:18
  67.3 17.5 %all-to-all-done.3 = bf16[8,16,2048]{2,1,0:T(8,128)(2,1)S(1)} async-done(((bf16[8,16,2048]{2,1,0:T(8,128)(2,1)}), bf16[8,16,2048]{2,1,0:T(8,128)(2,1)S(1)}, u32[]{:S(2)}, u32[]{:S(2)}) %all-to-all-start.3) | async-done | bytes 524320 | tf_op jit(solution)/shard_map/all_to_all | solution.py:18
  84.8 4.7 %all_to_all.48 = bf16[2,8,16,2048]{3,2,1,0:T(8,128)(2,1)S(1)} all-to-all(bf16[2,8,16,2048]{3,2,1,0:T(8,128)(2,1)S(1)} %broadcast_in_dim.19), channel_id=1, replica_groups=mesh['sp'=32,'tp_0'=8,'tp_1'=2] {'tp_1'}, dimensions={0} | all-to-all | bytes 2097152 | tf_op jit(solution)/shard_map/all_to_all | solution.py:18
  91.4 1.4 copy-done.1
  93.1 6.0 %gather_fusion = bf16[1024,2048]{1,0:T(8,128)(2,1)} fusion(bf16[257,2048]{1,0:T(8,128)(2,1)S(1)} %concatenate.15, s32[1024]{0:T(1024)S(1)} %broadcast_clamp_fusion), kind=kCustom, calls=%fused_computation | custom fusion | bytes 8392704 | tf_op jit(solution)/shard_map/gather | solution.py:145
  99.1 1.5 constant_dynamic-slice_fusion
  100.6 25.3 %all_to_all.49 = bf16[32,2,2048]{2,1,0:T(2,128)(2,1)S(1)} all-to-all(bf16[32,2,2048]{2,1,0:T(2,128)(2,1)S(1)} %constant_dynamic-slice_fusion), channel_id=1, replica_groups=mesh['sp'=32,'tp_0'=8,'tp_1'=2] {'sp'}, dimensions={0} | all-to-all | bytes 524288 | tf_op jit(solution)/shard_map/all_to_all | solution.py:151
  126.7 36.6 %all-gather.2.cloned.1.call-done = bf16[32,32,2048]{2,0,1:T(8,128)(2,1)} async-done(((bf16[32,2,2048]{2,0,1:T(8,128)(2,1)}), bf16[32,32,2048]{2,0,1:T(8,128)(2,1)}) %all-gather.2.cloned.1.call-update) | async-done | bytes 4194320 | tf_op jit(solution)/shard_map/all_gather | solution.py:152
  163.4 4.5 %copy.72 = bf16[32,32,2048]{2,1,0:T(8,128)(2,1)S(1)} copy(bf16[32,32,2048]{2,0,1:T(8,128)(2,1)} %all-gather.2.cloned.1.call-done) | data formatting | bytes 8388608 | tf_op jit(solution)/shard_map/all_gather | solution.py:152
  171.7 2.5 copy.88
  174.3 6.9 %reshape.142 = bf16[8,32,32,2,128]{4,3,2,1,0:T(2,128)(2,1)} reshape(bf16[8,32,32,256]{3,2,1,0:T(8,128)(2,1)} %bitcast.156) | data formatting | bytes 8388608 | tf_op jit(solution)/shard_map/reshape | solution.py:56
  181.2 6.1 %copy.74 = bf16[2,8,32,32,128]{4,1,3,2,0:T(8,128)(2,1)S(1)} copy(bf16[2,8,32,32,128]{4,0,3,2,1:T(2,128)(2,1)} %bitcast.157) | data formatting | bytes 8388608 | tf_op jit(solution)/shard_map/transpose | solution.py:57
  187.3 8.1 %all_to_all.50 = bf16[2,8,32,32,128]{4,1,3,2,0:T(8,128)(2,1)} all-to-all(bf16[2,8,32,32,128]{4,1,3,2,0:T(8,128)(2,1)S(1)} %copy.74), channel_id=1, replica_groups=mesh['sp'=32,'tp_0'=8,'tp_1'=2] {'tp_1'}, dimensions={0} | all-to-all | bytes 8388608 | tf_op jit(solution)/shard_map/all_to_all | solution.py:62
  195.4 3.3 %reduce_sum.121 = bf16[8,32,32,128]{3,0,2,1:T(8,128)(2,1)S(1)} reduce(bf16[2,8,32,32,128]{4,1,3,2,0:T(8,128)(2,1)} %all_to_all.50, bf16[]{:T(256)} %constant.58.clone.1), dimensions={0}, to_apply=%region_10.11 | reduce | flops 1048576 | bytes 6291458 | tf_op jit(solution)/shard_map/reduce_sum | solution.py:63
  199.1 54.1 %all_to_all.51 = bf16[8,32,32,128]{3,2,1,0:T(8,128)(2,1)S(1)} all-to-all(bf16[8,32,32,128]{3,2,1,0:T(8,128)(2,1)S(1)} %copy.76), channel_id=1, replica_groups=mesh['sp'=32,'tp_0'=8,'tp_1'=2] {'tp_0'}, dimensions={0} | all-to-all | bytes 4194304 | tf_op jit(solution)/shard_map/all_to_all | solution.py:70
  254.2 9.9 %all-to-all-start.8 = ((bf16[32,32,128]{2,1,0:T(8,128)(2,1)}), bf16[32,32,128]{2,1,0:T(8,128)(2,1)S(1)}, u32[]{:S(2)}, u32[]{:S(2)}) async-start(bf16[32,32,128]{2,1,0:T(8,128)(2,1)} %reduce_sum.122), calls=%async_computation.8 | async-start | bytes 524288 | tf_op jit(solution)/shard_map/all_to_all | solution.py:162
  264.6 9.9 %all-to-all-done.8 = bf16[32,32,128]{2,1,0:T(8,128)(2,1)S(1)} async-done(((bf16[32,32,128]{2,1,0:T(8,128)(2,1)}), bf16[32,32,128]{2,1,0:T(8,128)(2,1)S(1)}, u32[]{:S(2)}, u32[]{:S(2)}) %all-to-all-start.8) | async-done | bytes 262176 | tf_op jit(solution)/shard_map/all_to_all | solution.py:162
  276.3 1.6 add_convert_fusion
  (71 shorter events, 20.9 us)
Async XLA Ops:
  6.5 163.9 %copy-start = (bf16[1,256,2048]{2,1,0:T(8,128)(2,1)S(1)}, bf16[1,256,2048]{2,1,0:T(8,128)(2,1)}, u32[]{:S(2)}) copy-start(bf16[1,256,2048]{2,1,0:T(8,128)(2,1)} %param.21) | copy-start | bytes 3145732
  6.5 28.1 %copy-start.6 = (f32[64]{0:T(128)S(1)}, f32[64]{0:T(128)}, u32[]{:S(2)}) copy-start(f32[64]{0:T(128)} %param.14) | copy-start | bytes 772
  6.5 28.1 %copy-start.3 = (bf16[64,2048]{1,0:T(8,128)(2,1)S(1)}, bf16[64,2048]{1,0:T(8,128)(2,1)}, u32[]{:S(2)}) copy-start(bf16[64,2048]{1,0:T(8,128)(2,1)} %param.15) | copy-start | bytes 786436
  7.4 9.8 %collective-permute-start = (bf16[30,64]{0,1:T(8,128)(2,1)S(1)}, bf16[30,64]{0,1:T(8,128)(2,1)S(1)}, u32[]{:S(2)}, u32[]{:S(2)}) collective-permute-start(bf16[30,64]{0,1:T(8,128)(2,1)S(1)} %slice.205), channel_id=1, source_target_pairs={{0,16},{16,32},{32,48},{48,64},{64,80},{80,96},{96,112},{112,128},... | collective-permute-start | bytes 11528 | tf_op jit(solution)/shard_map/ppermute | solution.py:13
  12.2 5.1 %collective-permute-start.1 = (bf16[30,64]{0,1:T(8,128)(2,1)S(1)}, bf16[30,64]{0,1:T(8,128)(2,1)S(1)}, u32[]{:S(2)}, u32[]{:S(2)}) collective-permute-start(bf16[30,64]{0,1:T(8,128)(2,1)S(1)} %slice.206), channel_id=1, source_target_pairs={{0,16},{16,32},{32,48},{48,64},{64,80},{80,96},{96,112},{112,128},... | collective-permute-start | bytes 11528 | tf_op jit(solution)/shard_map/ppermute | solution.py:13
  35.3 9.2 %copy-start.4 = (s32[256,2]{0,1:T(2,128)S(1)}, s32[256,2]{0,1:T(2,128)}, u32[]{:S(2)}) copy-start(s32[256,2]{0,1:T(2,128)} %param.17) | copy-start | bytes 6148
  41.0 21.4 %all-to-all-start.2 = ((bf16[8,16,2048]{2,1,0:T(8,128)(2,1)}), bf16[8,16,2048]{2,1,0:T(8,128)(2,1)S(1)}, u32[]{:S(2)}, u32[]{:S(2)}) async-start(bf16[8,16,2048]{2,1,0:T(8,128)(2,1)} %reduce_sum.116), calls=%async_computation.2 | async-start | bytes 1048576 | tf_op jit(solution)/shard_map/all_to_all | solution.py:70
  63.4 21.4 %all-to-all-start.3 = ((bf16[8,16,2048]{2,1,0:T(8,128)(2,1)}), bf16[8,16,2048]{2,1,0:T(8,128)(2,1)S(1)}, u32[]{:S(2)}, u32[]{:S(2)}) async-start(bf16[8,16,2048]{2,1,0:T(8,128)(2,1)} %broadcast_in_dim.18), calls=%async_computation.3 | async-start | bytes 1048576 | tf_op jit(solution)/shard_map/all_to_all | solution.py:18
  66.9 96.5 %all-gather.2.cloned.1.call-start = ((), (), s32[]{:S(2)}) async-start(), calls=%async_computation.9 | async-start | bytes 4456448 | tf_op jit(solution)/shard_map/all_gather | solution.py:152
  89.8 1.2 copy-start.2
  91.4 1.4 copy-start.1
  126.7 41.1 %copy-start.7 = (bf16[1,2048,256]{2,1,0:T(8,128)(2,1)S(1)}, bf16[1,2048,256]{2,1,0:T(8,128)(2,1)}, u32[]{:S(2)}) copy-start(bf16[1,2048,256]{2,1,0:T(8,128)(2,1)} %param.19) | copy-start | bytes 3145732
  167.9 1.3 copy-start.8
  253.2 11.3 %copy-start.5 = (f32[256,2]{0,1:T(2,128)S(1)}, f32[256,2]{0,1:T(2,128)}, u32[]{:S(2)}) copy-start(f32[256,2]{0,1:T(2,128)} %param.18) | copy-start | bytes 6148
  254.2 20.3 %all-to-all-start.8 = ((bf16[32,32,128]{2,1,0:T(8,128)(2,1)}), bf16[32,32,128]{2,1,0:T(8,128)(2,1)S(1)}, u32[]{:S(2)}, u32[]{:S(2)}) async-start(bf16[32,32,128]{2,1,0:T(8,128)(2,1)} %reduce_sum.122), calls=%async_computation.8 | async-start | bytes 524288 | tf_op jit(solution)/shard_map/all_to_all | solution.py:162
Sparse Core Ops, SparseCore 0:
  126.8 36.4 all-gather.1
where the time goes:
time: 287 us; the launch traced here: 285 us
  blocking collectives  112 us (39%)
  waiting for transfers between devices  79.9 us (28%)
  local copies, waits for them, and re-layouts  36.6 us (13%)
  starting transfers between devices  24 us (8%)
  between operations  13.8 us (5%)
  other arithmetic  13.7 us (5%)
  matrix products  4.37 us (2%)
    all_to_all x1, blocking collectives, sum_in_two_steps(): lax.all_to_all(nearer.astype(jnp.bfloat16), far, split_axis=0, concat_axi...  54.1 us
    all_gather x1, waiting for transfers between devices, local(): block = lax.all_gather(arrived, TP, axis=1, tiled=True)  36.6 us
    all_to_all x1, blocking collectives, local(): lax.all_to_all(mine, 'sp', split_axis=0, concat_axis=0, tiled=True)  25.3 us
    all_to_all x2, blocking collectives, sent_to_all(): lax.all_to_all(jnp.broadcast_to(value[None], (size, *value.shape)), axis,...  20.2 us
    all_to_all x1, waiting for transfers between devices, sent_to_all(): lax.all_to_all(jnp.broadcast_to(value[None], (size, *value.shape)), axis,...  17.5 us
    all_to_all x1, waiting for transfers between devices, sum_in_two_steps(): lax.all_to_all(nearer.astype(jnp.bfloat16), far, split_axis=0, concat_axi...  15.9 us
    all_to_all x2, blocking collectives, summed_on_arrival(): blocks = lax.all_to_all(split_up(value, dim, size), axis, 0, 0, tiled=True)  12.7 us
    all_to_all x1, waiting for transfers between devices, local(): back = lax.all_to_all(summed, 'sp', split_axis=0, concat_axis=0, tiled=True)  9.92 us
  transfers between devices with their start and end apart: 6, of which 4 were waited for; matrix products, arithmetic and copies ran while one was open for 2% of the time, Pallas kernels for 0%

commit v1 on v0

v1 whole, which is shorter than its diff:
```python
import jax
import jax.numpy as jnp
from jax import lax
from jax.experimental import pallas as pl
from jax.experimental.pallas import tpu as pltpu
from jax.sharding import Mesh
from jax.sharding import PartitionSpec as P

TP = ("y", "c")
VMEM = pl.BlockSpec(memory_space=pltpu.VMEM)
SMEM = pl.BlockSpec(memory_space=pltpu.SMEM)
F32 = jnp.float32
BF16 = jnp.bfloat16


def pieces(value):
    first = lax.reduce_precision(value, 8, 7)
    second = lax.reduce_precision(value - first, 8, 7)
    third = lax.reduce_precision(value - first - second, 8, 7)
    return first, second, third


def twin(value):
    return lax.ppermute(value, "c", [(0, 1), (1, 0)])


def across(contract_left, contract_right):
    return (((contract_left,), (contract_right,)), ((), ()))


def token_kernel(core_ref, rows_ref, own_ref, other_ref, res_ref, ids_ref, upd_ref, send_ref, rank_ref):
    core = core_ref[0]
    blocks, _, group, tokens = rows_ref.shape
    half = blocks * group
    width = res_ref.shape[1]
    own = rows_ref[:, core].reshape(half, tokens).astype(F32)
    other = rows_ref[:, 1 - core].reshape(half, tokens).astype(F32)
    channels = 2 * half
    total = jnp.sum(own, axis=0, keepdims=True) + jnp.sum(other, axis=0, keepdims=True)
    squares = jnp.sum(own * own, axis=0, keepdims=True) + jnp.sum(other * other, axis=0, keepdims=True)
    average = total / channels
    variance = squares / channels - average * average
    scale = lax.rsqrt(variance + 1e-05)
    mixed = jnp.zeros((tokens, width), F32)
    for values, weight_ref in ((own, own_ref), (other, other_ref)):
        weight = weight_ref[...].reshape(half, weight_ref.shape[2])
        parts = weight[:, width : width + 128].astype(F32)
        gain = parts[:, 0:1] + parts[:, 1:2] + parts[:, 2:3]
        normed = (values - average) * scale * gain
        activated = (normed / (1.0 + jnp.exp(-normed))).astype(BF16)
        mixed = mixed + lax.dot_general(
            activated, weight[:, :width], across(0, 0), preferred_element_type=F32
        )
    updated = res_ref[...].astype(F32) + mixed
    upd_ref[...] = updated
    experts, slots = send_ref.shape[:2]
    expert = lax.broadcasted_iota(jnp.int32, (experts, tokens), 0)
    named = (ids_ref[0:1, :] == expert) | (ids_ref[1:2, :] == expert)
    before = lax.broadcasted_iota(jnp.int32, (tokens, tokens), 0)
    after = lax.broadcasted_iota(jnp.int32, (tokens, tokens), 1)
    earlier = jnp.dot(
        named.astype(F32).astype(BF16),
        (before < after).astype(F32).astype(BF16),
        preferred_element_type=F32,
    )
    rank = jnp.where(named, earlier, -1.0)
    rank_ref[...] = rank
    slot = lax.broadcasted_iota(jnp.int32, (experts, slots, tokens), 1) + core * slots
    pick = (rank[:, None, :] == slot.astype(F32)).astype(F32).astype(BF16)
    sent = jnp.dot(
        pick.reshape(experts * slots, tokens), updated.astype(BF16), preferred_element_type=F32
    )
    send_ref[...] = sent.astype(BF16).reshape(experts, slots, width)


def expert_kernel(x_ref, g0_ref, g1_ref, u0_ref, u1_ref, d0_ref, d1_ref, out_ref):
    chunks, rows, width = x_ref.shape
    x = jnp.concatenate([x_ref[i] for i in range(chunks)], axis=1)
    squares = jnp.zeros((rows, 1), F32)
    for i in range(chunks):
        part = x_ref[i].astype(F32)
        squares = squares + jnp.sum(part * part, axis=1, keepdims=True)
    scale = lax.rsqrt(squares / (chunks * width) + 1e-06)
    result = jnp.zeros((rows, chunks * width), F32)
    for g_ref, u_ref, d_ref in ((g0_ref, u0_ref, d0_ref), (g1_ref, u1_ref, d1_ref)):
        gate = jnp.dot(x, g_ref[...], preferred_element_type=F32) * scale
        up = jnp.dot(x, u_ref[...], preferred_element_type=F32) * scale
        hidden = (gate / (1.0 + jnp.exp(-gate)) * up).astype(BF16)
        result = result + jnp.dot(hidden, d_ref[...], preferred_element_type=F32)
    for i in range(chunks):
        out_ref[i] = result[:, i * width : (i + 1) * width].astype(BF16)


def combine_kernel(core_ref, back_ref, rank_ref, ids_ref, w_ref, out_ref):
    core = core_ref[0]
    experts, slots, width = back_ref.shape
    tokens = rank_ref.shape[1]
    expert = lax.broadcasted_iota(jnp.int32, (experts, tokens), 0)
    weight = jnp.where(ids_ref[0:1, :] == expert, w_ref[0:1, :], 0.0) + jnp.where(
        ids_ref[1:2, :] == expert, w_ref[1:2, :], 0.0
    )
    slot = lax.broadcasted_iota(jnp.int32, (experts, slots, tokens), 1) + core * slots
    here = rank_ref[...][:, None, :] == slot.astype(F32)
    spread = jnp.where(here, weight[:, None, :], 0.0).reshape(experts * slots, tokens)
    back = back_ref[...].reshape(experts * slots, width)
    total = jnp.zeros((tokens, width), F32)
    for _ in range(3):
        piece = spread.astype(BF16)
        spread = spread - piece.astype(F32)
        total = total + lax.dot_general(piece, back, across(0, 0), preferred_element_type=F32)
    out_ref[...] = total


def local(
    conv_value,
    conv_gate,
    conv_taps,
    conv_gain,
    out_weight,
    residual,
    route_ids,
    route_weight,
    expert_gate,
    expert_up,
    expert_down,
):
    chips, experts = lax.axis_size("y"), lax.axis_size("sp")
    chip, core = lax.axis_index("y"), lax.axis_index("c")
    core_arg = core.astype(jnp.int32).reshape(1)
    taps_count, group = conv_taps.shape
    tokens = conv_value.shape[0]
    model = residual.shape[1]
    width = model // chips

    lanes = jnp.stack(pieces(conv_gain), axis=1).astype(BF16)
    lanes = jnp.broadcast_to(jnp.pad(lanes, ((0, 0), (0, 125)))[None], (chips, group, 128))
    columns = jnp.moveaxis(out_weight.reshape(group, chips, width), 1, 0)
    own_out = lax.all_to_all(jnp.concatenate([columns, lanes], axis=2), "y", 0, 0, tiled=True)
    other_out = twin(own_out)
    gates = (expert_gate[0], twin(expert_gate[0]))
    ups = (expert_up[0], twin(expert_up[0]))
    downs = (expert_down[0], twin(expert_down[0]))

    value, gate = conv_value.T.astype(F32), conv_gate.T.astype(F32)
    gated = value * jax.nn.sigmoid(gate)
    order = lax.axis_size("sp")
    head = lax.ppermute(
        gated[:, tokens - taps_count + 1 :], "sp", [(i, i + 1) for i in range(order - 1)]
    )
    gated = jnp.concatenate([head, gated], axis=1)
    taps = conv_taps.T.astype(F32)
    filtered = jnp.zeros((group, tokens), F32)
    for offset in range(taps_count):
        filtered = filtered + taps[:, offset : offset + 1] * gated[:, offset : offset + tokens]
    rows = lax.all_gather(filtered.astype(BF16), TP, axis=0, tiled=True)
    rows = rows.reshape(chips, 2, group, tokens)

    ids, weights = route_ids.T, route_weight.T
    res = lax.dynamic_slice_in_dim(residual, chip * width, width, 1)
    slots = 2 * tokens * route_ids.shape[1] // experts // 2
    updated, send, rank = pl.pallas_call(
        token_kernel,
        out_shape=(
            jax.ShapeDtypeStruct((tokens, width), F32),
            jax.ShapeDtypeStruct((experts, slots, width), BF16),
            jax.ShapeDtypeStruct((experts, tokens), F32),
        ),
        in_specs=[SMEM] + [VMEM] * 5,
        out_specs=(VMEM,) * 3,
        name="token",
    )(core_arg, rows, own_out, other_out, res, ids)

    arrived = lax.all_to_all(send, "sp", 0, 0, tiled=True).reshape(1, experts * slots, width)
    full = lax.all_gather(arrived, "y", axis=0, tiled=True)
    partial = pl.pallas_call(
        expert_kernel,
        out_shape=jax.ShapeDtypeStruct(full.shape, BF16),
        in_specs=[VMEM] * 7,
        out_specs=VMEM,
        name="expert",
    )(full, *gates, *ups, *downs)
    summed = lax.psum_scatter(partial, "y", scatter_dimension=0, tiled=True)
    back = lax.all_to_all(
        summed.reshape(experts, slots, width), "sp", 0, 0, tiled=True
    )
    part = pl.pallas_call(
        combine_kernel,
        out_shape=jax.ShapeDtypeStruct((tokens, width), F32),
        in_specs=[SMEM] + [VMEM] * 4,
        out_specs=VMEM,
        name="combine",
    )(core_arg, back, rank, ids, weights)
    mine = width // 2
    given = lax.dynamic_slice_in_dim(part, (1 - core) * mine, mine, 1)
    kept = lax.dynamic_slice_in_dim(part, core * mine, mine, 1)
    kept = kept + lax.dynamic_slice_in_dim(updated, core * mine, mine, 1)
    return (kept + twin(given)).astype(BF16)


def solution(mesh):
    grid = Mesh(mesh.devices.reshape(mesh.shape["sp"], 8, 2), ("sp", "y", "c"))
    placed = (
        P("sp", TP),
        P("sp", TP),
        P(None, TP),
        P(TP),
        P(TP, None),
        P("sp", None),
        P("sp", None),
        P("sp", None),
        P("sp", None, TP),
        P("sp", None, TP),
        P("sp", TP, None),
    )
    return jax.shard_map(local, mesh=grid, in_specs=placed, out_specs=P("sp", TP), check_vma=False)
```

time: 287 us -> 218 us (0.76)
  blocking collectives: 112 us -> 41.1 us
  local copies, waits for them, and re-layouts: 36.6 us -> 8.56 us
  starting transfers between devices: 24 us -> 42 us
  Pallas kernels: 0 us -> 13.6 us
  waiting for transfers between devices: 79.9 us -> 89.2 us
  other arithmetic: 13.7 us -> 9.09 us
  matrix products: 4.37 us -> 0 us
    all_to_all x6 -> x1, blocking collectives: 112 us -> 23.7 us  [local(): lax.all_to_all(send, 'sp', 0, 0, tiled=True)]
    reduce_scatter x0 -> x1, waiting for transfers between devices: none -> 43.9 us  [local(): summed = lax.psum_scatter(partial, 'y', scatter_dimension=0, tiled=True)]
    all_to_all x3 -> x2, waiting for transfers between devices: 43.3 us -> 21.9 us  [the longest x1 11.5 us: local(): lax.all_to_all(jnp.concatenate([columns, lanes], axis=2), 'y', 0, 0, tile...]
    ppermute x2 -> x6, starting transfers between devices: 7.03 us -> 25.1 us  [the longest x5 20.5 us: twin(): return lax.ppermute(value, 'c', [(0, 1), (1, 0)])]
    all_gather x0 -> x1, blocking collectives: none -> 17.4 us  [local(): rows = lax.all_gather(filtered.astype(BF16), TP, axis=0, tiled=True)]
    all_gather x1, waiting for transfers between devices: 36.6 us -> 21.5 us  [local(): full = lax.all_gather(arrived, 'y', axis=0, tiled=True)]
    pallas_call x0 -> x3, Pallas kernels: none -> 13.6 us  [the longest x1 8.17 us: local(): pl.pallas_call(expert_kernel, out_shape=jax.ShapeDtypeStruct(full.shape,...]
    reshape x3 -> x1, local copies, waits for them, and re-layouts: 9.58 us -> 0.97 us  [local(): columns = jnp.moveaxis(out_weight.reshape(group, chips, width), 1, 0)]
  transfers between devices with their start and end apart: 6 -> 10, of which waited for: 4 -> 7; matrix products, arithmetic and copies ran while one was open for 2% -> 4% of each run, Pallas kernels for 0% -> 0%
where the time goes in v1:
time: 218 us; the launch traced here: 217 us
  waiting for transfers between devices  89.2 us (41%)
  starting transfers between devices  42 us (19%)
  blocking collectives  41.1 us (19%)
  Pallas kernels  13.6 us (6%)
  between operations  13.6 us (6%)
  other arithmetic  9.09 us (4%)
  local copies, waits for them, and re-layouts  8.56 us (4%)
    reduce_scatter x1, waiting for transfers between devices, local(): summed = lax.psum_scatter(partial, 'y', scatter_dimension=0, tiled=True)  43.9 us
    all_to_all x1, blocking collectives, local(): lax.all_to_all(send, 'sp', 0, 0, tiled=True)  23.7 us
    all_gather x1, waiting for transfers between devices, local(): full = lax.all_gather(arrived, 'y', axis=0, tiled=True)  21.5 us
    ppermute x5, starting transfers between devices, twin(): return lax.ppermute(value, 'c', [(0, 1), (1, 0)])  20.5 us
    all_gather x1, blocking collectives, local(): rows = lax.all_gather(filtered.astype(BF16), TP, axis=0, tiled=True)  17.4 us
    all_to_all x1, waiting for transfers between devices, local(): lax.all_to_all(jnp.concatenate([columns, lanes], axis=2), 'y', 0, 0, tile...  11.5 us
    all_to_all x1, waiting for transfers between devices, local(): lax.all_to_all(summed.reshape(experts, slots, width), 'sp', 0, 0, tiled=T...  10.5 us
    all_to_all x1, starting transfers between devices, local(): lax.all_to_all(summed.reshape(experts, slots, width), 'sp', 0, 0, tiled=T...  9.9 us
  transfers between devices with their start and end apart: 10, of which 7 were waited for; matrix products, arithmetic and copies ran while one was open for 4% of the time, Pallas kernels for 0%

profile of v1, /device:TPU:1, one launch (start us, length us, event | category | flops | bytes accessed | tf_op | source)
XLA Modules:
  0.0 217.1 jit_solution(2926802791243704495)
XLA Ops:
  6.5 0.9 multiply_bitcast_fusion
  8.8 4.5 %collective-permute-start = (f32[64,30]{1,0:T(8,128)}, f32[64,30]{1,0:T(8,128)}, u32[]{:S(2)}, u32[]{:S(2)}) collective-permute-start(f32[64,30]{1,0:T(8,128)} %slice.249), channel_id=1, source_target_pairs={{0,16},{16,32},{32,48},{48,64},{64,80},{80,96},{96,112},{112,128},... | collective-permute-start | bytes 23048 | tf_op jit(solution)/shard_map/ppermute | solution.py:147
  14.1 1.0 copy.20
  15.9 7.0 %all-to-all-start = ((bf16[8,64,384]{2,1,0:T(8,128)(2,1)}), bf16[8,64,384]{2,1,0:T(8,128)(2,1)S(1)}, u32[]{:S(2)}, u32[]{:S(2)}) async-start(bf16[8,64,384]{2,1,0:T(8,128)(2,1)} %pad_maximum_fusion), calls=%async_computation | async-start | bytes 786432 | tf_op jit(solution)/shard_map/all_to_all | solution.py:138
  24.9 11.5 %all-to-all-done.own_ref = bf16[8,64,384]{2,1,0:T(8,128)(2,1)S(1)} async-done(((bf16[8,64,384]{2,1,0:T(8,128)(2,1)}), bf16[8,64,384]{2,1,0:T(8,128)(2,1)S(1)}, u32[]{:S(2)}, u32[]{:S(2)}) %all-to-all-start) | async-done | bytes 393248 | tf_op jit(solution)/shard_map/all_to_all | solution.py:138
  36.4 4.0 %collective-permute-start.1 = (bf16[8,64,384]{2,1,0:T(8,128)(2,1)S(1)}, bf16[8,64,384]{2,1,0:T(8,128)(2,1)S(1)}, u32[]{:S(2)}, u32[]{:S(2)}) collective-permute-start(bf16[8,64,384]{2,1,0:T(8,128)(2,1)S(1)} %all-to-all-done.own_ref), channel_id=1, source_target_pairs={{0,1},{1,0},{2,3},{3,2},{4,5},{5,4},{6,7},{7,6},{8,9},{9,8},{10,11... | collective-permute-start | bytes 1179656 | tf_op jit(solution)/shard_map/ppermute | solution.py:24
  40.4 5.1 %fusion.5 = bf16[64,256]{1,0:T(8,128)(2,1)S(1)} fusion(f32[64,256]{1,0:T(8,128)} %copy-done.7, f32[64,30]{1,0:T(8,128)} %collective-permute-done, f32[64]{0:T(128)} %get-tuple-element.12, f32[64]{0:T(128)} %get-tuple-element.13, f32[64]{0:T(128)} %get-tuple-element.14, f32[64]{0:T(128)} %get-tuple-element.15, f32[64]{0:T(128)} %get-tuple-element.16, ...), kind=kLoop, calls=%fused_computation.66 | loop fusion | flops 1507328 | bytes 113920 | tf_op jit(solution)/shard_map/convert_element_type | solution.py:155
  45.6 17.4 %all_gather.6 = bf16[1024,256]{1,0:T(8,128)(2,1)} all-gather(bf16[64,256]{1,0:T(8,128)(2,1)S(1)} %fusion.5), channel_id=1, replica_groups=mesh['sp'=32,'y'=8,'c'=2] {'y','c'}, dimensions={0}, use_global_device_ids=true | all-gather | bytes 557056 | tf_op jit(solution)/shard_map/all_gather | solution.py:155
  63.7 3.3 %token_.1 = (f32[256,256]{1,0:T(8,128)}, bf16[32,16,256]{2,1,0:T(8,128)(2,1)}, f32[32,256]{1,0:T(8,128)}) custom-call(s32[1]{0:T(128)} %bitcast.core_ref, bf16[8,2,64,256]{3,2,1,0:T(8,128)(2,1)} %bitcast.88, bf16[8,64,384]{2,1,0:T(8,128)(2,1)} %copy-done.1, bf16[8,64,384]{2,1,0:T(8,128)(2,1)} %copy-done.8, ...), custom_call_target="tpu_custom_call" | custom-call | tf_op jit(solution)/shard_map/token/pallas_call | solution.py:161
  67.0 23.7 %all_to_all.15 = bf16[32,16,256]{2,1,0:T(8,128)(2,1)} all-to-all(bf16[32,16,256]{2,1,0:T(8,128)(2,1)} %get-tuple-element.8), channel_id=1, replica_groups=mesh['sp'=32,'y'=8,'c'=2] {'sp'}, dimensions={0} | all-to-all | bytes 524288 | tf_op jit(solution)/shard_map/all_to_all | solution.py:173
  90.8 4.3 %collective-permute-start.2 = (bf16[2048,256]{1,0:T(8,128)(2,1)S(1)}, bf16[2048,256]{1,0:T(8,128)(2,1)S(1)}, u32[]{:S(2)}, u32[]{:S(2)}) collective-permute-start(bf16[2048,256]{1,0:T(8,128)(2,1)S(1)} %bitcast.90), channel_id=1, source_target_pairs={{0,1},{1,0},{2,3},{3,2},{4,5},{5,4},{6,7},{7,6},{8,9},{9,8},{10,11... | collective-permute-start | bytes 3145736 | tf_op jit(solution)/shard_map/ppermute | solution.py:24
  95.1 1.9 collective-permute-start.3
  97.0 2.4 %collective-permute-start.4 = (bf16[256,2048]{1,0:T(8,128)(2,1)}, bf16[256,2048]{1,0:T(8,128)(2,1)}, u32[]{:S(2)}, u32[]{:S(2)}) collective-permute-start(bf16[256,2048]{1,0:T(8,128)(2,1)} %bitcast.93), channel_id=1, source_target_pairs={{0,1},{1,0},{2,3},{3,2},{4,5},{5,4},{6,7},{7,6},{8,9},{9,8},{10,11... | collective-permute-start | bytes 3145736 | tf_op jit(solution)/shard_map/ppermute | solution.py:24
  100.5 1.0 copy-done.5
  102.1 21.5 %all-gather.2.cloned.1.call-done.x_ref = bf16[8,512,256]{2,1,0:T(8,128)(2,1)} async-done(((bf16[1,512,256]{2,1,0:T(8,128)(2,1)}), bf16[8,512,256]{2,1,0:T(8,128)(2,1)}) %all-gather.2.cloned.1.call-update) | async-done | bytes 2097168 | tf_op jit(solution)/shard_map/all_gather | solution.py:174
  123.6 8.2 %expert.1 = bf16[8,512,256]{2,1,0:T(8,128)(2,1)} custom-call(bf16[8,512,256]{2,1,0:T(8,128)(2,1)} %all-gather.2.cloned.1.call-done.x_ref, bf16[2048,256]{1,0:T(8,128)(2,1)} %bitcast.89, bf16[2048,256]{1,0:T(8,128)(2,1)} %copy-done.4, bf16[2048,256]{1,0:T(8,128)(2,1)} %bitcast.91, bf16[2048,256]{1,0:T(8,128)(2,1)} %copy-done.5, bf16[256,2048]{1,0:T(8,128)(2,1)} %bitcast.94, ...), custom_call_target="tpu_custom_call" | custom-call | tf_op jit(solution)/shard_map/expert/pallas_call | solution.py:175
  131.8 43.9 %reduce-scatter.2.cloned.1.call-done = bf16[1,512,256]{2,1,0:T(8,128)(2,1)} async-done(((bf16[8,512,256]{2,1,0:T(8,128)(2,1)}), bf16[1,512,256]{2,1,0:T(8,128)(2,1)}) %reduce-scatter.2.cloned.1.call-update) | async-done | bytes 262160 | tf_op jit(solution)/shard_map/reduce_scatter | solution.py:182
  175.7 9.9 %all-to-all-start.2 = ((bf16[32,16,256]{2,1,0:T(8,128)(2,1)}), bf16[32,16,256]{2,1,0:T(8,128)(2,1)S(1)}, u32[]{:S(2)}, u32[]{:S(2)}) async-start(bf16[32,16,256]{2,1,0:T(8,128)(2,1)} %bitcast.98), calls=%async_computation.3 | async-start | bytes 524288 | tf_op jit(solution)/shard_map/all_to_all | solution.py:183
  185.6 10.5 %all-to-all-done.2.back_ref = bf16[32,16,256]{2,1,0:T(8,128)(2,1)S(1)} async-done(((bf16[32,16,256]{2,1,0:T(8,128)(2,1)}), bf16[32,16,256]{2,1,0:T(8,128)(2,1)S(1)}, u32[]{:S(2)}, u32[]{:S(2)}) %all-to-all-start.2) | async-done | bytes 262176 | tf_op jit(solution)/shard_map/all_to_all | solution.py:183
  196.8 2.2 combine.1
  198.9 0.9 constant_dynamic-slice_fusion
  199.8 7.9 %collective-permute-start.5 = (f32[256,128]{1,0:T(8,128)S(1)}, f32[256,128]{1,0:T(8,128)S(1)}, u32[]{:S(2)}, u32[]{:S(2)}) collective-permute-start(f32[256,128]{1,0:T(8,128)S(1)} %constant_dynamic-slice_fusion), channel_id=1, source_target_pairs={{0,1},{1,0},{2,3},{3,2},{4,5},{5,4},{6,7},{7,6},{8,9},{9,8},{10,11... | collective-permute-start | bytes 393224 | tf_op jit(solution)/shard_map/ppermute | solution.py:24
  207.8 1.0 collective-permute-done.5
  208.7 1.6 add_convert_fusion
  (41 shorter events, 8.1 us)
Async XLA Ops:
  6.5 17.7 %copy-start = (bf16[256,2048]{1,0:T(8,128)(2,1)S(1)}, bf16[256,2048]{1,0:T(8,128)(2,1)}, u32[]{:S(2)}) copy-start(bf16[256,2048]{1,0:T(8,128)(2,1)} %param.16) | copy-start | bytes 3145732
  6.5 16.4 %copy-start.10 = (bf16[31,64]{1,0:T(8,128)(2,1)S(1)}, bf16[31,64]{1,0:T(8,128)(2,1)}, u32[]{:S(2)}) copy-start(bf16[31,64]{1,0:T(8,128)(2,1)} %param.13) | copy-start | bytes 11908
  7.4 0.6 copy-start.7
  8.8 31.6 %collective-permute-start = (f32[64,30]{1,0:T(8,128)}, f32[64,30]{1,0:T(8,128)}, u32[]{:S(2)}, u32[]{:S(2)}) collective-permute-start(f32[64,30]{1,0:T(8,128)} %slice.249), channel_id=1, source_target_pairs={{0,16},{16,32},{32,48},{48,64},{64,80},{80,96},{96,112},{112,128},... | collective-permute-start | bytes 23048 | tf_op jit(solution)/shard_map/ppermute | solution.py:147
  15.9 74.9 %copy-start.2 = (bf16[1,2048,256]{2,1,0:T(8,128)(2,1)S(1)}, bf16[1,2048,256]{2,1,0:T(8,128)(2,1)}, u32[]{:S(2)}) copy-start(bf16[1,2048,256]{2,1,0:T(8,128)(2,1)} %param.19) | copy-start | bytes 3145732
  15.9 79.2 %copy-start.3 = (bf16[1,2048,256]{2,1,0:T(8,128)(2,1)S(1)}, bf16[1,2048,256]{2,1,0:T(8,128)(2,1)}, u32[]{:S(2)}) copy-start(bf16[1,2048,256]{2,1,0:T(8,128)(2,1)} %param.20) | copy-start | bytes 3145732
  15.9 20.5 %all-to-all-start = ((bf16[8,64,384]{2,1,0:T(8,128)(2,1)}), bf16[8,64,384]{2,1,0:T(8,128)(2,1)S(1)}, u32[]{:S(2)}, u32[]{:S(2)}) async-start(bf16[8,64,384]{2,1,0:T(8,128)(2,1)} %pad_maximum_fusion), calls=%async_computation | async-start | bytes 786432 | tf_op jit(solution)/shard_map/all_to_all | solution.py:138
  22.9 100.7 %all-gather.2.cloned.1.call-start = ((), (), s32[]{:S(2)}) async-start(), calls=%async_computation.4 | async-start | bytes 2359296 | tf_op jit(solution)/shard_map/all_gather | solution.py:174
  36.4 27.3 %copy-start.1 = (bf16[8,64,384]{2,1,0:T(8,128)(2,1)}, bf16[8,64,384]{2,1,0:T(8,128)(2,1)S(1)}, u32[]{:S(2)}) copy-start(bf16[8,64,384]{2,1,0:T(8,128)(2,1)S(1)} %all-to-all-done.own_ref) | copy-start | bytes 1179652
  36.4 26.6 %collective-permute-start.1 = (bf16[8,64,384]{2,1,0:T(8,128)(2,1)S(1)}, bf16[8,64,384]{2,1,0:T(8,128)(2,1)S(1)}, u32[]{:S(2)}, u32[]{:S(2)}) collective-permute-start(bf16[8,64,384]{2,1,0:T(8,128)(2,1)S(1)} %all-to-all-done.own_ref), channel_id=1, source_target_pairs={{0,1},{1,0},{2,3},{3,2},{4,5},{5,4},{6,7},{7,6},{8,9},{9,8},{10,11... | collective-permute-start | bytes 1179656 | tf_op jit(solution)/shard_map/ppermute | solution.py:24
  62.9 0.8 copy-start.8
  90.8 84.9 %reduce-scatter.2.cloned.1.call-start = ((), (), s32[]{:S(2)}) async-start(), calls=%async_computation.5 | async-start | bytes 2359296 | tf_op jit(solution)/shard_map/reduce_scatter | solution.py:182
  90.8 8.6 %collective-permute-start.2 = (bf16[2048,256]{1,0:T(8,128)(2,1)S(1)}, bf16[2048,256]{1,0:T(8,128)(2,1)S(1)}, u32[]{:S(2)}, u32[]{:S(2)}) collective-permute-start(bf16[2048,256]{1,0:T(8,128)(2,1)S(1)} %bitcast.90), channel_id=1, source_target_pairs={{0,1},{1,0},{2,3},{3,2},{4,5},{5,4},{6,7},{7,6},{8,9},{9,8},{10,11... | collective-permute-start | bytes 3145736 | tf_op jit(solution)/shard_map/ppermute | solution.py:24
  95.1 4.6 %collective-permute-start.3 = (bf16[2048,256]{1,0:T(8,128)(2,1)S(1)}, bf16[2048,256]{1,0:T(8,128)(2,1)S(1)}, u32[]{:S(2)}, u32[]{:S(2)}) collective-permute-start(bf16[2048,256]{1,0:T(8,128)(2,1)S(1)} %bitcast.92), channel_id=1, source_target_pairs={{0,1},{1,0},{2,3},{3,2},{4,5},{5,4},{6,7},{7,6},{8,9},{9,8},{10,11... | collective-permute-start | bytes 3145736 | tf_op jit(solution)/shard_map/ppermute | solution.py:24
  97.0 5.0 %collective-permute-start.4 = (bf16[256,2048]{1,0:T(8,128)(2,1)}, bf16[256,2048]{1,0:T(8,128)(2,1)}, u32[]{:S(2)}, u32[]{:S(2)}) collective-permute-start(bf16[256,2048]{1,0:T(8,128)(2,1)} %bitcast.93), channel_id=1, source_target_pairs={{0,1},{1,0},{2,3},{3,2},{4,5},{5,4},{6,7},{7,6},{8,9},{9,8},{10,11... | collective-permute-start | bytes 3145736 | tf_op jit(solution)/shard_map/ppermute | solution.py:24
  99.5 1.0 copy-start.4
  100.5 1.0 copy-start.5
  131.7 77.0 %copy-start.9 = (f32[256,256]{1,0:T(8,128)S(1)}, f32[256,256]{1,0:T(8,128)}, u32[]{:S(2)}) copy-start(f32[256,256]{1,0:T(8,128)} %get-tuple-element.10) | copy-start | bytes 786436
  175.7 20.4 %all-to-all-start.2 = ((bf16[32,16,256]{2,1,0:T(8,128)(2,1)}), bf16[32,16,256]{2,1,0:T(8,128)(2,1)S(1)}, u32[]{:S(2)}, u32[]{:S(2)}) async-start(bf16[32,16,256]{2,1,0:T(8,128)(2,1)} %bitcast.98), calls=%async_computation.3 | async-start | bytes 524288 | tf_op jit(solution)/shard_map/all_to_all | solution.py:183
  196.1 0.7 copy-start.6
  199.8 8.9 %collective-permute-start.5 = (f32[256,128]{1,0:T(8,128)S(1)}, f32[256,128]{1,0:T(8,128)S(1)}, u32[]{:S(2)}, u32[]{:S(2)}) collective-permute-start(f32[256,128]{1,0:T(8,128)S(1)} %constant_dynamic-slice_fusion), channel_id=1, source_target_pairs={{0,1},{1,0},{2,3},{3,2},{4,5},{5,4},{6,7},{7,6},{8,9},{9,8},{10,11... | collective-permute-start | bytes 393224 | tf_op jit(solution)/shard_map/ppermute | solution.py:24
Sparse Core Ops, SparseCore 0:
  90.9 32.6 all-gather.1
  131.9 43.7 reduce-scatter.1

commit v2 on v1

v2 whole, which is shorter than its diff:
```python
import jax
import jax.numpy as jnp
from jax import lax
from jax.experimental import pallas as pl
from jax.experimental.pallas import tpu as pltpu
from jax.sharding import Mesh
from jax.sharding import PartitionSpec as P

TP = ("y", "c")
VMEM = pl.BlockSpec(memory_space=pltpu.VMEM)
SMEM = pl.BlockSpec(memory_space=pltpu.SMEM)
HBM = pl.BlockSpec(memory_space=pltpu.HBM)
F32 = jnp.float32
BF16 = jnp.bfloat16


def twin(value):
    return lax.ppermute(value, "c", [(0, 1), (1, 0)])


def across(contract_left, contract_right):
    return (((contract_left,), (contract_right,)), ((), ()))


def room(mebibytes):
    return pltpu.CompilerParams(vmem_limit_bytes=mebibytes << 20)


def near(value):
    return pltpu.with_memory_space_constraint(value, pltpu.VMEM)


def far(value):
    return pltpu.with_memory_space_constraint(value, pltpu.HBM)


def gate_kernel(value_ref, gate_ref, out_ref, tail_ref):
    value, gate = value_ref[...].astype(F32), gate_ref[...].astype(F32)
    gated = value * (1.0 / (1.0 + jnp.exp(-gate)))
    out_ref[...] = gated
    tail_ref[...] = gated[:, gated.shape[1] - tail_ref.shape[1] :]


def pack_kernel(weight_ref, gain_ref, out_ref):
    chips, group, full = out_ref.shape
    width = full - 128
    rows = lax.broadcasted_iota(jnp.int32, (group, group), 0)
    lanes = lax.broadcasted_iota(jnp.int32, (group, group), 1)
    gain = jnp.sum(jnp.where(rows == lanes, gain_ref[...], 0.0), axis=1, keepdims=True)
    first = gain.astype(BF16).astype(F32)
    second = (gain - first).astype(BF16).astype(F32)
    third = gain - first - second
    lane = lax.broadcasted_iota(jnp.int32, (group, 128), 1)
    extra = jnp.where(lane == 0, first, jnp.where(lane == 1, second, jnp.where(lane == 2, third, 0.0)))
    extra = extra.astype(BF16)
    for i in range(chips):
        out_ref[i, :, :width] = weight_ref[:, i * width : (i + 1) * width]
        out_ref[i, :, width:] = extra


def filter_kernel(head_ref, gated_ref, taps_ref, out_ref):
    line = jnp.concatenate([head_ref[...], gated_ref[...]], axis=1)
    length, tokens = line.shape[1], out_ref.shape[1]
    count = taps_ref.shape[1]
    taps = taps_ref[...]
    total = jnp.zeros(out_ref.shape, F32)
    for i in range(count):
        begin = length - tokens - (count - 1) + i
        shifted = pltpu.roll(line, (length - begin) % length, 1)[:, :tokens]
        total = total + taps[:, i : i + 1] * shifted
    out_ref[...] = total.astype(out_ref.dtype)


def token_kernel(place_ref, rows_ref, own_ref, other_ref, ids_ref, all_ref, upd_ref, send_ref, rank_ref, res_ref, sem):
    chip, core = place_ref[0], place_ref[1]
    blocks, _, group, tokens = rows_ref.shape
    half = blocks * group
    width = res_ref.shape[1]
    columns = pl.ds(pl.multiple_of(chip * width, width), width)
    copy = pltpu.make_async_copy(all_ref.at[:, columns], res_ref, sem)
    copy.start()
    own = rows_ref[:, core].reshape(half, tokens).astype(F32)
    other = rows_ref[:, 1 - core].reshape(half, tokens).astype(F32)
    channels = 2 * half
    total = jnp.sum(own, axis=0, keepdims=True) + jnp.sum(other, axis=0, keepdims=True)
    squares = jnp.sum(own * own, axis=0, keepdims=True) + jnp.sum(other * other, axis=0, keepdims=True)
    average = total / channels
    variance = squares / channels - average * average
    scale = lax.rsqrt(variance + 1e-05)
    mixed = jnp.zeros((tokens, width), F32)
    for values, weight_ref in ((own, own_ref), (other, other_ref)):
        weight = weight_ref[...].reshape(half, weight_ref.shape[2])
        parts = weight[:, width : width + 128].astype(F32)
        gain = parts[:, 0:1] + parts[:, 1:2] + parts[:, 2:3]
        normed = (values - average) * scale * gain
        activated = (normed / (1.0 + jnp.exp(-normed))).astype(BF16)
        mixed = mixed + lax.dot_general(
            activated, weight[:, :width], across(0, 0), preferred_element_type=F32
        )
    copy.wait()
    updated = res_ref[...].astype(F32) + mixed
    mine = width // 2
    upd_ref[...] = jnp.where(core == 0, updated[:, :mine], updated[:, mine:])
    experts, slots = send_ref.shape[:2]
    expert = lax.broadcasted_iota(jnp.int32, (experts, tokens), 0)
    named = (ids_ref[0:1, :] == expert) | (ids_ref[1:2, :] == expert)
    before = lax.broadcasted_iota(jnp.int32, (tokens, tokens), 0)
    after = lax.broadcasted_iota(jnp.int32, (tokens, tokens), 1)
    earlier = jnp.dot(
        named.astype(F32).astype(BF16),
        (before < after).astype(F32).astype(BF16),
        preferred_element_type=F32,
    )
    rank = jnp.where(named, earlier, -1.0)
    rank_ref[...] = rank
    slot = lax.broadcasted_iota(jnp.int32, (experts, slots, tokens), 1) + core * slots
    pick = (rank[:, None, :] == slot.astype(F32)).astype(F32).astype(BF16)
    sent = jnp.dot(
        pick.reshape(experts * slots, tokens), updated.astype(BF16), preferred_element_type=F32
    )
    send_ref[...] = sent.astype(BF16).reshape(experts, slots, width)


def expert_kernel(x_hbm, *refs):
    weights_hbm, out_hbm = refs[:6], refs[6]
    x_ref, g0, g1, u0, u1, d0, d1, out_ref, in_sem, weight_sem, out_sem = refs[7:]
    chunks, rows, width = x_hbm.shape
    parts, part = x_ref.shape[0], x_ref.shape[2]
    ins = [
        pltpu.make_async_copy(x_hbm.at[:, pl.ds(k * part, part)], x_ref.at[k], in_sem.at[k])
        for k in range(parts)
    ]
    held = (g0, g1, u0, u1, d0, d1)
    moves = [pltpu.make_async_copy(weights_hbm[k], held[k], weight_sem.at[k]) for k in range(6)]
    ins[0].start()
    for k in (0, 2, 1, 3, 4, 5):
        moves[k].start()
    for k in range(1, parts):
        ins[k].start()
    outs = []
    for k in range(parts):
        ins[k].wait()
        x = jnp.concatenate([x_ref[k, i] for i in range(chunks)], axis=1)
        squares = jnp.zeros((part, 1), F32)
        for i in range(chunks):
            piece = x_ref[k, i].astype(F32)
            squares = squares + jnp.sum(piece * piece, axis=1, keepdims=True)
        scale = lax.rsqrt(squares / (chunks * width) + 1e-06)
        hidden = []
        for j in (0, 1):
            if k == 0:
                moves[j].wait()
            gate = jnp.dot(x, held[j][...], preferred_element_type=F32) * scale
            if k == 0:
                moves[2 + j].wait()
            up = jnp.dot(x, held[2 + j][...], preferred_element_type=F32) * scale
            hidden.append((gate / (1.0 + jnp.exp(-gate)) * up).astype(BF16))
        if k == 0:
            moves[4].wait()
            moves[5].wait()
        for i in range(chunks):
            columns = slice(i * width, (i + 1) * width)
            piece = jnp.dot(hidden[0], d0[:, columns], preferred_element_type=F32)
            piece = piece + jnp.dot(hidden[1], d1[:, columns], preferred_element_type=F32)
            out_ref[k, i] = piece.astype(BF16)
        out = pltpu.make_async_copy(out_ref.at[k], out_hbm.at[:, pl.ds(k * part, part)], out_sem.at[k])
        out.start()
        outs.append(out)
    for out in outs:
        out.wait()


def combine_kernel(place_ref, back_ref, rank_ref, ids_ref, w_ref, upd_ref, kept_ref, given_ref):
    core = place_ref[1]
    experts, slots, width = back_ref.shape
    tokens = rank_ref.shape[1]
    expert = lax.broadcasted_iota(jnp.int32, (experts, tokens), 0)
    weight = jnp.where(ids_ref[0:1, :] == expert, w_ref[0:1, :], 0.0) + jnp.where(
        ids_ref[1:2, :] == expert, w_ref[1:2, :], 0.0
    )
    slot = lax.broadcasted_iota(jnp.int32, (experts, slots, tokens), 1) + core * slots
    here = rank_ref[...][:, None, :] == slot.astype(F32)
    spread = jnp.where(here, weight[:, None, :], 0.0).reshape(experts * slots, tokens)
    back = back_ref[...].reshape(experts * slots, width)
    total = jnp.zeros((tokens, width), F32)
    for _ in range(3):
        piece = spread.astype(BF16)
        spread = spread - piece.astype(F32)
        total = total + lax.dot_general(piece, back, across(0, 0), preferred_element_type=F32)
    mine = width // 2
    low, high = total[:, :mine], total[:, mine:]
    kept_ref[...] = upd_ref[...] + jnp.where(core == 0, low, high)
    given_ref[...] = jnp.where(core == 0, high, low)


def local(
    conv_value,
    conv_gate,
    conv_taps,
    conv_gain,
    out_weight,
    residual,
    route_ids,
    route_weight,
    expert_gate,
    expert_up,
    expert_down,
):
    chips, experts = lax.axis_size("y"), lax.axis_size("sp")
    chip, core = lax.axis_index("y"), lax.axis_index("c")
    place = jnp.stack([chip, core]).astype(jnp.int32)
    taps_count, group = conv_taps.shape
    tokens = conv_value.shape[0]
    model = residual.shape[1]
    width = model // chips

    gated, tail = pl.pallas_call(
        gate_kernel,
        out_shape=(pltpu.VMEM((group, tokens), F32), pltpu.VMEM((group, 128), F32)),
        in_specs=[VMEM] * 2,
        out_specs=(VMEM,) * 2,
        compiler_params=room(4),
        name="gate",
    )(far(conv_value.T), far(conv_gate.T))
    tail, out_weight, conv_gain = lax.optimization_barrier((tail, out_weight, conv_gain))
    order = lax.axis_size("sp")
    head = lax.ppermute(tail, "sp", [(i, i + 1) for i in range(order - 1)])
    filtered = pl.pallas_call(
        filter_kernel,
        out_shape=pltpu.VMEM((group, tokens), BF16),
        in_specs=[VMEM] * 3,
        out_specs=VMEM,
        compiler_params=room(4),
        name="filter",
    )(near(head), near(gated), near(conv_taps.T.astype(F32)))
    rows = lax.all_gather(filtered, TP, axis=0, tiled=True)

    packed = pl.pallas_call(
        pack_kernel,
        out_shape=pltpu.VMEM((chips, group, width + 128), BF16),
        in_specs=[VMEM] * 2,
        out_specs=VMEM,
        compiler_params=room(4),
        name="pack",
    )(far(out_weight), far(conv_gain[None]))
    own_out = lax.all_to_all(packed, "y", 0, 0, tiled=True)
    rows, own_out = lax.optimization_barrier((rows, own_out))
    other_out = twin(own_out)
    rows = rows.reshape(chips, 2, group, tokens)
    gates = (expert_gate[0], twin(expert_gate[0]))
    ups = (expert_up[0], twin(expert_up[0]))
    downs = (expert_down[0], twin(expert_down[0]))

    ids, weights = route_ids.T, route_weight.T
    slots = 2 * tokens * route_ids.shape[1] // experts // 2
    mine = width // 2
    updated, send, rank = pl.pallas_call(
        token_kernel,
        out_shape=(
            pltpu.VMEM((tokens, mine), F32),
            pltpu.VMEM((experts, slots, width), BF16),
            pltpu.VMEM((experts, tokens), F32),
        ),
        in_specs=[SMEM] + [VMEM] * 4 + [HBM],
        out_specs=(VMEM,) * 3,
        scratch_shapes=[pltpu.VMEM((tokens, width), BF16), pltpu.SemaphoreType.DMA],
        compiler_params=room(12),
        name="token",
    )(place, near(rows), near(own_out), near(other_out), near(ids), far(residual))

    arrived = lax.all_to_all(send, "sp", 0, 0, tiled=True).reshape(1, experts * slots, width)
    full = lax.all_gather(arrived, "y", axis=0, tiled=True)
    parts, part = 2, full.shape[1] // 2
    partial = pl.pallas_call(
        expert_kernel,
        out_shape=pltpu.HBM(full.shape, BF16),
        in_specs=[HBM] * 7,
        out_specs=HBM,
        scratch_shapes=[
            pltpu.VMEM((parts, chips, part, width), BF16),
            *(pltpu.VMEM(w.shape, BF16) for w in (*gates, *ups, *downs)),
            pltpu.VMEM((parts, chips, part, width), BF16),
            pltpu.SemaphoreType.DMA((parts,)),
            pltpu.SemaphoreType.DMA((6,)),
            pltpu.SemaphoreType.DMA((parts,)),
        ],
        compiler_params=room(32),
        name="expert",
    )(far(full), *(far(w) for w in (*gates, *ups, *downs)))
    summed = lax.psum_scatter(partial, "y", scatter_dimension=0, tiled=True)
    back = lax.all_to_all(summed.reshape(experts, slots, width), "sp", 0, 0, tiled=True)
    kept, given = pl.pallas_call(
        combine_kernel,
        out_shape=(pltpu.VMEM((tokens, mine), F32), pltpu.VMEM((tokens, mine), F32)),
        in_specs=[SMEM] + [VMEM] * 5,
        out_specs=(VMEM,) * 2,
        compiler_params=room(8),
        name="combine",
    )(place, near(back), near(rank), near(ids), near(weights), near(updated))
    return (kept + twin(given)).astype(BF16)


def solution(mesh):
    grid = Mesh(mesh.devices.reshape(mesh.shape["sp"], 8, 2), ("sp", "y", "c"))
    placed = (
        P("sp", TP),
        P("sp", TP),
        P(None, TP),
        P(TP),
        P(TP, None),
        P("sp", None),
        P("sp", None),
        P("sp", None),
        P("sp", None, TP),
        P("sp", None, TP),
        P("sp", TP, None),
    )
    return jax.shard_map(local, mesh=grid, in_specs=placed, out_specs=P("sp", TP), check_vma=False)
```

time: 218 us -> 201 us (0.922)
  blocking collectives: 41.1 us -> 67 us
  waiting for transfers between devices: 89.2 us -> 71.1 us
  starting transfers between devices: 42 us -> 30.1 us
  other arithmetic: 9.09 us -> 0.72 us
  local copies, waits for them, and re-layouts: 8.56 us -> 0.81 us
  Pallas kernels: 13.6 us -> 16.9 us
    all_to_all x2 -> x1, waiting for transfers between devices: 21.9 us -> 0.01 us  [local(): own_out = lax.all_to_all(packed, 'y', 0, 0, tiled=True)]
    all_to_all x0 -> x1, blocking collectives: none -> 20.5 us  [local(): lax.all_to_all(summed.reshape(experts, slots, width), 'sp', 0, 0, tiled=T...]
    all_to_all x2 -> x1, starting transfers between devices: 16.9 us -> 7.64 us  [local(): own_out = lax.all_to_all(packed, 'y', 0, 0, tiled=True)]
    convert_element_type x2 -> x0, other arithmetic: 5.15 us -> none  [the longest x1 5.15 us: local(): rows = lax.all_gather(filtered.astype(BF16), TP, axis=0, tiled=True)]
    unnamed x23 -> x10, local copies, waits for them, and re-layouts: 4.01 us -> 0.02 us
    pallas_call x3 -> x6, Pallas kernels: 13.6 us -> 16.9 us  [the longest x1 9.28 us: local(): pl.pallas_call(expert_kernel, out_shape=pltpu.HBM(full.shape, BF16), in_s...]
    ppermute x5, waiting for transfers between devices: 1.76 us -> 5.01 us  [twin(): return lax.ppermute(value, 'c', [(0, 1), (1, 0)])]
    all_gather x1, blocking collectives: 17.4 us -> 20.4 us  [local(): rows = lax.all_gather(filtered, TP, axis=0, tiled=True)]
  transfers between devices with their start and end apart: 10 -> 9, of which waited for: 7 -> 7; matrix products, arithmetic and copies ran while one was open for 4% -> 0% of each run, Pallas kernels for 0% -> 1%
where the time goes in v2:
time: 201 us; the launch traced here: 200 us
  waiting for transfers between devices  71.1 us (35%)
  blocking collectives  67 us (33%)
  starting transfers between devices  30.1 us (15%)
  Pallas kernels  16.9 us (8%)
  between operations  13.5 us (7%)
    reduce_scatter x1, waiting for transfers between devices, local(): summed = lax.psum_scatter(partial, 'y', scatter_dimension=0, tiled=True)  43.5 us
    all_to_all x1, blocking collectives, local(): lax.all_to_all(send, 'sp', 0, 0, tiled=True)  26.1 us
    all_gather x1, waiting for transfers between devices, local(): full = lax.all_gather(arrived, 'y', axis=0, tiled=True)  22.4 us
    all_to_all x1, blocking collectives, local(): lax.all_to_all(summed.reshape(experts, slots, width), 'sp', 0, 0, tiled=T...  20.5 us
    all_gather x1, blocking collectives, local(): rows = lax.all_gather(filtered, TP, axis=0, tiled=True)  20.4 us
    ppermute x5, starting transfers between devices, twin(): return lax.ppermute(value, 'c', [(0, 1), (1, 0)])  19.2 us
    pallas_call x1, Pallas kernels, local(): pl.pallas_call(expert_kernel, out_shape=pltpu.HBM(full.shape, BF16), in_s...  9.28 us
    all_to_all x1, starting transfers between devices, local(): own_out = lax.all_to_all(packed, 'y', 0, 0, tiled=True)  7.64 us
  transfers between devices with their start and end apart: 9, of which 7 were waited for; matrix products, arithmetic and copies ran while one was open for 0% of the time, Pallas kernels for 1%

profile of v2, /device:TPU:1, one launch (start us, length us, event | category | flops | bytes accessed | tf_op | source)
XLA Modules:
  0.0 200.2 jit_solution(4221822522115641887)
XLA Ops:
  6.5 0.8 gate.1
  7.4 1.8 pack.1
  9.2 7.6 %all-to-all-start = ((bf16[8,64,384]{2,1,0:T(8,128)(2,1)}), bf16[8,64,384]{2,1,0:T(8,128)(2,1)S(1)}, u32[]{:S(2)}, u32[]{:S(2)}) async-start(bf16[8,64,384]{2,1,0:T(8,128)(2,1)} %pack.1), calls=%async_computation | async-start | bytes 786432 | tf_op jit(solution)/shard_map/all_to_all | solution.py:246
  16.9 3.2 %collective-permute-start = (f32[64,128]{1,0:T(8,128)S(1)}, f32[64,128]{1,0:T(8,128)S(1)}, u32[]{:S(2)}, u32[]{:S(2)}) collective-permute-start(f32[64,128]{1,0:T(8,128)S(1)} %get-tuple-element.18), channel_id=1, source_target_pairs={{0,16},{16,32},{32,48},{48,64},{64,80},{80,96},{96,112},{112,128},... | collective-permute-start | bytes 98312 | tf_op jit(solution)/shard_map/ppermute | solution.py:227
  20.1 0.8 copy.14
  21.1 1.2 filter.1
  22.3 20.4 %all_gather.6 = bf16[1024,256]{1,0:T(8,128)(2,1)S(1)} all-gather(bf16[64,256]{1,0:T(8,128)(2,1)S(1)} %filter.1), channel_id=1, replica_groups=mesh['sp'=32,'y'=8,'c'=2] {'y','c'}, dimensions={0}, use_global_device_ids=true | all-gather | bytes 557056 | tf_op jit(solution)/shard_map/all_gather | solution.py:236
  42.7 2.1 %collective-permute-start.1 = (bf16[8,64,384]{2,1,0:T(8,128)(2,1)S(1)}, bf16[8,64,384]{2,1,0:T(8,128)(2,1)S(1)}, u32[]{:S(2)}, u32[]{:S(2)}) collective-permute-start(bf16[8,64,384]{2,1,0:T(8,128)(2,1)S(1)} %all-to-all-done.own_ref), channel_id=1, source_target_pairs={{0,1},{1,0},{2,3},{3,2},{4,5},{5,4},{6,7},{7,6},{8,9},{9,8},{10,11... | collective-permute-start | bytes 1179656 | tf_op jit(solution)/shard_map/ppermute | solution.py:18
  44.9 1.5 collective-permute-done.1.other_ref
  46.3 2.8 %token_.1 = (f32[256,128]{1,0:T(8,128)S(1)}, bf16[32,16,256]{2,1,0:T(8,128)(2,1)S(1)}, f32[32,256]{1,0:T(8,128)S(1)}) custom-call(s32[2]{0:T(128)S(1)} %pad_add_fusion.place_ref, bf16[8,2,64,256]{3,2,1,0:T(8,128)(2,1)S(1)} %bitcast.14, bf16[8,64,384]{2,1,0:T(8,128)(2,1)S(1)} %all-to-all-done.own_ref, ...), custom_call_target="tpu_custom_call" | custom-call | tf_op jit(solution)/shard_map/token/pallas_call | solution.py:257
  49.1 26.1 %all_to_all.15 = bf16[32,16,256]{2,1,0:T(8,128)(2,1)} all-to-all(bf16[32,16,256]{2,1,0:T(8,128)(2,1)S(1)} %get-tuple-element.24), channel_id=1, replica_groups=mesh['sp'=32,'y'=8,'c'=2] {'sp'}, dimensions={0} | all-to-all | bytes 524288 | tf_op jit(solution)/shard_map/all_to_all | solution.py:271
  75.3 4.3 %collective-permute-start.2 = (bf16[2048,256]{1,0:T(8,128)(2,1)S(1)}, bf16[2048,256]{1,0:T(8,128)(2,1)S(1)}, u32[]{:S(2)}, u32[]{:S(2)}) collective-permute-start(bf16[2048,256]{1,0:T(8,128)(2,1)S(1)} %bitcast.20), channel_id=1, source_target_pairs={{0,1},{1,0},{2,3},{3,2},{4,5},{5,4},{6,7},{7,6},{8,9},{9,8},{10,11... | collective-permute-start | bytes 3145736 | tf_op jit(solution)/shard_map/ppermute | solution.py:18
  79.5 1.9 collective-permute-start.3
  81.5 2.4 %collective-permute-start.4 = (bf16[256,2048]{1,0:T(8,128)(2,1)}, bf16[256,2048]{1,0:T(8,128)(2,1)}, u32[]{:S(2)}, u32[]{:S(2)}) collective-permute-start(bf16[256,2048]{1,0:T(8,128)(2,1)} %bitcast.23), channel_id=1, source_target_pairs={{0,1},{1,0},{2,3},{3,2},{4,5},{5,4},{6,7},{7,6},{8,9},{9,8},{10,11... | collective-permute-start | bytes 3145736 | tf_op jit(solution)/shard_map/ppermute | solution.py:18
  83.9 0.4 collective-permute-done.3.refs_3_
  84.3 2.2 %collective-permute-done.4.refs_5_ = bf16[256,2048]{1,0:T(8,128)(2,1)} collective-permute-done((bf16[256,2048]{1,0:T(8,128)(2,1)}, bf16[256,2048]{1,0:T(8,128)(2,1)}, u32[]{:S(2)}, u32[]{:S(2)}) %collective-permute-start.4) | collective-permute-done | bytes 1048608 | tf_op jit(solution)/shard_map/ppermute | solution.py:18
  86.5 22.4 %all-gather.2.cloned.1.call-done.x_hbm = bf16[8,512,256]{2,1,0:T(8,128)(2,1)} async-done(((bf16[1,512,256]{2,1,0:T(8,128)(2,1)}), bf16[8,512,256]{2,1,0:T(8,128)(2,1)}) %all-gather.2.cloned.1.call-update) | async-done | bytes 2097168 | tf_op jit(solution)/shard_map/all_gather | solution.py:272
  108.9 9.3 %expert.1 = bf16[8,512,256]{2,1,0:T(8,128)(2,1)} custom-call(bf16[8,512,256]{2,1,0:T(8,128)(2,1)} %all-gather.2.cloned.1.call-done.x_hbm, bf16[2048,256]{1,0:T(8,128)(2,1)} %bitcast.19, bf16[2048,256]{1,0:T(8,128)(2,1)} %copy-done.3, bf16[2048,256]{1,0:T(8,128)(2,1)} %bitcast.22, bf16[2048,256]{1,0:T(8,128)(2,1)} %copy-done.4, bf16[256,2048]{1,0:T(8,128)(2,1)} %bitcast.24, ...), custom_call_target="tpu_custom_call" | custom-call | tf_op jit(solution)/shard_map/expert/pallas_call | solution.py:274
  118.2 43.5 %reduce-scatter.2.cloned.1.call-done = bf16[1,512,256]{2,1,0:T(8,128)(2,1)} async-done(((bf16[8,512,256]{2,1,0:T(8,128)(2,1)}), bf16[1,512,256]{2,1,0:T(8,128)(2,1)}) %reduce-scatter.2.cloned.1.call-update) | async-done | bytes 262160 | tf_op jit(solution)/shard_map/reduce_scatter | solution.py:290
  161.7 20.5 %all_to_all.16.back_ref = bf16[32,16,256]{2,1,0:T(8,128)(2,1)S(1)} all-to-all(bf16[32,16,256]{2,1,0:T(8,128)(2,1)} %bitcast.26), channel_id=1, replica_groups=mesh['sp'=32,'y'=8,'c'=2] {'sp'}, dimensions={0} | all-to-all | bytes 524288 | tf_op jit(solution)/shard_map/all_to_all | solution.py:291
  182.2 1.0 combine.1
  183.2 8.5 %collective-permute-start.5 = (f32[256,128]{1,0:T(8,128)S(1)}, f32[256,128]{1,0:T(8,128)S(1)}, u32[]{:S(2)}, u32[]{:S(2)}) collective-permute-start(f32[256,128]{1,0:T(8,128)S(1)} %get-tuple-element.28), channel_id=1, source_target_pairs={{0,1},{1,0},{2,3},{3,2},{4,5},{5,4},{6,7},{7,6},{8,9},{9,8},{10,11... | collective-permute-start | bytes 393224 | tf_op jit(solution)/shard_map/ppermute | solution.py:18
  191.8 1.0 collective-permute-done.5
  192.7 0.6 add_convert_fusion
  (18 shorter events, 0.4 us)
Async XLA Ops:
  6.5 39.8 %copy-start = (s32[256,2]{0,1:T(2,128)S(1)}, s32[256,2]{0,1:T(2,128)}, u32[]{:S(2)}) copy-start(s32[256,2]{0,1:T(2,128)} %param.17) | copy-start | bytes 6148
  9.2 33.5 %all-to-all-start = ((bf16[8,64,384]{2,1,0:T(8,128)(2,1)}), bf16[8,64,384]{2,1,0:T(8,128)(2,1)S(1)}, u32[]{:S(2)}, u32[]{:S(2)}) async-start(bf16[8,64,384]{2,1,0:T(8,128)(2,1)} %pack.1), calls=%async_computation | async-start | bytes 786432 | tf_op jit(solution)/shard_map/all_to_all | solution.py:246
  16.8 58.5 %copy-start.2 = (bf16[1,2048,256]{2,1,0:T(8,128)(2,1)S(1)}, bf16[1,2048,256]{2,1,0:T(8,128)(2,1)}, u32[]{:S(2)}) copy-start(bf16[1,2048,256]{2,1,0:T(8,128)(2,1)} %param.19) | copy-start | bytes 3145732
  16.8 92.1 %all-gather.2.cloned.1.call-start = ((), (), s32[]{:S(2)}) async-start(), calls=%async_computation.4 | async-start | bytes 2359296 | tf_op jit(solution)/shard_map/all_gather | solution.py:272
  16.9 4.3 %collective-permute-start = (f32[64,128]{1,0:T(8,128)S(1)}, f32[64,128]{1,0:T(8,128)S(1)}, u32[]{:S(2)}, u32[]{:S(2)}) collective-permute-start(f32[64,128]{1,0:T(8,128)S(1)} %get-tuple-element.18), channel_id=1, source_target_pairs={{0,16},{16,32},{32,48},{48,64},{64,80},{80,96},{96,112},{112,128},... | collective-permute-start | bytes 98312 | tf_op jit(solution)/shard_map/ppermute | solution.py:227
  42.7 3.6 %collective-permute-start.1 = (bf16[8,64,384]{2,1,0:T(8,128)(2,1)S(1)}, bf16[8,64,384]{2,1,0:T(8,128)(2,1)S(1)}, u32[]{:S(2)}, u32[]{:S(2)}) collective-permute-start(bf16[8,64,384]{2,1,0:T(8,128)(2,1)S(1)} %all-to-all-done.own_ref), channel_id=1, source_target_pairs={{0,1},{1,0},{2,3},{3,2},{4,5},{5,4},{6,7},{7,6},{8,9},{9,8},{10,11... | collective-permute-start | bytes 1179656 | tf_op jit(solution)/shard_map/ppermute | solution.py:18
  75.2 86.5 %reduce-scatter.2.cloned.1.call-start = ((), (), s32[]{:S(2)}) async-start(), calls=%async_computation.5 | async-start | bytes 2359296 | tf_op jit(solution)/shard_map/reduce_scatter | solution.py:290
  75.3 8.6 %collective-permute-start.2 = (bf16[2048,256]{1,0:T(8,128)(2,1)S(1)}, bf16[2048,256]{1,0:T(8,128)(2,1)S(1)}, u32[]{:S(2)}, u32[]{:S(2)}) collective-permute-start(bf16[2048,256]{1,0:T(8,128)(2,1)S(1)} %bitcast.20), channel_id=1, source_target_pairs={{0,1},{1,0},{2,3},{3,2},{4,5},{5,4},{6,7},{7,6},{8,9},{9,8},{10,11... | collective-permute-start | bytes 3145736 | tf_op jit(solution)/shard_map/ppermute | solution.py:18
  79.5 4.8 %collective-permute-start.3 = (bf16[2048,256]{1,0:T(8,128)(2,1)}, bf16[2048,256]{1,0:T(8,128)(2,1)S(1)}, u32[]{:S(2)}, u32[]{:S(2)}) collective-permute-start(bf16[2048,256]{1,0:T(8,128)(2,1)} %bitcast.21), channel_id=1, source_target_pairs={{0,1},{1,0},{2,3},{3,2},{4,5},{5,4},{6,7},{7,6},{8,9},{9,8},{10,11... | collective-permute-start | bytes 3145736 | tf_op jit(solution)/shard_map/ppermute | solution.py:18
  81.5 5.0 %collective-permute-start.4 = (bf16[256,2048]{1,0:T(8,128)(2,1)}, bf16[256,2048]{1,0:T(8,128)(2,1)}, u32[]{:S(2)}, u32[]{:S(2)}) collective-permute-start(bf16[256,2048]{1,0:T(8,128)(2,1)} %bitcast.23), channel_id=1, source_target_pairs={{0,1},{1,0},{2,3},{3,2},{4,5},{5,4},{6,7},{7,6},{8,9},{9,8},{10,11... | collective-permute-start | bytes 3145736 | tf_op jit(solution)/shard_map/ppermute | solution.py:18
  83.9 25.0 %copy-start.3 = (bf16[2048,256]{1,0:T(8,128)(2,1)}, bf16[2048,256]{1,0:T(8,128)(2,1)S(1)}, u32[]{:S(2)}) copy-start(bf16[2048,256]{1,0:T(8,128)(2,1)S(1)} %collective-permute-done.2.refs_1_) | copy-start | bytes 3145732
  84.3 24.6 %copy-start.4 = (bf16[2048,256]{1,0:T(8,128)(2,1)}, bf16[2048,256]{1,0:T(8,128)(2,1)S(1)}, u32[]{:S(2)}) copy-start(bf16[2048,256]{1,0:T(8,128)(2,1)S(1)} %collective-permute-done.3.refs_3_) | copy-start | bytes 3145732
  118.2 64.0 %copy-start.1 = (f32[256,2]{0,1:T(2,128)S(1)}, f32[256,2]{0,1:T(2,128)}, u32[]{:S(2)}) copy-start(f32[256,2]{0,1:T(2,128)} %param.18) | copy-start | bytes 6148
  183.2 9.5 %collective-permute-start.5 = (f32[256,128]{1,0:T(8,128)S(1)}, f32[256,128]{1,0:T(8,128)S(1)}, u32[]{:S(2)}, u32[]{:S(2)}) collective-permute-start(f32[256,128]{1,0:T(8,128)S(1)} %get-tuple-element.28), channel_id=1, source_target_pairs={{0,1},{1,0},{2,3},{3,2},{4,5},{5,4},{6,7},{7,6},{8,9},{9,8},{10,11... | collective-permute-start | bytes 393224 | tf_op jit(solution)/shard_map/ppermute | solution.py:18
Sparse Core Ops, SparseCore 0:
  75.3 33.5 all-gather.1
  118.4 43.2 reduce-scatter.1

commit v3 on v2

--- a/solution.py
+++ b/solution.py
@@ -61,8 +61,13 @@
 def filter_kernel(head_ref, gated_ref, taps_ref, out_ref):
     line = jnp.concatenate([head_ref[...], gated_ref[...]], axis=1)
     length, tokens = line.shape[1], out_ref.shape[1]
-    count = taps_ref.shape[1]
-    taps = taps_ref[...]
+    count, group = taps_ref.shape
+    same = lax.broadcasted_iota(jnp.int32, (group, group), 0) == lax.broadcasted_iota(
+        jnp.int32, (group, group), 1
+    )
+    taps = lax.dot_general(
+        same.astype(F32).astype(BF16), taps_ref[...], across(1, 1), preferred_element_type=F32
+    )
     total = jnp.zeros(out_ref.shape, F32)
     for i in range(count):
         begin = length - tokens - (count - 1) + i
@@ -121,47 +126,53 @@
     send_ref[...] = sent.astype(BF16).reshape(experts, slots, width)
 
 
-def expert_kernel(x_hbm, *refs):
-    weights_hbm, out_hbm = refs[:6], refs[6]
-    x_ref, g0, g1, u0, u1, d0, d1, out_ref, in_sem, weight_sem, out_sem = refs[7:]
-    chunks, rows, width = x_hbm.shape
+def expert_kernel(x_hbm, g0, g1, u0_hbm, u1_hbm, d0_hbm, d1_hbm, out_hbm, *refs):
+    x_ref, up_ref, down_ref, out_ref, in_sem, up_sem, down_sem, out_sem = refs
+    chunks, _, width = x_hbm.shape
     parts, part = x_ref.shape[0], x_ref.shape[2]
+    half = d0_hbm.shape[0]
     ins = [
         pltpu.make_async_copy(x_hbm.at[:, pl.ds(k * part, part)], x_ref.at[k], in_sem.at[k])
         for k in range(parts)
     ]
-    held = (g0, g1, u0, u1, d0, d1)
-    moves = [pltpu.make_async_copy(weights_hbm[k], held[k], weight_sem.at[k]) for k in range(6)]
+    ups = [
+        pltpu.make_async_copy(w, up_ref.at[k], up_sem.at[k]) for k, w in enumerate((u0_hbm, u1_hbm))
+    ]
+    downs = [
+        pltpu.make_async_copy(w, down_ref.at[pl.ds(k * half, half)], down_sem.at[k])
+        for k, w in enumerate((d0_hbm, d1_hbm))
+    ]
     ins[0].start()
-    for k in (0, 2, 1, 3, 4, 5):
-        moves[k].start()
-    for k in range(1, parts):
-        ins[k].start()
+    ups[0].start()
+    ups[1].start()
     outs = []
     for k in range(parts):
         ins[k].wait()
+        if k == 0:
+            downs[0].start()
+            downs[1].start()
+            for copy in ins[1:]:
+                copy.start()
         x = jnp.concatenate([x_ref[k, i] for i in range(chunks)], axis=1)
         squares = jnp.zeros((part, 1), F32)
         for i in range(chunks):
             piece = x_ref[k, i].astype(F32)
             squares = squares + jnp.sum(piece * piece, axis=1, keepdims=True)
         scale = lax.rsqrt(squares / (chunks * width) + 1e-06)
+        gates = [jnp.dot(x, g[...], preferred_element_type=F32) * scale for g in (g0, g1)]
         hidden = []
-        for j in (0, 1):
+        for j, gate in enumerate(gates):
             if k == 0:
-                moves[j].wait()
-            gate = jnp.dot(x, held[j][...], preferred_element_type=F32) * scale
-            if k == 0:
-                moves[2 + j].wait()
-            up = jnp.dot(x, held[2 + j][...], preferred_element_type=F32) * scale
+                ups[j].wait()
+            up = jnp.dot(x, up_ref[j], preferred_element_type=F32) * scale
             hidden.append((gate / (1.0 + jnp.exp(-gate)) * up).astype(BF16))
+        hidden = jnp.concatenate(hidden, axis=1)
         if k == 0:
-            moves[4].wait()
-            moves[5].wait()
+            downs[0].wait()
+            downs[1].wait()
         for i in range(chunks):
             columns = slice(i * width, (i + 1) * width)
-            piece = jnp.dot(hidden[0], d0[:, columns], preferred_element_type=F32)
-            piece = piece + jnp.dot(hidden[1], d1[:, columns], preferred_element_type=F32)
+            piece = jnp.dot(hidden, down_ref[:, columns], preferred_element_type=F32)
             out_ref[k, i] = piece.astype(BF16)
         out = pltpu.make_async_copy(out_ref.at[k], out_hbm.at[:, pl.ds(k * part, part)], out_sem.at[k])
         out.start()
@@ -209,7 +220,7 @@
     chips, experts = lax.axis_size("y"), lax.axis_size("sp")
     chip, core = lax.axis_index("y"), lax.axis_index("c")
     place = jnp.stack([chip, core]).astype(jnp.int32)
-    taps_count, group = conv_taps.shape
+    _, group = conv_taps.shape
     tokens = conv_value.shape[0]
     model = residual.shape[1]
     width = model // chips
@@ -232,7 +243,7 @@
         out_specs=VMEM,
         compiler_params=room(4),
         name="filter",
-    )(near(head), near(gated), near(conv_taps.T.astype(F32)))
+    )(near(head), near(gated), far(conv_taps))
     rows = lax.all_gather(filtered, TP, axis=0, tiled=True)
 
     packed = pl.pallas_call(
@@ -274,19 +285,21 @@
     partial = pl.pallas_call(
         expert_kernel,
         out_shape=pltpu.HBM(full.shape, BF16),
-        in_specs=[HBM] * 7,
+        in_specs=[HBM] + [VMEM] * 2 + [HBM] * 4,
         out_specs=HBM,
         scratch_shapes=[
             pltpu.VMEM((parts, chips, part, width), BF16),
-            *(pltpu.VMEM(w.shape, BF16) for w in (*gates, *ups, *downs)),
+            pltpu.VMEM((2, *ups[0].shape), BF16),
+            pltpu.VMEM((2 * downs[0].shape[0], model), BF16),
             pltpu.VMEM((parts, chips, part, width), BF16),
             pltpu.SemaphoreType.DMA((parts,)),
-            pltpu.SemaphoreType.DMA((6,)),
+            pltpu.SemaphoreType.DMA((2,)),
+            pltpu.SemaphoreType.DMA((2,)),
             pltpu.SemaphoreType.DMA((parts,)),
         ],
         compiler_params=room(32),
         name="expert",
-    )(far(full), *(far(w) for w in (*gates, *ups, *downs)))
+    )(far(full), *(near(w) for w in gates), *(far(w) for w in (*ups, *downs)))
     summed = lax.psum_scatter(partial, "y", scatter_dimension=0, tiled=True)
     back = lax.all_to_all(summed.reshape(experts, slots, width), "sp", 0, 0, tiled=True)
     kept, given = pl.pallas_call(
@@ -315,4 +328,5 @@
         P("sp", None, TP),
         P("sp", TP, None),
     )
+
     return jax.shard_map(local, mesh=grid, in_specs=placed, out_specs=P("sp", TP), check_vma=False)

time: 201 us -> 199 us (0.990)
  no operation moved by 1% of the time
where the time goes in v3:
time: 199 us
  waiting for transfers between devices  72.1 us (36%)
  blocking collectives  67.1 us (34%)
  starting transfers between devices  29.6 us (15%)
  Pallas kernels  15.8 us (8%)
  between operations  13.5 us (7%)
    reduce_scatter x1, waiting for transfers between devices, local(): summed = lax.psum_scatter(partial, 'y', scatter_dimension=0, tiled=True)  43.6 us
    all_to_all x1, blocking collectives, local(): lax.all_to_all(send, 'sp', 0, 0, tiled=True)  26.1 us
    all_gather x1, waiting for transfers between devices, local(): full = lax.all_gather(arrived, 'y', axis=0, tiled=True)  22.4 us
    all_to_all x1, blocking collectives, local(): lax.all_to_all(summed.reshape(experts, slots, width), 'sp', 0, 0, tiled=T...  20.7 us
    all_gather x1, blocking collectives, local(): rows = lax.all_gather(filtered, TP, axis=0, tiled=True)  20.4 us
    ppermute x5, starting transfers between devices, twin(): return lax.ppermute(value, 'c', [(0, 1), (1, 0)])  18.6 us
    all_to_all x1, starting transfers between devices, local(): own_out = lax.all_to_all(packed, 'y', 0, 0, tiled=True)  7.64 us
    pallas_call x1, Pallas kernels, local(): pl.pallas_call(expert_kernel, out_shape=pltpu.HBM(full.shape, BF16), in_s...  7.43 us
  transfers between devices with their start and end apart: 9, of which 7 were waited for; matrix products, arithmetic and copies ran while one was open for 0% of the time, Pallas kernels for 1%

profile of v3, /device:TPU:1, one launch (start us, length us, event | category | flops | bytes accessed | tf_op | source)
XLA Modules:
  0.0 198.8 jit_solution(1910796211235745033)
XLA Ops:
  6.5 0.8 gate.1
  7.4 1.8 pack.1
  9.2 7.6 %all-to-all-start = ((bf16[8,64,384]{2,1,0:T(8,128)(2,1)}), bf16[8,64,384]{2,1,0:T(8,128)(2,1)S(1)}, u32[]{:S(2)}, u32[]{:S(2)}) async-start(bf16[8,64,384]{2,1,0:T(8,128)(2,1)} %pack.1), calls=%async_computation | async-start | bytes 786432 | tf_op jit(solution)/shard_map/all_to_all | solution.py:257
  16.9 3.2 %collective-permute-start = (f32[64,128]{1,0:T(8,128)S(1)}, f32[64,128]{1,0:T(8,128)S(1)}, u32[]{:S(2)}, u32[]{:S(2)}) collective-permute-start(f32[64,128]{1,0:T(8,128)S(1)} %get-tuple-element.18), channel_id=1, source_target_pairs={{0,16},{16,32},{32,48},{48,64},{64,80},{80,96},{96,112},{112,128},... | collective-permute-start | bytes 98312 | tf_op jit(solution)/shard_map/ppermute | solution.py:238
  20.1 1.0 collective-permute-done.head_ref
  21.1 1.9 filter.1
  23.1 20.4 %all_gather.6 = bf16[1024,256]{1,0:T(8,128)(2,1)S(1)} all-gather(bf16[64,256]{1,0:T(8,128)(2,1)S(1)} %filter.1), channel_id=1, replica_groups=mesh['sp'=32,'y'=8,'c'=2] {'y','c'}, dimensions={0}, use_global_device_ids=true | all-gather | bytes 557056 | tf_op jit(solution)/shard_map/all_gather | solution.py:247
  43.5 2.1 %collective-permute-start.1 = (bf16[8,64,384]{2,1,0:T(8,128)(2,1)S(1)}, bf16[8,64,384]{2,1,0:T(8,128)(2,1)S(1)}, u32[]{:S(2)}, u32[]{:S(2)}) collective-permute-start(bf16[8,64,384]{2,1,0:T(8,128)(2,1)S(1)} %all-to-all-done.own_ref), channel_id=1, source_target_pairs={{0,1},{1,0},{2,3},{3,2},{4,5},{5,4},{6,7},{7,6},{8,9},{9,8},{10,11... | collective-permute-start | bytes 1179656 | tf_op jit(solution)/shard_map/ppermute | solution.py:18
  45.6 1.5 collective-permute-done.1.other_ref
  47.1 2.8 %token_.1 = (f32[256,128]{1,0:T(8,128)S(1)}, bf16[32,16,256]{2,1,0:T(8,128)(2,1)S(1)}, f32[32,256]{1,0:T(8,128)S(1)}) custom-call(s32[2]{0:T(128)S(1)} %pad_add_fusion.place_ref, bf16[8,2,64,256]{3,2,1,0:T(8,128)(2,1)S(1)} %bitcast.13, bf16[8,64,384]{2,1,0:T(8,128)(2,1)S(1)} %all-to-all-done.own_ref, ...), custom_call_target="tpu_custom_call" | custom-call | tf_op jit(solution)/shard_map/token/pallas_call | solution.py:268
  49.8 26.1 %all_to_all.15 = bf16[32,16,256]{2,1,0:T(8,128)(2,1)} all-to-all(bf16[32,16,256]{2,1,0:T(8,128)(2,1)S(1)} %get-tuple-element.24), channel_id=1, replica_groups=mesh['sp'=32,'y'=8,'c'=2] {'sp'}, dimensions={0} | all-to-all | bytes 524288 | tf_op jit(solution)/shard_map/all_to_all | solution.py:282
  76.0 4.3 %collective-permute-start.2 = (bf16[2048,256]{1,0:T(8,128)(2,1)S(1)}, bf16[2048,256]{1,0:T(8,128)(2,1)S(1)}, u32[]{:S(2)}, u32[]{:S(2)}) collective-permute-start(bf16[2048,256]{1,0:T(8,128)(2,1)S(1)} %bitcast.14), channel_id=1, source_target_pairs={{0,1},{1,0},{2,3},{3,2},{4,5},{5,4},{6,7},{7,6},{8,9},{9,8},{10,11... | collective-permute-start | bytes 3145736 | tf_op jit(solution)/shard_map/ppermute | solution.py:18
  80.3 1.9 collective-permute-start.3
  82.2 2.4 %collective-permute-start.4 = (bf16[256,2048]{1,0:T(8,128)(2,1)}, bf16[256,2048]{1,0:T(8,128)(2,1)}, u32[]{:S(2)}, u32[]{:S(2)}) collective-permute-start(bf16[256,2048]{1,0:T(8,128)(2,1)} %bitcast.21), channel_id=1, source_target_pairs={{0,1},{1,0},{2,3},{3,2},{4,5},{5,4},{6,7},{7,6},{8,9},{9,8},{10,11... | collective-permute-start | bytes 3145736 | tf_op jit(solution)/shard_map/ppermute | solution.py:18
  84.6 0.4 collective-permute-done.3.u1_hbm
  85.0 2.2 %collective-permute-done.4.d1_hbm = bf16[256,2048]{1,0:T(8,128)(2,1)} collective-permute-done((bf16[256,2048]{1,0:T(8,128)(2,1)}, bf16[256,2048]{1,0:T(8,128)(2,1)}, u32[]{:S(2)}, u32[]{:S(2)}) %collective-permute-start.4) | collective-permute-done | bytes 1048608 | tf_op jit(solution)/shard_map/ppermute | solution.py:18
  87.2 22.4 %all-gather.2.cloned.1.call-done.x_hbm = bf16[8,512,256]{2,1,0:T(8,128)(2,1)} async-done(((bf16[1,512,256]{2,1,0:T(8,128)(2,1)}), bf16[8,512,256]{2,1,0:T(8,128)(2,1)}) %all-gather.2.cloned.1.call-update) | async-done | bytes 2097168 | tf_op jit(solution)/shard_map/all_gather | solution.py:283
  109.7 7.4 %expert.1 = bf16[8,512,256]{2,1,0:T(8,128)(2,1)} custom-call(bf16[8,512,256]{2,1,0:T(8,128)(2,1)} %all-gather.2.cloned.1.call-done.x_hbm, bf16[2048,256]{1,0:T(8,128)(2,1)S(1)} %bitcast.15, bf16[2048,256]{1,0:T(8,128)(2,1)S(1)} %collective-permute-done.2.g1, bf16[2048,256]{1,0:T(8,128)(2,1)} %bitcast.20, bf16[2048,256]{1,0:T(8,128)(2,1)} %copy-done.3, ...), custom_call_target="tpu_custom_call" | custom-call | tf_op jit(solution)/shard_map/expert/pallas_call | solution.py:285
  117.1 43.6 %reduce-scatter.2.cloned.1.call-done = bf16[1,512,256]{2,1,0:T(8,128)(2,1)} async-done(((bf16[8,512,256]{2,1,0:T(8,128)(2,1)}), bf16[1,512,256]{2,1,0:T(8,128)(2,1)}) %reduce-scatter.2.cloned.1.call-update) | async-done | bytes 262160 | tf_op jit(solution)/shard_map/reduce_scatter | solution.py:303
  160.7 20.7 %all_to_all.16.back_ref = bf16[32,16,256]{2,1,0:T(8,128)(2,1)S(1)} all-to-all(bf16[32,16,256]{2,1,0:T(8,128)(2,1)} %bitcast.24), channel_id=1, replica_groups=mesh['sp'=32,'y'=8,'c'=2] {'sp'}, dimensions={0} | all-to-all | bytes 524288 | tf_op jit(solution)/shard_map/all_to_all | solution.py:304
  181.4 1.0 combine.1
  182.4 8.0 %collective-permute-start.5 = (f32[256,128]{1,0:T(8,128)S(1)}, f32[256,128]{1,0:T(8,128)S(1)}, u32[]{:S(2)}, u32[]{:S(2)}) collective-permute-start(f32[256,128]{1,0:T(8,128)S(1)} %get-tuple-element.28), channel_id=1, source_target_pairs={{0,1},{1,0},{2,3},{3,2},{4,5},{5,4},{6,7},{7,6},{8,9},{9,8},{10,11... | collective-permute-start | bytes 393224 | tf_op jit(solution)/shard_map/ppermute | solution.py:18
  190.4 1.0 collective-permute-done.5
  191.3 0.6 add_convert_fusion
  (15 shorter events, 0.2 us)
Async XLA Ops:
  6.5 40.5 %copy-start.1 = (s32[256,2]{0,1:T(2,128)S(1)}, s32[256,2]{0,1:T(2,128)}, u32[]{:S(2)}) copy-start(s32[256,2]{0,1:T(2,128)} %param.17) | copy-start | bytes 6148
  9.2 34.3 %all-to-all-start = ((bf16[8,64,384]{2,1,0:T(8,128)(2,1)}), bf16[8,64,384]{2,1,0:T(8,128)(2,1)S(1)}, u32[]{:S(2)}, u32[]{:S(2)}) async-start(bf16[8,64,384]{2,1,0:T(8,128)(2,1)} %pack.1), calls=%async_computation | async-start | bytes 786432 | tf_op jit(solution)/shard_map/all_to_all | solution.py:257
  16.8 59.2 %copy-start = (bf16[1,2048,256]{2,1,0:T(8,128)(2,1)S(1)}, bf16[1,2048,256]{2,1,0:T(8,128)(2,1)}, u32[]{:S(2)}) copy-start(bf16[1,2048,256]{2,1,0:T(8,128)(2,1)} %param.19) | copy-start | bytes 3145732
  16.8 92.8 %all-gather.2.cloned.1.call-start = ((), (), s32[]{:S(2)}) async-start(), calls=%async_computation.4 | async-start | bytes 2359296 | tf_op jit(solution)/shard_map/all_gather | solution.py:283
  16.9 4.3 %collective-permute-start = (f32[64,128]{1,0:T(8,128)S(1)}, f32[64,128]{1,0:T(8,128)S(1)}, u32[]{:S(2)}, u32[]{:S(2)}) collective-permute-start(f32[64,128]{1,0:T(8,128)S(1)} %get-tuple-element.18), channel_id=1, source_target_pairs={{0,16},{16,32},{32,48},{48,64},{64,80},{80,96},{96,112},{112,128},... | collective-permute-start | bytes 98312 | tf_op jit(solution)/shard_map/ppermute | solution.py:238
  43.5 3.6 %collective-permute-start.1 = (bf16[8,64,384]{2,1,0:T(8,128)(2,1)S(1)}, bf16[8,64,384]{2,1,0:T(8,128)(2,1)S(1)}, u32[]{:S(2)}, u32[]{:S(2)}) collective-permute-start(bf16[8,64,384]{2,1,0:T(8,128)(2,1)S(1)} %all-to-all-done.own_ref), channel_id=1, source_target_pairs={{0,1},{1,0},{2,3},{3,2},{4,5},{5,4},{6,7},{7,6},{8,9},{9,8},{10,11... | collective-permute-start | bytes 1179656 | tf_op jit(solution)/shard_map/ppermute | solution.py:18
  76.0 84.8 %reduce-scatter.2.cloned.1.call-start = ((), (), s32[]{:S(2)}) async-start(), calls=%async_computation.5 | async-start | bytes 2359296 | tf_op jit(solution)/shard_map/reduce_scatter | solution.py:303
  76.0 8.6 %collective-permute-start.2 = (bf16[2048,256]{1,0:T(8,128)(2,1)S(1)}, bf16[2048,256]{1,0:T(8,128)(2,1)S(1)}, u32[]{:S(2)}, u32[]{:S(2)}) collective-permute-start(bf16[2048,256]{1,0:T(8,128)(2,1)S(1)} %bitcast.14), channel_id=1, source_target_pairs={{0,1},{1,0},{2,3},{3,2},{4,5},{5,4},{6,7},{7,6},{8,9},{9,8},{10,11... | collective-permute-start | bytes 3145736 | tf_op jit(solution)/shard_map/ppermute | solution.py:18
  80.3 4.8 %collective-permute-start.3 = (bf16[2048,256]{1,0:T(8,128)(2,1)}, bf16[2048,256]{1,0:T(8,128)(2,1)S(1)}, u32[]{:S(2)}, u32[]{:S(2)}) collective-permute-start(bf16[2048,256]{1,0:T(8,128)(2,1)} %bitcast.19), channel_id=1, source_target_pairs={{0,1},{1,0},{2,3},{3,2},{4,5},{5,4},{6,7},{7,6},{8,9},{9,8},{10,11... | collective-permute-start | bytes 3145736 | tf_op jit(solution)/shard_map/ppermute | solution.py:18
  82.2 5.0 %collective-permute-start.4 = (bf16[256,2048]{1,0:T(8,128)(2,1)}, bf16[256,2048]{1,0:T(8,128)(2,1)}, u32[]{:S(2)}, u32[]{:S(2)}) collective-permute-start(bf16[256,2048]{1,0:T(8,128)(2,1)} %bitcast.21), channel_id=1, source_target_pairs={{0,1},{1,0},{2,3},{3,2},{4,5},{5,4},{6,7},{7,6},{8,9},{9,8},{10,11... | collective-permute-start | bytes 3145736 | tf_op jit(solution)/shard_map/ppermute | solution.py:18
  85.0 24.6 %copy-start.3 = (bf16[2048,256]{1,0:T(8,128)(2,1)}, bf16[2048,256]{1,0:T(8,128)(2,1)S(1)}, u32[]{:S(2)}) copy-start(bf16[2048,256]{1,0:T(8,128)(2,1)S(1)} %collective-permute-done.3.u1_hbm) | copy-start | bytes 3145732
  117.1 64.3 %copy-start.2 = (f32[256,2]{0,1:T(2,128)S(1)}, f32[256,2]{0,1:T(2,128)}, u32[]{:S(2)}) copy-start(f32[256,2]{0,1:T(2,128)} %param.18) | copy-start | bytes 6148
  182.4 8.9 %collective-permute-start.5 = (f32[256,128]{1,0:T(8,128)S(1)}, f32[256,128]{1,0:T(8,128)S(1)}, u32[]{:S(2)}, u32[]{:S(2)}) collective-permute-start(f32[256,128]{1,0:T(8,128)S(1)} %get-tuple-element.28), channel_id=1, source_target_pairs={{0,1},{1,0},{2,3},{3,2},{4,5},{5,4},{6,7},{7,6},{8,9},{9,8},{10,11... | collective-permute-start | bytes 393224 | tf_op jit(solution)/shard_map/ppermute | solution.py:18
Sparse Core Ops, SparseCore 0:
  76.1 33.5 all-gather.1
  117.2 43.4 reduce-scatter.1

commit v4 on v3

--- a/solution.py
+++ b/solution.py
@@ -41,51 +41,62 @@
     tail_ref[...] = gated[:, gated.shape[1] - tail_ref.shape[1] :]
 
 
-def pack_kernel(weight_ref, gain_ref, out_ref):
-    chips, group, full = out_ref.shape
-    width = full - 128
-    rows = lax.broadcasted_iota(jnp.int32, (group, group), 0)
-    lanes = lax.broadcasted_iota(jnp.int32, (group, group), 1)
-    gain = jnp.sum(jnp.where(rows == lanes, gain_ref[...], 0.0), axis=1, keepdims=True)
-    first = gain.astype(BF16).astype(F32)
-    second = (gain - first).astype(BF16).astype(F32)
-    third = gain - first - second
-    lane = lax.broadcasted_iota(jnp.int32, (group, 128), 1)
-    extra = jnp.where(lane == 0, first, jnp.where(lane == 1, second, jnp.where(lane == 2, third, 0.0)))
-    extra = extra.astype(BF16)
+def diagonal(size):
+    rows = lax.broadcasted_iota(jnp.int32, (size, size), 0)
+    return rows == lax.broadcasted_iota(jnp.int32, (size, size), 1)
+
+
+def pack_kernel(weight_ref, taps_ref, out_ref, columns_ref):
+    chips, group, width = out_ref.shape
     for i in range(chips):
-        out_ref[i, :, :width] = weight_ref[:, i * width : (i + 1) * width]
-        out_ref[i, :, width:] = extra
-
-
-def filter_kernel(head_ref, gated_ref, taps_ref, out_ref):
+        out_ref[i] = weight_ref[:, i * width : (i + 1) * width]
+    columns_ref[...] = lax.dot_general(
+        diagonal(group).astype(F32).astype(BF16),
+        taps_ref[...],
+        across(1, 1),
+        preferred_element_type=F32,
+    )
+
+
+def filter_kernel(head_ref, gated_ref, taps_ref, gain_ref, out_ref):
     line = jnp.concatenate([head_ref[...], gated_ref[...]], axis=1)
-    length, tokens = line.shape[1], out_ref.shape[1]
-    count, group = taps_ref.shape
-    same = lax.broadcasted_iota(jnp.int32, (group, group), 0) == lax.broadcasted_iota(
-        jnp.int32, (group, group), 1
-    )
-    taps = lax.dot_general(
-        same.astype(F32).astype(BF16), taps_ref[...], across(1, 1), preferred_element_type=F32
-    )
-    total = jnp.zeros(out_ref.shape, F32)
+    group, tokens = gated_ref.shape
+    length, count = line.shape[1], taps_ref.shape[1]
+    taps = taps_ref[...]
+    total = jnp.zeros((group, tokens), F32)
     for i in range(count):
         begin = length - tokens - (count - 1) + i
         shifted = pltpu.roll(line, (length - begin) % length, 1)[:, :tokens]
         total = total + taps[:, i : i + 1] * shifted
-    out_ref[...] = total.astype(out_ref.dtype)
+    out_ref[:group, :] = total.astype(BF16)
+    gain = jnp.concatenate([gain_ref[...], jnp.zeros((1, tokens - group), F32)], axis=1)
+    first = gain.astype(BF16).astype(F32)
+    second = (gain - first).astype(BF16).astype(F32)
+    third = gain - first - second
+    row = lax.broadcasted_iota(jnp.int32, (out_ref.shape[0] - group, tokens), 0)
+    extra = jnp.where(row == 0, first, jnp.where(row == 1, second, jnp.where(row == 2, third, 0.0)))
+    out_ref[group:, :] = extra.astype(BF16)
 
 
 def token_kernel(place_ref, rows_ref, own_ref, other_ref, ids_ref, all_ref, upd_ref, send_ref, rank_ref, res_ref, sem):
     chip, core = place_ref[0], place_ref[1]
-    blocks, _, group, tokens = rows_ref.shape
+    blocks, _, _, tokens = rows_ref.shape
+    group = own_ref.shape[1]
     half = blocks * group
     width = res_ref.shape[1]
     columns = pl.ds(pl.multiple_of(chip * width, width), width)
     copy = pltpu.make_async_copy(all_ref.at[:, columns], res_ref, sem)
     copy.start()
-    own = rows_ref[:, core].reshape(half, tokens).astype(F32)
-    other = rows_ref[:, 1 - core].reshape(half, tokens).astype(F32)
+    both = []
+    for which in (core, 1 - core):
+        values = rows_ref[:, which, :group].reshape(half, tokens).astype(F32)
+        parts = rows_ref[:, which, group:].astype(F32)
+        gains = []
+        for i in range(blocks):
+            line = (parts[i, 0:1] + parts[i, 1:2] + parts[i, 2:3])[:, :group]
+            gains.append(jnp.sum(jnp.where(diagonal(group), line, 0.0), axis=1, keepdims=True))
+        both.append((values, jnp.concatenate(gains, axis=0)))
+    (own, own_gain), (other, other_gain) = both
     channels = 2 * half
     total = jnp.sum(own, axis=0, keepdims=True) + jnp.sum(other, axis=0, keepdims=True)
     squares = jnp.sum(own * own, axis=0, keepdims=True) + jnp.sum(other * other, axis=0, keepdims=True)
@@ -93,14 +104,12 @@
     variance = squares / channels - average * average
     scale = lax.rsqrt(variance + 1e-05)
     mixed = jnp.zeros((tokens, width), F32)
-    for values, weight_ref in ((own, own_ref), (other, other_ref)):
-        weight = weight_ref[...].reshape(half, weight_ref.shape[2])
-        parts = weight[:, width : width + 128].astype(F32)
-        gain = parts[:, 0:1] + parts[:, 1:2] + parts[:, 2:3]
+    for values, gain, weight_ref in ((own, own_gain, own_ref), (other, other_gain, other_ref)):
+        weight = weight_ref[...].reshape(half, width)
         normed = (values - average) * scale * gain
         activated = (normed / (1.0 + jnp.exp(-normed))).astype(BF16)
         mixed = mixed + lax.dot_general(
-            activated, weight[:, :width], across(0, 0), preferred_element_type=F32
+            activated, weight, across(0, 0), preferred_element_type=F32
         )
     copy.wait()
     updated = res_ref[...].astype(F32) + mixed
@@ -220,7 +229,7 @@
     chips, experts = lax.axis_size("y"), lax.axis_size("sp")
     chip, core = lax.axis_index("y"), lax.axis_index("c")
     place = jnp.stack([chip, core]).astype(jnp.int32)
-    _, group = conv_taps.shape
+    taps_count, group = conv_taps.shape
     tokens = conv_value.shape[0]
     model = residual.shape[1]
     width = model // chips
@@ -233,31 +242,31 @@
         compiler_params=room(4),
         name="gate",
     )(far(conv_value.T), far(conv_gate.T))
-    tail, out_weight, conv_gain = lax.optimization_barrier((tail, out_weight, conv_gain))
+    tail, out_weight = lax.optimization_barrier((tail, out_weight))
     order = lax.axis_size("sp")
     head = lax.ppermute(tail, "sp", [(i, i + 1) for i in range(order - 1)])
+    packed, taps = pl.pallas_call(
+        pack_kernel,
+        out_shape=(pltpu.VMEM((chips, group, width), BF16), pltpu.VMEM((group, taps_count), F32)),
+        in_specs=[VMEM] * 2,
+        out_specs=(VMEM,) * 2,
+        compiler_params=room(4),
+        name="pack",
+    )(far(out_weight), far(conv_taps))
+    own_out = lax.all_to_all(packed, "y", 0, 0, tiled=True)
+    sent = group + 16
     filtered = pl.pallas_call(
         filter_kernel,
-        out_shape=pltpu.VMEM((group, tokens), BF16),
-        in_specs=[VMEM] * 3,
+        out_shape=pltpu.VMEM((sent, tokens), BF16),
+        in_specs=[VMEM] * 4,
         out_specs=VMEM,
         compiler_params=room(4),
         name="filter",
-    )(near(head), near(gated), far(conv_taps))
+    )(near(head), near(gated), near(taps), far(conv_gain[None]))
     rows = lax.all_gather(filtered, TP, axis=0, tiled=True)
-
-    packed = pl.pallas_call(
-        pack_kernel,
-        out_shape=pltpu.VMEM((chips, group, width + 128), BF16),
-        in_specs=[VMEM] * 2,
-        out_specs=VMEM,
-        compiler_params=room(4),
-        name="pack",
-    )(far(out_weight), far(conv_gain[None]))
-    own_out = lax.all_to_all(packed, "y", 0, 0, tiled=True)
     rows, own_out = lax.optimization_barrier((rows, own_out))
     other_out = twin(own_out)
-    rows = rows.reshape(chips, 2, group, tokens)
+    rows = rows.reshape(chips, 2, sent, tokens)
     gates = (expert_gate[0], twin(expert_gate[0]))
     ups = (expert_up[0], twin(expert_up[0]))
     downs = (expert_down[0], twin(expert_down[0]))

time: 199 us -> 200 us (level)
  no operation moved by 1% of the time
where the time goes in v4:
time: 200 us; the launch traced here: 199 us
  waiting for transfers between devices  70.9 us (35%)
  blocking collectives  67.5 us (34%)
  starting transfers between devices  29.8 us (15%)
  Pallas kernels  15.3 us (8%)
  between operations  13.5 us (7%)
    reduce_scatter x1, waiting for transfers between devices, local(): summed = lax.psum_scatter(partial, 'y', scatter_dimension=0, tiled=True)  43.6 us
    all_to_all x1, blocking collectives, local(): lax.all_to_all(send, 'sp', 0, 0, tiled=True)  26.1 us
    all_gather x1, waiting for transfers between devices, local(): full = lax.all_gather(arrived, 'y', axis=0, tiled=True)  22.4 us
    all_gather x1, blocking collectives, local(): rows = lax.all_gather(filtered, TP, axis=0, tiled=True)  20.7 us
    all_to_all x1, blocking collectives, local(): lax.all_to_all(summed.reshape(experts, slots, width), 'sp', 0, 0, tiled=T...  20.7 us
    ppermute x5, starting transfers between devices, twin(): return lax.ppermute(value, 'c', [(0, 1), (1, 0)])  18.8 us
    all_to_all x1, starting transfers between devices, local(): own_out = lax.all_to_all(packed, 'y', 0, 0, tiled=True)  7.77 us
    pallas_call x1, Pallas kernels, local(): pl.pallas_call(expert_kernel, out_shape=pltpu.HBM(full.shape, BF16), in_s...  7.32 us
  transfers between devices with their start and end apart: 9, of which 7 were waited for; matrix products, arithmetic and copies ran while one was open for 0% of the time, Pallas kernels for 1%

profile of v4, /device:TPU:1, one launch (start us, length us, event | category | flops | bytes accessed | tf_op | source)
XLA Modules:
  0.0 199.5 jit_solution(17406338129273657262)
XLA Ops:
  6.5 0.8 gate.1
  7.3 1.7 pack.1
  9.0 7.8 %all-to-all-start = ((bf16[8,64,256]{2,1,0:T(8,128)(2,1)}), bf16[8,64,256]{2,1,0:T(8,128)(2,1)S(1)}, u32[]{:S(2)}, u32[]{:S(2)}) async-start(bf16[8,64,256]{2,1,0:T(8,128)(2,1)} %get-tuple-element.23), calls=%async_computation | async-start | bytes 524288 | tf_op jit(solution)/shard_map/all_to_all | solution.py:256
  16.8 3.1 %collective-permute-start = (f32[64,128]{1,0:T(8,128)S(1)}, f32[64,128]{1,0:T(8,128)S(1)}, u32[]{:S(2)}, u32[]{:S(2)}) collective-permute-start(f32[64,128]{1,0:T(8,128)S(1)} %get-tuple-element.19), channel_id=1, source_target_pairs={{0,16},{16,32},{32,48},{48,64},{64,80},{80,96},{96,112},{112,128},... | collective-permute-start | bytes 98312 | tf_op jit(solution)/shard_map/ppermute | solution.py:247
  20.0 1.0 collective-permute-done.head_ref
  21.0 1.9 filter.1
  22.8 20.7 %all_gather.6 = bf16[1280,256]{1,0:T(8,128)(2,1)S(1)} all-gather(bf16[80,256]{1,0:T(8,128)(2,1)S(1)} %filter.1), channel_id=1, replica_groups=mesh['sp'=32,'y'=8,'c'=2] {'y','c'}, dimensions={0}, use_global_device_ids=true | all-gather | bytes 696320 | tf_op jit(solution)/shard_map/all_gather | solution.py:266
  43.6 2.1 %collective-permute-start.1 = (bf16[8,64,256]{2,1,0:T(8,128)(2,1)S(1)}, bf16[8,64,256]{2,1,0:T(8,128)(2,1)S(1)}, u32[]{:S(2)}, u32[]{:S(2)}) collective-permute-start(bf16[8,64,256]{2,1,0:T(8,128)(2,1)S(1)} %all-to-all-done.own_ref), channel_id=1, source_target_pairs={{0,1},{1,0},{2,3},{3,2},{4,5},{5,4},{6,7},{7,6},{8,9},{9,8},{10,11... | collective-permute-start | bytes 786440 | tf_op jit(solution)/shard_map/ppermute | solution.py:18
  45.7 1.3 collective-permute-done.1.other_ref
  47.0 0.7 copy-done.1
  47.7 2.6 %token_.1 = (f32[256,128]{1,0:T(8,128)S(1)}, bf16[32,16,256]{2,1,0:T(8,128)(2,1)S(1)}, f32[32,256]{1,0:T(8,128)S(1)}) custom-call(s32[2]{0:T(128)S(1)} %pad_add_fusion.place_ref, bf16[8,2,80,256]{3,2,1,0:T(8,128)(2,1)S(1)} %bitcast.13, bf16[8,64,256]{2,1,0:T(8,128)(2,1)S(1)} %all-to-all-done.own_ref, ...), custom_call_target="tpu_custom_call" | custom-call | tf_op jit(solution)/shard_map/token/pallas_call | solution.py:277
  50.3 26.1 %all_to_all.15 = bf16[32,16,256]{2,1,0:T(8,128)(2,1)} all-to-all(bf16[32,16,256]{2,1,0:T(8,128)(2,1)S(1)} %get-tuple-element.26), channel_id=1, replica_groups=mesh['sp'=32,'y'=8,'c'=2] {'sp'}, dimensions={0} | all-to-all | bytes 524288 | tf_op jit(solution)/shard_map/all_to_all | solution.py:291
  76.5 4.3 %collective-permute-start.2 = (bf16[2048,256]{1,0:T(8,128)(2,1)S(1)}, bf16[2048,256]{1,0:T(8,128)(2,1)S(1)}, u32[]{:S(2)}, u32[]{:S(2)}) collective-permute-start(bf16[2048,256]{1,0:T(8,128)(2,1)S(1)} %bitcast.14), channel_id=1, source_target_pairs={{0,1},{1,0},{2,3},{3,2},{4,5},{5,4},{6,7},{7,6},{8,9},{9,8},{10,11... | collective-permute-start | bytes 3145736 | tf_op jit(solution)/shard_map/ppermute | solution.py:18
  80.8 1.9 collective-permute-start.3
  82.7 2.4 %collective-permute-start.4 = (bf16[256,2048]{1,0:T(8,128)(2,1)}, bf16[256,2048]{1,0:T(8,128)(2,1)}, u32[]{:S(2)}, u32[]{:S(2)}) collective-permute-start(bf16[256,2048]{1,0:T(8,128)(2,1)} %bitcast.21), channel_id=1, source_target_pairs={{0,1},{1,0},{2,3},{3,2},{4,5},{5,4},{6,7},{7,6},{8,9},{9,8},{10,11... | collective-permute-start | bytes 3145736 | tf_op jit(solution)/shard_map/ppermute | solution.py:18
  85.3 1.0 copy-done.5
  86.3 1.4 collective-permute-done.4.d1_hbm
  87.7 22.4 %all-gather.2.cloned.1.call-done.x_hbm = bf16[8,512,256]{2,1,0:T(8,128)(2,1)} async-done(((bf16[1,512,256]{2,1,0:T(8,128)(2,1)}), bf16[8,512,256]{2,1,0:T(8,128)(2,1)}) %all-gather.2.cloned.1.call-update) | async-done | bytes 2097168 | tf_op jit(solution)/shard_map/all_gather | solution.py:292
  110.1 7.3 %expert.1 = bf16[8,512,256]{2,1,0:T(8,128)(2,1)} custom-call(bf16[8,512,256]{2,1,0:T(8,128)(2,1)} %all-gather.2.cloned.1.call-done.x_hbm, bf16[2048,256]{1,0:T(8,128)(2,1)S(1)} %bitcast.15, bf16[2048,256]{1,0:T(8,128)(2,1)S(1)} %collective-permute-done.2.g1, bf16[2048,256]{1,0:T(8,128)(2,1)} %bitcast.19, bf16[2048,256]{1,0:T(8,128)(2,1)} %copy-done.5, ...), custom_call_target="tpu_custom_call" | custom-call | tf_op jit(solution)/shard_map/expert/pallas_call | solution.py:294
  117.5 43.6 %reduce-scatter.2.cloned.1.call-done = bf16[1,512,256]{2,1,0:T(8,128)(2,1)} async-done(((bf16[8,512,256]{2,1,0:T(8,128)(2,1)}), bf16[1,512,256]{2,1,0:T(8,128)(2,1)}) %reduce-scatter.2.cloned.1.call-update) | async-done | bytes 262160 | tf_op jit(solution)/shard_map/reduce_scatter | solution.py:312
  161.1 20.7 %all_to_all.16.back_ref = bf16[32,16,256]{2,1,0:T(8,128)(2,1)S(1)} all-to-all(bf16[32,16,256]{2,1,0:T(8,128)(2,1)} %bitcast.24), channel_id=1, replica_groups=mesh['sp'=32,'y'=8,'c'=2] {'sp'}, dimensions={0} | all-to-all | bytes 524288 | tf_op jit(solution)/shard_map/all_to_all | solution.py:313
  181.8 1.0 combine.1
  182.8 8.2 %collective-permute-start.5 = (f32[256,128]{1,0:T(8,128)S(1)}, f32[256,128]{1,0:T(8,128)S(1)}, u32[]{:S(2)}, u32[]{:S(2)}) collective-permute-start(f32[256,128]{1,0:T(8,128)S(1)} %get-tuple-element.30), channel_id=1, source_target_pairs={{0,1},{1,0},{2,3},{3,2},{4,5},{5,4},{6,7},{7,6},{8,9},{9,8},{10,11... | collective-permute-start | bytes 393224 | tf_op jit(solution)/shard_map/ppermute | solution.py:18
  191.0 1.0 collective-permute-done.5
  (19 shorter events, 1.1 us)
Async XLA Ops:
  9.0 67.5 %copy-start = (bf16[1,2048,256]{2,1,0:T(8,128)(2,1)S(1)}, bf16[1,2048,256]{2,1,0:T(8,128)(2,1)}, u32[]{:S(2)}) copy-start(bf16[1,2048,256]{2,1,0:T(8,128)(2,1)} %param.19) | copy-start | bytes 3145732
  9.0 34.6 %all-to-all-start = ((bf16[8,64,256]{2,1,0:T(8,128)(2,1)}), bf16[8,64,256]{2,1,0:T(8,128)(2,1)S(1)}, u32[]{:S(2)}, u32[]{:S(2)}) async-start(bf16[8,64,256]{2,1,0:T(8,128)(2,1)} %get-tuple-element.23), calls=%async_computation | async-start | bytes 524288 | tf_op jit(solution)/shard_map/all_to_all | solution.py:256
  16.8 93.3 %all-gather.2.cloned.1.call-start = ((), (), s32[]{:S(2)}) async-start(), calls=%async_computation.4 | async-start | bytes 2359296 | tf_op jit(solution)/shard_map/all_gather | solution.py:292
  16.8 4.1 %collective-permute-start = (f32[64,128]{1,0:T(8,128)S(1)}, f32[64,128]{1,0:T(8,128)S(1)}, u32[]{:S(2)}, u32[]{:S(2)}) collective-permute-start(f32[64,128]{1,0:T(8,128)S(1)} %get-tuple-element.19), channel_id=1, source_target_pairs={{0,16},{16,32},{32,48},{48,64},{64,80},{80,96},{96,112},{112,128},... | collective-permute-start | bytes 98312 | tf_op jit(solution)/shard_map/ppermute | solution.py:247
  43.6 3.4 %collective-permute-start.1 = (bf16[8,64,256]{2,1,0:T(8,128)(2,1)S(1)}, bf16[8,64,256]{2,1,0:T(8,128)(2,1)S(1)}, u32[]{:S(2)}, u32[]{:S(2)}) collective-permute-start(bf16[8,64,256]{2,1,0:T(8,128)(2,1)S(1)} %all-to-all-done.own_ref), channel_id=1, source_target_pairs={{0,1},{1,0},{2,3},{3,2},{4,5},{5,4},{6,7},{7,6},{8,9},{9,8},{10,11... | collective-permute-start | bytes 786440 | tf_op jit(solution)/shard_map/ppermute | solution.py:18
  47.0 0.7 copy-start.1
  47.7 33.1 %copy-start.4 = (bf16[1,2048,256]{2,1,0:T(8,128)(2,1)S(1)}, bf16[1,2048,256]{2,1,0:T(8,128)(2,1)}, u32[]{:S(2)}) copy-start(bf16[1,2048,256]{2,1,0:T(8,128)(2,1)} %param.20) | copy-start | bytes 3145732
  76.4 84.7 %reduce-scatter.2.cloned.1.call-start = ((), (), s32[]{:S(2)}) async-start(), calls=%async_computation.5 | async-start | bytes 2359296 | tf_op jit(solution)/shard_map/reduce_scatter | solution.py:312
  76.5 8.6 %collective-permute-start.2 = (bf16[2048,256]{1,0:T(8,128)(2,1)S(1)}, bf16[2048,256]{1,0:T(8,128)(2,1)S(1)}, u32[]{:S(2)}, u32[]{:S(2)}) collective-permute-start(bf16[2048,256]{1,0:T(8,128)(2,1)S(1)} %bitcast.14), channel_id=1, source_target_pairs={{0,1},{1,0},{2,3},{3,2},{4,5},{5,4},{6,7},{7,6},{8,9},{9,8},{10,11... | collective-permute-start | bytes 3145736 | tf_op jit(solution)/shard_map/ppermute | solution.py:18
  80.8 4.6 %collective-permute-start.3 = (bf16[2048,256]{1,0:T(8,128)(2,1)S(1)}, bf16[2048,256]{1,0:T(8,128)(2,1)S(1)}, u32[]{:S(2)}, u32[]{:S(2)}) collective-permute-start(bf16[2048,256]{1,0:T(8,128)(2,1)S(1)} %bitcast.20), channel_id=1, source_target_pairs={{0,1},{1,0},{2,3},{3,2},{4,5},{5,4},{6,7},{7,6},{8,9},{9,8},{10,11... | collective-permute-start | bytes 3145736 | tf_op jit(solution)/shard_map/ppermute | solution.py:18
  82.7 5.0 %collective-permute-start.4 = (bf16[256,2048]{1,0:T(8,128)(2,1)}, bf16[256,2048]{1,0:T(8,128)(2,1)}, u32[]{:S(2)}, u32[]{:S(2)}) collective-permute-start(bf16[256,2048]{1,0:T(8,128)(2,1)} %bitcast.21), channel_id=1, source_target_pairs={{0,1},{1,0},{2,3},{3,2},{4,5},{5,4},{6,7},{7,6},{8,9},{9,8},{10,11... | collective-permute-start | bytes 3145736 | tf_op jit(solution)/shard_map/ppermute | solution.py:18
  85.3 1.0 copy-start.5
  117.4 64.4 %copy-start.2 = (s32[256,2]{0,1:T(2,128)S(1)}, s32[256,2]{0,1:T(2,128)}, u32[]{:S(2)}) copy-start(s32[256,2]{0,1:T(2,128)} %param.17) | copy-start | bytes 6148
  117.5 64.4 %copy-start.3 = (f32[256,2]{0,1:T(2,128)S(1)}, f32[256,2]{0,1:T(2,128)}, u32[]{:S(2)}) copy-start(f32[256,2]{0,1:T(2,128)} %param.18) | copy-start | bytes 6148
  182.8 9.2 %collective-permute-start.5 = (f32[256,128]{1,0:T(8,128)S(1)}, f32[256,128]{1,0:T(8,128)S(1)}, u32[]{:S(2)}, u32[]{:S(2)}) collective-permute-start(f32[256,128]{1,0:T(8,128)S(1)} %get-tuple-element.30), channel_id=1, source_target_pairs={{0,1},{1,0},{2,3},{3,2},{4,5},{5,4},{6,7},{7,6},{8,9},{9,8},{10,11... | collective-permute-start | bytes 393224 | tf_op jit(solution)/shard_map/ppermute | solution.py:18
Sparse Core Ops, SparseCore 0:
  76.5 33.5 all-gather.1
  117.6 43.4 reduce-scatter.1

commit v5 on v4

--- a/solution.py
+++ b/solution.py
@@ -47,9 +47,9 @@
 
 
 def pack_kernel(weight_ref, taps_ref, out_ref, columns_ref):
-    chips, group, width = out_ref.shape
-    for i in range(chips):
-        out_ref[i] = weight_ref[:, i * width : (i + 1) * width]
+    receivers, group, width = out_ref.shape
+    for i in range(receivers):
+        out_ref[i] = weight_ref[:, i // 2 * width : (i // 2 + 1) * width]
     columns_ref[...] = lax.dot_general(
         diagonal(group).astype(F32).astype(BF16),
         taps_ref[...],
@@ -78,17 +78,17 @@
     out_ref[group:, :] = extra.astype(BF16)
 
 
-def token_kernel(place_ref, rows_ref, own_ref, other_ref, ids_ref, all_ref, upd_ref, send_ref, rank_ref, res_ref, sem):
+def token_kernel(place_ref, rows_ref, weight_ref, ids_ref, all_ref, upd_ref, send_ref, rank_ref, res_ref, sem):
     chip, core = place_ref[0], place_ref[1]
     blocks, _, _, tokens = rows_ref.shape
-    group = own_ref.shape[1]
+    group = weight_ref.shape[2]
     half = blocks * group
     width = res_ref.shape[1]
     columns = pl.ds(pl.multiple_of(chip * width, width), width)
     copy = pltpu.make_async_copy(all_ref.at[:, columns], res_ref, sem)
     copy.start()
     both = []
-    for which in (core, 1 - core):
+    for which in (0, 1):
         values = rows_ref[:, which, :group].reshape(half, tokens).astype(F32)
         parts = rows_ref[:, which, group:].astype(F32)
         gains = []
@@ -96,7 +96,7 @@
             line = (parts[i, 0:1] + parts[i, 1:2] + parts[i, 2:3])[:, :group]
             gains.append(jnp.sum(jnp.where(diagonal(group), line, 0.0), axis=1, keepdims=True))
         both.append((values, jnp.concatenate(gains, axis=0)))
-    (own, own_gain), (other, other_gain) = both
+    (own, _), (other, _) = both
     channels = 2 * half
     total = jnp.sum(own, axis=0, keepdims=True) + jnp.sum(other, axis=0, keepdims=True)
     squares = jnp.sum(own * own, axis=0, keepdims=True) + jnp.sum(other * other, axis=0, keepdims=True)
@@ -104,8 +104,8 @@
     variance = squares / channels - average * average
     scale = lax.rsqrt(variance + 1e-05)
     mixed = jnp.zeros((tokens, width), F32)
-    for values, gain, weight_ref in ((own, own_gain, own_ref), (other, other_gain, other_ref)):
-        weight = weight_ref[...].reshape(half, width)
+    for which, (values, gain) in enumerate(both):
+        weight = weight_ref[:, which].reshape(half, width)
         normed = (values - average) * scale * gain
         activated = (normed / (1.0 + jnp.exp(-normed))).astype(BF16)
         mixed = mixed + lax.dot_general(
@@ -152,15 +152,11 @@
         for k, w in enumerate((d0_hbm, d1_hbm))
     ]
     ins[0].start()
-    ups[0].start()
-    ups[1].start()
     outs = []
     for k in range(parts):
         ins[k].wait()
         if k == 0:
-            downs[0].start()
-            downs[1].start()
-            for copy in ins[1:]:
+            for copy in (*ups, *downs, *ins[1:]):
                 copy.start()
         x = jnp.concatenate([x_ref[k, i] for i in range(chunks)], axis=1)
         squares = jnp.zeros((part, 1), F32)
@@ -247,13 +243,13 @@
     head = lax.ppermute(tail, "sp", [(i, i + 1) for i in range(order - 1)])
     packed, taps = pl.pallas_call(
         pack_kernel,
-        out_shape=(pltpu.VMEM((chips, group, width), BF16), pltpu.VMEM((group, taps_count), F32)),
+        out_shape=(pltpu.VMEM((2 * chips, group, width), BF16), pltpu.VMEM((group, taps_count), F32)),
         in_specs=[VMEM] * 2,
         out_specs=(VMEM,) * 2,
         compiler_params=room(4),
         name="pack",
     )(far(out_weight), far(conv_taps))
-    own_out = lax.all_to_all(packed, "y", 0, 0, tiled=True)
+    columns = lax.all_to_all(packed, TP, 0, 0, tiled=True)
     sent = group + 16
     filtered = pl.pallas_call(
         filter_kernel,
@@ -264,9 +260,9 @@
         name="filter",
     )(near(head), near(gated), near(taps), far(conv_gain[None]))
     rows = lax.all_gather(filtered, TP, axis=0, tiled=True)
-    rows, own_out = lax.optimization_barrier((rows, own_out))
-    other_out = twin(own_out)
+    rows, columns = lax.optimization_barrier((rows, columns))
     rows = rows.reshape(chips, 2, sent, tokens)
+    columns = columns.reshape(chips, 2, group, width)
     gates = (expert_gate[0], twin(expert_gate[0]))
     ups = (expert_up[0], twin(expert_up[0]))
     downs = (expert_down[0], twin(expert_down[0]))
@@ -281,12 +277,12 @@
             pltpu.VMEM((experts, slots, width), BF16),
             pltpu.VMEM((experts, tokens), F32),
         ),
-        in_specs=[SMEM] + [VMEM] * 4 + [HBM],
+        in_specs=[SMEM] + [VMEM] * 3 + [HBM],
         out_specs=(VMEM,) * 3,
         scratch_shapes=[pltpu.VMEM((tokens, width), BF16), pltpu.SemaphoreType.DMA],
         compiler_params=room(12),
         name="token",
-    )(place, near(rows), near(own_out), near(other_out), near(ids), far(residual))
+    )(place, near(rows), near(columns), far(ids), far(residual))
 
     arrived = lax.all_to_all(send, "sp", 0, 0, tiled=True).reshape(1, experts * slots, width)
     full = lax.all_gather(arrived, "y", axis=0, tiled=True)

time: 200 us -> 198 us (0.990)
    all_to_all x1, blocking collectives: 26.1 us -> 22.7 us  [local(): lax.all_to_all(send, 'sp', 0, 0, tiled=True)]
    all_gather x1, blocking collectives: 20.7 us -> 23.2 us  [local(): rows = lax.all_gather(filtered, TP, axis=0, tiled=True)]
    all_to_all x1, starting transfers between devices: 7.77 us -> 10.2 us  [local(): columns = lax.all_to_all(packed, TP, 0, 0, tiled=True)]
    ppermute x5 -> x4, starting transfers between devices: 18.8 us -> 16.5 us  [twin(): return lax.ppermute(value, 'c', [(0, 1), (1, 0)])]
  transfers between devices with their start and end apart: 9 -> 8, of which waited for: 7 -> 6; matrix products, arithmetic and copies ran while one was open for 0% -> 0% of each run, Pallas kernels for 1% -> 1%
where the time goes in v5:
time: 198 us; the launch traced here: 197 us
  waiting for transfers between devices  70.9 us (36%)
  blocking collectives  66.6 us (34%)
  starting transfers between devices  28.5 us (14%)
  Pallas kernels  16 us (8%)
  between operations  13.5 us (7%)
    reduce_scatter x1, waiting for transfers between devices, local(): summed = lax.psum_scatter(partial, 'y', scatter_dimension=0, tiled=True)  43.6 us
    all_gather x1, waiting for transfers between devices, local(): full = lax.all_gather(arrived, 'y', axis=0, tiled=True)  23.8 us
    all_gather x1, blocking collectives, local(): rows = lax.all_gather(filtered, TP, axis=0, tiled=True)  23.2 us
    all_to_all x1, blocking collectives, local(): lax.all_to_all(send, 'sp', 0, 0, tiled=True)  22.7 us
    all_to_all x1, blocking collectives, local(): lax.all_to_all(summed.reshape(experts, slots, width), 'sp', 0, 0, tiled=T...  20.7 us
    ppermute x4, starting transfers between devices, twin(): return lax.ppermute(value, 'c', [(0, 1), (1, 0)])  16.5 us
    all_to_all x1, starting transfers between devices, local(): columns = lax.all_to_all(packed, TP, 0, 0, tiled=True)  10.2 us
    pallas_call x1, Pallas kernels, local(): pl.pallas_call(expert_kernel, out_shape=pltpu.HBM(full.shape, BF16), in_s...  7.77 us
  transfers between devices with their start and end apart: 8, of which 6 were waited for; matrix products, arithmetic and copies ran while one was open for 0% of the time, Pallas kernels for 1%

profile of v5, /device:TPU:1, one launch (start us, length us, event | category | flops | bytes accessed | tf_op | source)
XLA Modules:
  0.0 197.3 jit_solution(9501746683177569999)
XLA Ops:
  6.5 0.8 gate.1
  7.3 1.8 pack.1
  9.1 10.2 %all-to-all-start = ((bf16[16,64,256]{2,1,0:T(8,128)(2,1)}), bf16[16,64,256]{2,1,0:T(8,128)(2,1)S(1)}, u32[]{:S(2)}, u32[]{:S(2)}) async-start(bf16[16,64,256]{2,1,0:T(8,128)(2,1)} %get-tuple-element.23), calls=%async_computation | async-start | bytes 1048576 | tf_op jit(solution)/shard_map/all_to_all | solution.py:252
  19.4 1.7 collective-permute-start
  21.1 0.1 pad_add_fusion.place_ref
  21.1 0.9 collective-permute-done.head_ref
  22.1 1.9 filter.1
  24.0 23.2 %all_gather.6 = bf16[1280,256]{1,0:T(8,128)(2,1)S(1)} all-gather(bf16[80,256]{1,0:T(8,128)(2,1)S(1)} %filter.1), channel_id=1, replica_groups=mesh['sp'=32,'y'=8,'c'=2] {'y','c'}, dimensions={0}, use_global_device_ids=true | all-gather | bytes 696320 | tf_op jit(solution)/shard_map/all_gather | solution.py:262
  47.2 2.8 %token_.1 = (f32[256,128]{1,0:T(8,128)S(1)}, bf16[32,16,256]{2,1,0:T(8,128)(2,1)S(1)}, f32[32,256]{1,0:T(8,128)S(1)}) custom-call(s32[2]{0:T(128)S(1)} %pad_add_fusion.place_ref, bf16[8,2,80,256]{3,2,1,0:T(8,128)(2,1)S(1)} %bitcast.14, bf16[8,2,64,256]{3,2,1,0:T(8,128)(2,1)S(1)} %bitcast.15, s32[2,256]{1,0:T(2,128)} %bitcast.18, bf16[256,2048]{1,0:T(8,128)(2,1)} %all_ref.1), custom_call_target="tpu_custom_call" | custom-call | tf_op jit(solution)/shard_map/token/pallas_call | solution.py:273
  50.0 22.7 %all_to_all.15 = bf16[32,16,256]{2,1,0:T(8,128)(2,1)} all-to-all(bf16[32,16,256]{2,1,0:T(8,128)(2,1)S(1)} %get-tuple-element.26), channel_id=1, replica_groups=mesh['sp'=32,'y'=8,'c'=2] {'sp'}, dimensions={0} | all-to-all | bytes 524288 | tf_op jit(solution)/shard_map/all_to_all | solution.py:287
  72.8 4.3 %collective-permute-start.1 = (bf16[2048,256]{1,0:T(8,128)(2,1)S(1)}, bf16[2048,256]{1,0:T(8,128)(2,1)S(1)}, u32[]{:S(2)}, u32[]{:S(2)}) collective-permute-start(bf16[2048,256]{1,0:T(8,128)(2,1)S(1)} %bitcast.16), channel_id=1, source_target_pairs={{0,1},{1,0},{2,3},{3,2},{4,5},{5,4},{6,7},{7,6},{8,9},{9,8},{10,11... | collective-permute-start | bytes 3145736 | tf_op jit(solution)/shard_map/ppermute | solution.py:18
  77.0 1.9 collective-permute-start.2
  79.0 2.4 %collective-permute-start.3 = (bf16[256,2048]{1,0:T(8,128)(2,1)}, bf16[256,2048]{1,0:T(8,128)(2,1)}, u32[]{:S(2)}, u32[]{:S(2)}) collective-permute-start(bf16[256,2048]{1,0:T(8,128)(2,1)} %bitcast.23), channel_id=1, source_target_pairs={{0,1},{1,0},{2,3},{3,2},{4,5},{5,4},{6,7},{7,6},{8,9},{9,8},{10,11... | collective-permute-start | bytes 3145736 | tf_op jit(solution)/shard_map/ppermute | solution.py:18
  81.4 0.2 collective-permute-done.2.u1_hbm
  81.6 1.0 copy-done.4
  82.6 1.4 collective-permute-done.3.d1_hbm
  84.0 23.8 %all-gather.2.cloned.1.call-done.x_hbm = bf16[8,512,256]{2,1,0:T(8,128)(2,1)} async-done(((bf16[1,512,256]{2,1,0:T(8,128)(2,1)}), bf16[8,512,256]{2,1,0:T(8,128)(2,1)}) %all-gather.2.cloned.1.call-update) | async-done | bytes 2097168 | tf_op jit(solution)/shard_map/all_gather | solution.py:288
  107.7 7.8 %expert.1 = bf16[8,512,256]{2,1,0:T(8,128)(2,1)} custom-call(bf16[8,512,256]{2,1,0:T(8,128)(2,1)} %all-gather.2.cloned.1.call-done.x_hbm, bf16[2048,256]{1,0:T(8,128)(2,1)S(1)} %bitcast.17, bf16[2048,256]{1,0:T(8,128)(2,1)S(1)} %collective-permute-done.1.g1, bf16[2048,256]{1,0:T(8,128)(2,1)} %bitcast.21, bf16[2048,256]{1,0:T(8,128)(2,1)} %copy-done.4, ...), custom_call_target="tpu_custom_call" | custom-call | tf_op jit(solution)/shard_map/expert/pallas_call | solution.py:290
  115.6 43.6 %reduce-scatter.2.cloned.1.call-done = bf16[1,512,256]{2,1,0:T(8,128)(2,1)} async-done(((bf16[8,512,256]{2,1,0:T(8,128)(2,1)}), bf16[1,512,256]{2,1,0:T(8,128)(2,1)}) %reduce-scatter.2.cloned.1.call-update) | async-done | bytes 262160 | tf_op jit(solution)/shard_map/reduce_scatter | solution.py:308
  159.2 20.7 %all_to_all.16.back_ref = bf16[32,16,256]{2,1,0:T(8,128)(2,1)S(1)} all-to-all(bf16[32,16,256]{2,1,0:T(8,128)(2,1)} %bitcast.26), channel_id=1, replica_groups=mesh['sp'=32,'y'=8,'c'=2] {'sp'}, dimensions={0} | all-to-all | bytes 524288 | tf_op jit(solution)/shard_map/all_to_all | solution.py:309
  179.9 1.0 combine.1
  180.9 7.9 %collective-permute-start.4 = (f32[256,128]{1,0:T(8,128)S(1)}, f32[256,128]{1,0:T(8,128)S(1)}, u32[]{:S(2)}, u32[]{:S(2)}) collective-permute-start(f32[256,128]{1,0:T(8,128)S(1)} %get-tuple-element.30), channel_id=1, source_target_pairs={{0,1},{1,0},{2,3},{3,2},{4,5},{5,4},{6,7},{7,6},{8,9},{9,8},{10,11... | collective-permute-start | bytes 393224 | tf_op jit(solution)/shard_map/ppermute | solution.py:18
  188.8 1.0 collective-permute-done.4
  189.8 0.6 add_convert_fusion
  (15 shorter events, 0.1 us)
Async XLA Ops:
  9.1 38.1 %all-to-all-start = ((bf16[16,64,256]{2,1,0:T(8,128)(2,1)}), bf16[16,64,256]{2,1,0:T(8,128)(2,1)S(1)}, u32[]{:S(2)}, u32[]{:S(2)}) async-start(bf16[16,64,256]{2,1,0:T(8,128)(2,1)} %get-tuple-element.23), calls=%async_computation | async-start | bytes 1048576 | tf_op jit(solution)/shard_map/all_to_all | solution.py:252
  19.3 53.4 %copy-start = (bf16[1,2048,256]{2,1,0:T(8,128)(2,1)S(1)}, bf16[1,2048,256]{2,1,0:T(8,128)(2,1)}, u32[]{:S(2)}) copy-start(bf16[1,2048,256]{2,1,0:T(8,128)(2,1)} %param.19) | copy-start | bytes 3145732
  19.3 57.7 %copy-start.3 = (bf16[1,2048,256]{2,1,0:T(8,128)(2,1)S(1)}, bf16[1,2048,256]{2,1,0:T(8,128)(2,1)}, u32[]{:S(2)}) copy-start(bf16[1,2048,256]{2,1,0:T(8,128)(2,1)} %param.20) | copy-start | bytes 3145732
  19.3 88.4 %all-gather.2.cloned.1.call-start = ((), (), s32[]{:S(2)}) async-start(), calls=%async_computation.4 | async-start | bytes 2359296 | tf_op jit(solution)/shard_map/all_gather | solution.py:288
  19.4 2.7 %collective-permute-start = (f32[64,128]{1,0:T(8,128)S(1)}, f32[64,128]{1,0:T(8,128)S(1)}, u32[]{:S(2)}, u32[]{:S(2)}) collective-permute-start(f32[64,128]{1,0:T(8,128)S(1)} %get-tuple-element.19), channel_id=1, source_target_pairs={{0,16},{16,32},{32,48},{48,64},{64,80},{80,96},{96,112},{112,128},... | collective-permute-start | bytes 98312 | tf_op jit(solution)/shard_map/ppermute | solution.py:243
  72.7 86.4 %reduce-scatter.2.cloned.1.call-start = ((), (), s32[]{:S(2)}) async-start(), calls=%async_computation.5 | async-start | bytes 2359296 | tf_op jit(solution)/shard_map/reduce_scatter | solution.py:308
  72.8 8.6 %collective-permute-start.1 = (bf16[2048,256]{1,0:T(8,128)(2,1)S(1)}, bf16[2048,256]{1,0:T(8,128)(2,1)S(1)}, u32[]{:S(2)}, u32[]{:S(2)}) collective-permute-start(bf16[2048,256]{1,0:T(8,128)(2,1)S(1)} %bitcast.16), channel_id=1, source_target_pairs={{0,1},{1,0},{2,3},{3,2},{4,5},{5,4},{6,7},{7,6},{8,9},{9,8},{10,11... | collective-permute-start | bytes 3145736 | tf_op jit(solution)/shard_map/ppermute | solution.py:18
  77.0 4.6 %collective-permute-start.2 = (bf16[2048,256]{1,0:T(8,128)(2,1)S(1)}, bf16[2048,256]{1,0:T(8,128)(2,1)S(1)}, u32[]{:S(2)}, u32[]{:S(2)}) collective-permute-start(bf16[2048,256]{1,0:T(8,128)(2,1)S(1)} %bitcast.22), channel_id=1, source_target_pairs={{0,1},{1,0},{2,3},{3,2},{4,5},{5,4},{6,7},{7,6},{8,9},{9,8},{10,11... | collective-permute-start | bytes 3145736 | tf_op jit(solution)/shard_map/ppermute | solution.py:18
  79.0 5.0 %collective-permute-start.3 = (bf16[256,2048]{1,0:T(8,128)(2,1)}, bf16[256,2048]{1,0:T(8,128)(2,1)}, u32[]{:S(2)}, u32[]{:S(2)}) collective-permute-start(bf16[256,2048]{1,0:T(8,128)(2,1)} %bitcast.23), channel_id=1, source_target_pairs={{0,1},{1,0},{2,3},{3,2},{4,5},{5,4},{6,7},{7,6},{8,9},{9,8},{10,11... | collective-permute-start | bytes 3145736 | tf_op jit(solution)/shard_map/ppermute | solution.py:18
  81.6 1.0 copy-start.4
  115.5 64.3 %copy-start.1 = (s32[256,2]{0,1:T(2,128)S(1)}, s32[256,2]{0,1:T(2,128)}, u32[]{:S(2)}) copy-start(s32[256,2]{0,1:T(2,128)} %param.17) | copy-start | bytes 6148
  115.5 64.3 %copy-start.2 = (f32[256,2]{0,1:T(2,128)S(1)}, f32[256,2]{0,1:T(2,128)}, u32[]{:S(2)}) copy-start(f32[256,2]{0,1:T(2,128)} %param.18) | copy-start | bytes 6148
  180.9 8.9 %collective-permute-start.4 = (f32[256,128]{1,0:T(8,128)S(1)}, f32[256,128]{1,0:T(8,128)S(1)}, u32[]{:S(2)}, u32[]{:S(2)}) collective-permute-start(f32[256,128]{1,0:T(8,128)S(1)} %get-tuple-element.30), channel_id=1, source_target_pairs={{0,1},{1,0},{2,3},{3,2},{4,5},{5,4},{6,7},{7,6},{8,9},{9,8},{10,11... | collective-permute-start | bytes 393224 | tf_op jit(solution)/shard_map/ppermute | solution.py:18
Sparse Core Ops, SparseCore 0:
  72.8 34.8 all-gather.1
  115.7 43.4 reduce-scatter.1

commit v6 on v4

--- a/solution.py
+++ b/solution.py
@@ -46,16 +46,32 @@
     return rows == lax.broadcasted_iota(jnp.int32, (size, size), 1)
 
 
-def pack_kernel(weight_ref, taps_ref, out_ref, columns_ref):
-    chips, group, width = out_ref.shape
-    for i in range(chips):
-        out_ref[i] = weight_ref[:, i * width : (i + 1) * width]
+def pack_kernel(weight_hbm, taps_ref, gain_ref, out_hbm, columns_ref, rows_ref, sems):
+    chips, group, width = out_hbm.shape
+    copies = [
+        pltpu.make_async_copy(
+            weight_hbm.at[:, pl.ds(i * width, width)], out_hbm.at[i], sems.at[i]
+        )
+        for i in range(chips)
+    ]
+    for copy in copies:
+        copy.start()
     columns_ref[...] = lax.dot_general(
         diagonal(group).astype(F32).astype(BF16),
         taps_ref[...],
         across(1, 1),
         preferred_element_type=F32,
     )
+    tokens = rows_ref.shape[1]
+    gain = jnp.concatenate([gain_ref[...], jnp.zeros((1, tokens - group), F32)], axis=1)
+    first = gain.astype(BF16).astype(F32)
+    second = (gain - first).astype(BF16).astype(F32)
+    third = gain - first - second
+    row = lax.broadcasted_iota(jnp.int32, rows_ref.shape, 0)
+    extra = jnp.where(row == 0, first, jnp.where(row == 1, second, jnp.where(row == 2, third, 0.0)))
+    rows_ref[...] = extra.astype(BF16)
+    for copy in copies:
+        copy.wait()
 
 
 def filter_kernel(head_ref, gated_ref, taps_ref, gain_ref, out_ref):
@@ -69,13 +85,7 @@
         shifted = pltpu.roll(line, (length - begin) % length, 1)[:, :tokens]
         total = total + taps[:, i : i + 1] * shifted
     out_ref[:group, :] = total.astype(BF16)
-    gain = jnp.concatenate([gain_ref[...], jnp.zeros((1, tokens - group), F32)], axis=1)
-    first = gain.astype(BF16).astype(F32)
-    second = (gain - first).astype(BF16).astype(F32)
-    third = gain - first - second
-    row = lax.broadcasted_iota(jnp.int32, (out_ref.shape[0] - group, tokens), 0)
-    extra = jnp.where(row == 0, first, jnp.where(row == 1, second, jnp.where(row == 2, third, 0.0)))
-    out_ref[group:, :] = extra.astype(BF16)
+    out_ref[group:, :] = gain_ref[...]
 
 
 def token_kernel(place_ref, rows_ref, own_ref, other_ref, ids_ref, all_ref, upd_ref, send_ref, rank_ref, res_ref, sem):
@@ -245,16 +255,21 @@
     tail, out_weight = lax.optimization_barrier((tail, out_weight))
     order = lax.axis_size("sp")
     head = lax.ppermute(tail, "sp", [(i, i + 1) for i in range(order - 1)])
-    packed, taps = pl.pallas_call(
+    packed, taps, gains = pl.pallas_call(
         pack_kernel,
-        out_shape=(pltpu.VMEM((chips, group, width), BF16), pltpu.VMEM((group, taps_count), F32)),
-        in_specs=[VMEM] * 2,
-        out_specs=(VMEM,) * 2,
+        out_shape=(
+            pltpu.HBM((chips, group, width), BF16),
+            pltpu.VMEM((group, taps_count), F32),
+            pltpu.VMEM((16, tokens), BF16),
+        ),
+        in_specs=[HBM, VMEM, VMEM],
+        out_specs=(HBM, VMEM, VMEM),
+        scratch_shapes=[pltpu.SemaphoreType.DMA((chips,))],
         compiler_params=room(4),
         name="pack",
-    )(far(out_weight), far(conv_taps))
+    )(far(out_weight), far(conv_taps), far(conv_gain[None]))
     own_out = lax.all_to_all(packed, "y", 0, 0, tiled=True)
-    sent = group + 16
+    sent = group + gains.shape[0]
     filtered = pl.pallas_call(
         filter_kernel,
         out_shape=pltpu.VMEM((sent, tokens), BF16),
@@ -262,7 +277,7 @@
         out_specs=VMEM,
         compiler_params=room(4),
         name="filter",
-    )(near(head), near(gated), near(taps), far(conv_gain[None]))
+    )(near(head), near(gated), near(taps), near(gains))
     rows = lax.all_gather(filtered, TP, axis=0, tiled=True)
     rows, own_out = lax.optimization_barrier((rows, own_out))
     other_out = twin(own_out)
@@ -286,7 +301,7 @@
         scratch_shapes=[pltpu.VMEM((tokens, width), BF16), pltpu.SemaphoreType.DMA],
         compiler_params=room(12),
         name="token",
-    )(place, near(rows), near(own_out), near(other_out), near(ids), far(residual))
+    )(place, near(rows), near(own_out), near(other_out), far(ids), far(residual))
 
     arrived = lax.all_to_all(send, "sp", 0, 0, tiled=True).reshape(1, experts * slots, width)
     full = lax.all_gather(arrived, "y", axis=0, tiled=True)

time: 200 us -> 207 us (1.035)
  Pallas kernels: 15.3 us -> 23 us
    pallas_call x1, Pallas kernels: 1.67 us -> 9.82 us  [local(): pl.pallas_call(pack_kernel, out_shape=(pltpu.HBM((chips, group, width), B...]
where the time goes in v6:
time: 207 us
  waiting for transfers between devices  70.9 us (34%)
  blocking collectives  67.4 us (33%)
  starting transfers between devices  29.9 us (14%)
  Pallas kernels  23 us (11%)
  between operations  13.6 us (7%)
    reduce_scatter x1, waiting for transfers between devices, local(): summed = lax.psum_scatter(partial, 'y', scatter_dimension=0, tiled=True)  43.6 us
    all_to_all x1, blocking collectives, local(): lax.all_to_all(send, 'sp', 0, 0, tiled=True)  26.1 us
    all_gather x1, waiting for transfers between devices, local(): full = lax.all_gather(arrived, 'y', axis=0, tiled=True)  22.4 us
    all_gather x1, blocking collectives, local(): rows = lax.all_gather(filtered, TP, axis=0, tiled=True)  20.7 us
    all_to_all x1, blocking collectives, local(): lax.all_to_all(summed.reshape(experts, slots, width), 'sp', 0, 0, tiled=T...  20.6 us
    ppermute x5, starting transfers between devices, twin(): return lax.ppermute(value, 'c', [(0, 1), (1, 0)])  18.8 us
    pallas_call x1, Pallas kernels, local(): pl.pallas_call(pack_kernel, out_shape=(pltpu.HBM((chips, group, width), B...  9.82 us
    all_to_all x1, starting transfers between devices, local(): own_out = lax.all_to_all(packed, 'y', 0, 0, tiled=True)  7.78 us
  transfers between devices with their start and end apart: 9, of which 7 were waited for; matrix products, arithmetic and copies ran while one was open for 0% of the time, Pallas kernels for 1%

profile of v6, /device:TPU:1, one launch (start us, length us, event | category | flops | bytes accessed | tf_op | source)
XLA Modules:
  0.0 206.5 jit_solution(14046808532128897683)
XLA Ops:
  6.5 0.8 gate.1
  7.3 9.8 %pack.1 = (bf16[8,64,256]{2,1,0:T(8,128)(2,1)}, f32[64,31]{1,0:T(8,128)S(1)}, bf16[16,256]{1,0:T(8,128)(2,1)S(1)}) custom-call(bf16[64,2048]{1,0:T(8,128)(2,1)} %weight_hbm, bf16[31,64]{1,0:T(8,128)(2,1)} %taps_ref.1, f32[1,64]{1,0:T(1,128)} %bitcast.27), custom_call_target="tpu_custom_call" | custom-call | tf_op jit(solution)/shard_map/pack/pallas_call | solution.py:258
  17.2 7.8 %all-to-all-start = ((bf16[8,64,256]{2,1,0:T(8,128)(2,1)}), bf16[8,64,256]{2,1,0:T(8,128)(2,1)S(1)}, u32[]{:S(2)}, u32[]{:S(2)}) async-start(bf16[8,64,256]{2,1,0:T(8,128)(2,1)} %get-tuple-element.25), calls=%async_computation | async-start | bytes 524288 | tf_op jit(solution)/shard_map/all_to_all | solution.py:271
  25.0 3.2 %collective-permute-start = (f32[64,128]{1,0:T(8,128)S(1)}, f32[64,128]{1,0:T(8,128)S(1)}, u32[]{:S(2)}, u32[]{:S(2)}) collective-permute-start(f32[64,128]{1,0:T(8,128)S(1)} %get-tuple-element.20), channel_id=1, source_target_pairs={{0,16},{16,32},{32,48},{48,64},{64,80},{80,96},{96,112},{112,128},... | collective-permute-start | bytes 98312 | tf_op jit(solution)/shard_map/ppermute | solution.py:257
  28.3 1.0 collective-permute-done.head_ref
  29.3 1.2 filter.1
  30.5 20.7 %all_gather.6 = bf16[1280,256]{1,0:T(8,128)(2,1)S(1)} all-gather(bf16[80,256]{1,0:T(8,128)(2,1)S(1)} %filter.1), channel_id=1, replica_groups=mesh['sp'=32,'y'=8,'c'=2] {'y','c'}, dimensions={0}, use_global_device_ids=true | all-gather | bytes 696320 | tf_op jit(solution)/shard_map/all_gather | solution.py:281
  51.2 2.1 collective-permute-start.1
  53.4 1.3 collective-permute-done.1.other_ref
  54.6 2.8 %token_.1 = (f32[256,128]{1,0:T(8,128)S(1)}, bf16[32,16,256]{2,1,0:T(8,128)(2,1)S(1)}, f32[32,256]{1,0:T(8,128)S(1)}) custom-call(s32[2]{0:T(128)S(1)} %pad_add_fusion.place_ref, bf16[8,2,80,256]{3,2,1,0:T(8,128)(2,1)S(1)} %bitcast.13, bf16[8,64,256]{2,1,0:T(8,128)(2,1)S(1)} %all-to-all-done.own_ref, ...), custom_call_target="tpu_custom_call" | custom-call | tf_op jit(solution)/shard_map/token/pallas_call | solution.py:292
  57.4 26.1 %all_to_all.15 = bf16[32,16,256]{2,1,0:T(8,128)(2,1)} all-to-all(bf16[32,16,256]{2,1,0:T(8,128)(2,1)S(1)} %get-tuple-element.28), channel_id=1, replica_groups=mesh['sp'=32,'y'=8,'c'=2] {'sp'}, dimensions={0} | all-to-all | bytes 524288 | tf_op jit(solution)/shard_map/all_to_all | solution.py:306
  83.6 4.3 %collective-permute-start.2 = (bf16[2048,256]{1,0:T(8,128)(2,1)S(1)}, bf16[2048,256]{1,0:T(8,128)(2,1)S(1)}, u32[]{:S(2)}, u32[]{:S(2)}) collective-permute-start(bf16[2048,256]{1,0:T(8,128)(2,1)S(1)} %bitcast.14), channel_id=1, source_target_pairs={{0,1},{1,0},{2,3},{3,2},{4,5},{5,4},{6,7},{7,6},{8,9},{9,8},{10,11... | collective-permute-start | bytes 3145736 | tf_op jit(solution)/shard_map/ppermute | solution.py:18
  87.9 1.9 collective-permute-start.3
  89.8 2.4 %collective-permute-start.4 = (bf16[256,2048]{1,0:T(8,128)(2,1)}, bf16[256,2048]{1,0:T(8,128)(2,1)}, u32[]{:S(2)}, u32[]{:S(2)}) collective-permute-start(bf16[256,2048]{1,0:T(8,128)(2,1)} %bitcast.21), channel_id=1, source_target_pairs={{0,1},{1,0},{2,3},{3,2},{4,5},{5,4},{6,7},{7,6},{8,9},{9,8},{10,11... | collective-permute-start | bytes 3145736 | tf_op jit(solution)/shard_map/ppermute | solution.py:18
  92.4 1.0 copy-done.4
  93.4 1.4 collective-permute-done.4.d1_hbm
  94.8 22.4 %all-gather.2.cloned.1.call-done.x_hbm = bf16[8,512,256]{2,1,0:T(8,128)(2,1)} async-done(((bf16[1,512,256]{2,1,0:T(8,128)(2,1)}), bf16[8,512,256]{2,1,0:T(8,128)(2,1)}) %all-gather.2.cloned.1.call-update) | async-done | bytes 2097168 | tf_op jit(solution)/shard_map/all_gather | solution.py:307
  117.2 7.4 %expert.1 = bf16[8,512,256]{2,1,0:T(8,128)(2,1)} custom-call(bf16[8,512,256]{2,1,0:T(8,128)(2,1)} %all-gather.2.cloned.1.call-done.x_hbm, bf16[2048,256]{1,0:T(8,128)(2,1)S(1)} %bitcast.15, bf16[2048,256]{1,0:T(8,128)(2,1)S(1)} %collective-permute-done.2.g1, bf16[2048,256]{1,0:T(8,128)(2,1)} %bitcast.19, bf16[2048,256]{1,0:T(8,128)(2,1)} %copy-done.4, ...), custom_call_target="tpu_custom_call" | custom-call | tf_op jit(solution)/shard_map/expert/pallas_call | solution.py:309
  124.7 43.6 %reduce-scatter.2.cloned.1.call-done = bf16[1,512,256]{2,1,0:T(8,128)(2,1)} async-done(((bf16[8,512,256]{2,1,0:T(8,128)(2,1)}), bf16[1,512,256]{2,1,0:T(8,128)(2,1)}) %reduce-scatter.2.cloned.1.call-update) | async-done | bytes 262160 | tf_op jit(solution)/shard_map/reduce_scatter | solution.py:327
  168.3 20.6 %all_to_all.16.back_ref = bf16[32,16,256]{2,1,0:T(8,128)(2,1)S(1)} all-to-all(bf16[32,16,256]{2,1,0:T(8,128)(2,1)} %bitcast.24), channel_id=1, replica_groups=mesh['sp'=32,'y'=8,'c'=2] {'sp'}, dimensions={0} | all-to-all | bytes 524288 | tf_op jit(solution)/shard_map/all_to_all | solution.py:328
  188.9 1.0 combine.1
  189.9 8.1 %collective-permute-start.5 = (f32[256,128]{1,0:T(8,128)S(1)}, f32[256,128]{1,0:T(8,128)S(1)}, u32[]{:S(2)}, u32[]{:S(2)}) collective-permute-start(f32[256,128]{1,0:T(8,128)S(1)} %get-tuple-element.32), channel_id=1, source_target_pairs={{0,1},{1,0},{2,3},{3,2},{4,5},{5,4},{6,7},{7,6},{8,9},{9,8},{10,11... | collective-permute-start | bytes 393224 | tf_op jit(solution)/shard_map/ppermute | solution.py:18
  198.1 1.0 collective-permute-done.5
  199.0 0.6 add_convert_fusion
  (17 shorter events, 0.4 us)
Async XLA Ops:
  17.2 66.4 %copy-start = (bf16[1,2048,256]{2,1,0:T(8,128)(2,1)S(1)}, bf16[1,2048,256]{2,1,0:T(8,128)(2,1)}, u32[]{:S(2)}) copy-start(bf16[1,2048,256]{2,1,0:T(8,128)(2,1)} %param.19) | copy-start | bytes 3145732
  17.2 34.0 %all-to-all-start = ((bf16[8,64,256]{2,1,0:T(8,128)(2,1)}), bf16[8,64,256]{2,1,0:T(8,128)(2,1)S(1)}, u32[]{:S(2)}, u32[]{:S(2)}) async-start(bf16[8,64,256]{2,1,0:T(8,128)(2,1)} %get-tuple-element.25), calls=%async_computation | async-start | bytes 524288 | tf_op jit(solution)/shard_map/all_to_all | solution.py:271
  25.0 62.9 %copy-start.3 = (bf16[1,2048,256]{2,1,0:T(8,128)(2,1)S(1)}, bf16[1,2048,256]{2,1,0:T(8,128)(2,1)}, u32[]{:S(2)}) copy-start(bf16[1,2048,256]{2,1,0:T(8,128)(2,1)} %param.20) | copy-start | bytes 3145732
  25.0 92.3 %all-gather.2.cloned.1.call-start = ((), (), s32[]{:S(2)}) async-start(), calls=%async_computation.4 | async-start | bytes 2359296 | tf_op jit(solution)/shard_map/all_gather | solution.py:307
  25.0 4.3 %collective-permute-start = (f32[64,128]{1,0:T(8,128)S(1)}, f32[64,128]{1,0:T(8,128)S(1)}, u32[]{:S(2)}, u32[]{:S(2)}) collective-permute-start(f32[64,128]{1,0:T(8,128)S(1)} %get-tuple-element.20), channel_id=1, source_target_pairs={{0,16},{16,32},{32,48},{48,64},{64,80},{80,96},{96,112},{112,128},... | collective-permute-start | bytes 98312 | tf_op jit(solution)/shard_map/ppermute | solution.py:257
  51.2 3.4 %collective-permute-start.1 = (bf16[8,64,256]{2,1,0:T(8,128)(2,1)S(1)}, bf16[8,64,256]{2,1,0:T(8,128)(2,1)S(1)}, u32[]{:S(2)}, u32[]{:S(2)}) collective-permute-start(bf16[8,64,256]{2,1,0:T(8,128)(2,1)S(1)} %all-to-all-done.own_ref), channel_id=1, source_target_pairs={{0,1},{1,0},{2,3},{3,2},{4,5},{5,4},{6,7},{7,6},{8,9},{9,8},{10,11... | collective-permute-start | bytes 786440 | tf_op jit(solution)/shard_map/ppermute | solution.py:18
  83.5 84.7 %reduce-scatter.2.cloned.1.call-start = ((), (), s32[]{:S(2)}) async-start(), calls=%async_computation.5 | async-start | bytes 2359296 | tf_op jit(solution)/shard_map/reduce_scatter | solution.py:327
  83.6 8.6 %collective-permute-start.2 = (bf16[2048,256]{1,0:T(8,128)(2,1)S(1)}, bf16[2048,256]{1,0:T(8,128)(2,1)S(1)}, u32[]{:S(2)}, u32[]{:S(2)}) collective-permute-start(bf16[2048,256]{1,0:T(8,128)(2,1)S(1)} %bitcast.14), channel_id=1, source_target_pairs={{0,1},{1,0},{2,3},{3,2},{4,5},{5,4},{6,7},{7,6},{8,9},{9,8},{10,11... | collective-permute-start | bytes 3145736 | tf_op jit(solution)/shard_map/ppermute | solution.py:18
  87.9 4.6 %collective-permute-start.3 = (bf16[2048,256]{1,0:T(8,128)(2,1)S(1)}, bf16[2048,256]{1,0:T(8,128)(2,1)S(1)}, u32[]{:S(2)}, u32[]{:S(2)}) collective-permute-start(bf16[2048,256]{1,0:T(8,128)(2,1)S(1)} %bitcast.20), channel_id=1, source_target_pairs={{0,1},{1,0},{2,3},{3,2},{4,5},{5,4},{6,7},{7,6},{8,9},{9,8},{10,11... | collective-permute-start | bytes 3145736 | tf_op jit(solution)/shard_map/ppermute | solution.py:18
  89.8 5.0 %collective-permute-start.4 = (bf16[256,2048]{1,0:T(8,128)(2,1)}, bf16[256,2048]{1,0:T(8,128)(2,1)}, u32[]{:S(2)}, u32[]{:S(2)}) collective-permute-start(bf16[256,2048]{1,0:T(8,128)(2,1)} %bitcast.21), channel_id=1, source_target_pairs={{0,1},{1,0},{2,3},{3,2},{4,5},{5,4},{6,7},{7,6},{8,9},{9,8},{10,11... | collective-permute-start | bytes 3145736 | tf_op jit(solution)/shard_map/ppermute | solution.py:18
  92.4 1.0 copy-start.4
  124.6 64.3 %copy-start.1 = (s32[256,2]{0,1:T(2,128)S(1)}, s32[256,2]{0,1:T(2,128)}, u32[]{:S(2)}) copy-start(s32[256,2]{0,1:T(2,128)} %param.17) | copy-start | bytes 6148
  124.6 64.3 %copy-start.2 = (f32[256,2]{0,1:T(2,128)S(1)}, f32[256,2]{0,1:T(2,128)}, u32[]{:S(2)}) copy-start(f32[256,2]{0,1:T(2,128)} %param.18) | copy-start | bytes 6148
  189.9 9.1 %collective-permute-start.5 = (f32[256,128]{1,0:T(8,128)S(1)}, f32[256,128]{1,0:T(8,128)S(1)}, u32[]{:S(2)}, u32[]{:S(2)}) collective-permute-start(f32[256,128]{1,0:T(8,128)S(1)} %get-tuple-element.32), channel_id=1, source_target_pairs={{0,1},{1,0},{2,3},{3,2},{4,5},{5,4},{6,7},{7,6},{8,9},{9,8},{10,11... | collective-permute-start | bytes 393224 | tf_op jit(solution)/shard_map/ppermute | solution.py:18
Sparse Core Ops, SparseCore 0:
  83.7 33.5 all-gather.1
  124.8 43.4 reduce-scatter.1

commit v7 on v6

--- a/solution.py
+++ b/solution.py
@@ -46,16 +46,10 @@
     return rows == lax.broadcasted_iota(jnp.int32, (size, size), 1)
 
 
-def pack_kernel(weight_hbm, taps_ref, gain_ref, out_hbm, columns_ref, rows_ref, sems):
-    chips, group, width = out_hbm.shape
-    copies = [
-        pltpu.make_async_copy(
-            weight_hbm.at[:, pl.ds(i * width, width)], out_hbm.at[i], sems.at[i]
-        )
-        for i in range(chips)
-    ]
-    for copy in copies:
-        copy.start()
+def pack_kernel(weight_ref, taps_ref, gain_ref, out_ref, columns_ref, rows_ref):
+    chips, group, width = out_ref.shape
+    for i in range(chips):
+        out_ref[i] = weight_ref[:, i * width : (i + 1) * width]
     columns_ref[...] = lax.dot_general(
         diagonal(group).astype(F32).astype(BF16),
         taps_ref[...],
@@ -70,8 +64,6 @@
     row = lax.broadcasted_iota(jnp.int32, rows_ref.shape, 0)
     extra = jnp.where(row == 0, first, jnp.where(row == 1, second, jnp.where(row == 2, third, 0.0)))
     rows_ref[...] = extra.astype(BF16)
-    for copy in copies:
-        copy.wait()
 
 
 def filter_kernel(head_ref, gated_ref, taps_ref, gain_ref, out_ref):
@@ -252,19 +244,17 @@
         compiler_params=room(4),
         name="gate",
     )(far(conv_value.T), far(conv_gate.T))
-    tail, out_weight = lax.optimization_barrier((tail, out_weight))
     order = lax.axis_size("sp")
     head = lax.ppermute(tail, "sp", [(i, i + 1) for i in range(order - 1)])
     packed, taps, gains = pl.pallas_call(
         pack_kernel,
         out_shape=(
-            pltpu.HBM((chips, group, width), BF16),
+            pltpu.VMEM((chips, group, width), BF16),
             pltpu.VMEM((group, taps_count), F32),
             pltpu.VMEM((16, tokens), BF16),
         ),
-        in_specs=[HBM, VMEM, VMEM],
-        out_specs=(HBM, VMEM, VMEM),
-        scratch_shapes=[pltpu.SemaphoreType.DMA((chips,))],
+        in_specs=[VMEM] * 3,
+        out_specs=(VMEM,) * 3,
         compiler_params=room(4),
         name="pack",
     )(far(out_weight), far(conv_taps), far(conv_gain[None]))
@@ -279,7 +269,6 @@
         name="filter",
     )(near(head), near(gated), near(taps), near(gains))
     rows = lax.all_gather(filtered, TP, axis=0, tiled=True)
-    rows, own_out = lax.optimization_barrier((rows, own_out))
     other_out = twin(own_out)
     rows = rows.reshape(chips, 2, sent, tokens)
     gates = (expert_gate[0], twin(expert_gate[0]))

time: 207 us -> 197 us (0.952)
  Pallas kernels: 23 us -> 15 us
  blocking collectives: 67.4 us -> 61.2 us
  starting transfers between devices: 29.9 us -> 32.9 us
    pallas_call x1, Pallas kernels: 9.82 us -> 1.69 us  [local(): pl.pallas_call(pack_kernel, out_shape=(pltpu.VMEM((chips, group, width),...]
    all_gather x1, blocking collectives: 20.7 us -> 16.3 us  [local(): rows = lax.all_gather(filtered, TP, axis=0, tiled=True)]
    ppermute x5, starting transfers between devices: 18.8 us -> 22.1 us  [twin(): return lax.ppermute(value, 'c', [(0, 1), (1, 0)])]
    all_to_all x1, waiting for transfers between devices: 0.01 us -> 3.08 us  [local(): own_out = lax.all_to_all(packed, 'y', 0, 0, tiled=True)]
where the time goes in v7:
time: 197 us
  waiting for transfers between devices  72.3 us (37%)
  blocking collectives  61.2 us (31%)
  starting transfers between devices  32.9 us (17%)
  Pallas kernels  15 us (8%)
  between operations  13.5 us (7%)
    reduce_scatter x1, waiting for transfers between devices, local(): summed = lax.psum_scatter(partial, 'y', scatter_dimension=0, tiled=True)  43.6 us
    all_to_all x1, blocking collectives, local(): lax.all_to_all(send, 'sp', 0, 0, tiled=True)  24.2 us
    all_gather x1, waiting for transfers between devices, local(): full = lax.all_gather(arrived, 'y', axis=0, tiled=True)  22.1 us
    ppermute x5, starting transfers between devices, twin(): return lax.ppermute(value, 'c', [(0, 1), (1, 0)])  22.1 us
    all_to_all x1, blocking collectives, local(): lax.all_to_all(summed.reshape(experts, slots, width), 'sp', 0, 0, tiled=T...  20.6 us
    all_gather x1, blocking collectives, local(): rows = lax.all_gather(filtered, TP, axis=0, tiled=True)  16.3 us
    all_to_all x1, starting transfers between devices, local(): own_out = lax.all_to_all(packed, 'y', 0, 0, tiled=True)  7.64 us
    pallas_call x1, Pallas kernels, local(): pl.pallas_call(expert_kernel, out_shape=pltpu.HBM(full.shape, BF16), in_s...  7.35 us
  transfers between devices with their start and end apart: 9, of which 7 were waited for; matrix products, arithmetic and copies ran while one was open for 0% of the time, Pallas kernels for 1%

profile of v7, /device:TPU:1, one launch (start us, length us, event | category | flops | bytes accessed | tf_op | source)
XLA Modules:
  0.0 196.7 jit_solution(14064794798339259047)
XLA Ops:
  6.5 1.7 pack.1
  8.2 7.6 %all-to-all-start = ((bf16[8,64,256]{2,1,0:T(8,128)(2,1)}), bf16[8,64,256]{2,1,0:T(8,128)(2,1)S(1)}, u32[]{:S(2)}, u32[]{:S(2)}) async-start(bf16[8,64,256]{2,1,0:T(8,128)(2,1)} %get-tuple-element.19), calls=%async_computation | async-start | bytes 524288 | tf_op jit(solution)/shard_map/all_to_all | solution.py:261
  15.9 0.9 gate.1
  16.9 3.1 %collective-permute-start = (f32[64,128]{1,0:T(8,128)S(1)}, f32[64,128]{1,0:T(8,128)S(1)}, u32[]{:S(2)}, u32[]{:S(2)}) collective-permute-start(f32[64,128]{1,0:T(8,128)S(1)} %get-tuple-element.15), channel_id=1, source_target_pairs={{0,16},{16,32},{32,48},{48,64},{64,80},{80,96},{96,112},{112,128},... | collective-permute-start | bytes 98312 | tf_op jit(solution)/shard_map/ppermute | solution.py:248
  20.1 0.9 collective-permute-done.head_ref
  21.0 1.2 filter.1
  22.2 3.1 %all-to-all-done.own_ref = bf16[8,64,256]{2,1,0:T(8,128)(2,1)S(1)} async-done(((bf16[8,64,256]{2,1,0:T(8,128)(2,1)}), bf16[8,64,256]{2,1,0:T(8,128)(2,1)S(1)}, u32[]{:S(2)}, u32[]{:S(2)}) %all-to-all-start) | async-done | bytes 262176 | tf_op jit(solution)/shard_map/all_to_all | solution.py:261
  25.3 5.5 %collective-permute-start.1 = (bf16[8,64,256]{2,1,0:T(8,128)(2,1)S(1)}, bf16[8,64,256]{2,1,0:T(8,128)(2,1)S(1)}, u32[]{:S(2)}, u32[]{:S(2)}) collective-permute-start(bf16[8,64,256]{2,1,0:T(8,128)(2,1)S(1)} %all-to-all-done.own_ref), channel_id=1, source_target_pairs={{0,1},{1,0},{2,3},{3,2},{4,5},{5,4},{6,7},{7,6},{8,9},{9,8},{10,11... | collective-permute-start | bytes 786440 | tf_op jit(solution)/shard_map/ppermute | solution.py:18
  30.8 16.3 %all_gather.6 = bf16[1280,256]{1,0:T(8,128)(2,1)S(1)} all-gather(bf16[80,256]{1,0:T(8,128)(2,1)S(1)} %filter.1), channel_id=1, replica_groups=mesh['sp'=32,'y'=8,'c'=2] {'y','c'}, dimensions={0}, use_global_device_ids=true | all-gather | bytes 696320 | tf_op jit(solution)/shard_map/all_gather | solution.py:271
  47.1 2.8 %token_.1 = (f32[256,128]{1,0:T(8,128)S(1)}, bf16[32,16,256]{2,1,0:T(8,128)(2,1)S(1)}, f32[32,256]{1,0:T(8,128)S(1)}) custom-call(s32[2]{0:T(128)S(1)} %pad_add_fusion.place_ref, bf16[8,2,80,256]{3,2,1,0:T(8,128)(2,1)S(1)} %bitcast.13, bf16[8,64,256]{2,1,0:T(8,128)(2,1)S(1)} %all-to-all-done.own_ref, ...), custom_call_target="tpu_custom_call" | custom-call | tf_op jit(solution)/shard_map/token/pallas_call | solution.py:281
  49.9 24.2 %all_to_all.15 = bf16[32,16,256]{2,1,0:T(8,128)(2,1)} all-to-all(bf16[32,16,256]{2,1,0:T(8,128)(2,1)S(1)} %get-tuple-element.20), channel_id=1, replica_groups=mesh['sp'=32,'y'=8,'c'=2] {'sp'}, dimensions={0} | all-to-all | bytes 524288 | tf_op jit(solution)/shard_map/all_to_all | solution.py:295
  74.2 4.3 %collective-permute-start.2 = (bf16[2048,256]{1,0:T(8,128)(2,1)S(1)}, bf16[2048,256]{1,0:T(8,128)(2,1)S(1)}, u32[]{:S(2)}, u32[]{:S(2)}) collective-permute-start(bf16[2048,256]{1,0:T(8,128)(2,1)S(1)} %bitcast.14), channel_id=1, source_target_pairs={{0,1},{1,0},{2,3},{3,2},{4,5},{5,4},{6,7},{7,6},{8,9},{9,8},{10,11... | collective-permute-start | bytes 3145736 | tf_op jit(solution)/shard_map/ppermute | solution.py:18
  78.5 1.9 collective-permute-start.3
  80.4 2.4 %collective-permute-start.4 = (bf16[256,2048]{1,0:T(8,128)(2,1)}, bf16[256,2048]{1,0:T(8,128)(2,1)}, u32[]{:S(2)}, u32[]{:S(2)}) collective-permute-start(bf16[256,2048]{1,0:T(8,128)(2,1)} %bitcast.21), channel_id=1, source_target_pairs={{0,1},{1,0},{2,3},{3,2},{4,5},{5,4},{6,7},{7,6},{8,9},{9,8},{10,11... | collective-permute-start | bytes 3145736 | tf_op jit(solution)/shard_map/ppermute | solution.py:18
  83.1 1.0 copy-done.4
  84.0 1.4 collective-permute-done.4.d1_hbm
  85.5 22.1 %all-gather.2.cloned.1.call-done.x_hbm = bf16[8,512,256]{2,1,0:T(8,128)(2,1)} async-done(((bf16[1,512,256]{2,1,0:T(8,128)(2,1)}), bf16[8,512,256]{2,1,0:T(8,128)(2,1)}) %all-gather.2.cloned.1.call-update) | async-done | bytes 2097168 | tf_op jit(solution)/shard_map/all_gather | solution.py:296
  107.5 7.4 %expert.1 = bf16[8,512,256]{2,1,0:T(8,128)(2,1)} custom-call(bf16[8,512,256]{2,1,0:T(8,128)(2,1)} %all-gather.2.cloned.1.call-done.x_hbm, bf16[2048,256]{1,0:T(8,128)(2,1)S(1)} %bitcast.15, bf16[2048,256]{1,0:T(8,128)(2,1)S(1)} %collective-permute-done.2.g1, bf16[2048,256]{1,0:T(8,128)(2,1)} %bitcast.19, bf16[2048,256]{1,0:T(8,128)(2,1)} %copy-done.4, ...), custom_call_target="tpu_custom_call" | custom-call | tf_op jit(solution)/shard_map/expert/pallas_call | solution.py:298
  114.9 43.6 %reduce-scatter.2.cloned.1.call-done = bf16[1,512,256]{2,1,0:T(8,128)(2,1)} async-done(((bf16[8,512,256]{2,1,0:T(8,128)(2,1)}), bf16[1,512,256]{2,1,0:T(8,128)(2,1)}) %reduce-scatter.2.cloned.1.call-update) | async-done | bytes 262160 | tf_op jit(solution)/shard_map/reduce_scatter | solution.py:316
  158.5 20.6 %all_to_all.16.back_ref = bf16[32,16,256]{2,1,0:T(8,128)(2,1)S(1)} all-to-all(bf16[32,16,256]{2,1,0:T(8,128)(2,1)} %bitcast.24), channel_id=1, replica_groups=mesh['sp'=32,'y'=8,'c'=2] {'sp'}, dimensions={0} | all-to-all | bytes 524288 | tf_op jit(solution)/shard_map/all_to_all | solution.py:317
  179.2 1.0 combine.1
  180.2 8.0 %collective-permute-start.5 = (f32[256,128]{1,0:T(8,128)S(1)}, f32[256,128]{1,0:T(8,128)S(1)}, u32[]{:S(2)}, u32[]{:S(2)}) collective-permute-start(f32[256,128]{1,0:T(8,128)S(1)} %get-tuple-element.24), channel_id=1, source_target_pairs={{0,1},{1,0},{2,3},{3,2},{4,5},{5,4},{6,7},{7,6},{8,9},{9,8},{10,11... | collective-permute-start | bytes 393224 | tf_op jit(solution)/shard_map/ppermute | solution.py:18
  188.2 1.0 collective-permute-done.5
  189.2 0.6 add_convert_fusion
  (17 shorter events, 0.4 us)
Async XLA Ops:
  8.2 17.1 %all-to-all-start = ((bf16[8,64,256]{2,1,0:T(8,128)(2,1)}), bf16[8,64,256]{2,1,0:T(8,128)(2,1)S(1)}, u32[]{:S(2)}, u32[]{:S(2)}) async-start(bf16[8,64,256]{2,1,0:T(8,128)(2,1)} %get-tuple-element.19), calls=%async_computation | async-start | bytes 524288 | tf_op jit(solution)/shard_map/all_to_all | solution.py:261
  15.9 58.4 %copy-start = (bf16[1,2048,256]{2,1,0:T(8,128)(2,1)S(1)}, bf16[1,2048,256]{2,1,0:T(8,128)(2,1)}, u32[]{:S(2)}) copy-start(bf16[1,2048,256]{2,1,0:T(8,128)(2,1)} %param.19) | copy-start | bytes 3145732
  15.9 62.6 %copy-start.3 = (bf16[1,2048,256]{2,1,0:T(8,128)(2,1)S(1)}, bf16[1,2048,256]{2,1,0:T(8,128)(2,1)}, u32[]{:S(2)}) copy-start(bf16[1,2048,256]{2,1,0:T(8,128)(2,1)} %param.20) | copy-start | bytes 3145732
  15.9 91.6 %all-gather.2.cloned.1.call-start = ((), (), s32[]{:S(2)}) async-start(), calls=%async_computation.4 | async-start | bytes 2359296 | tf_op jit(solution)/shard_map/all_gather | solution.py:296
  16.9 4.1 %collective-permute-start = (f32[64,128]{1,0:T(8,128)S(1)}, f32[64,128]{1,0:T(8,128)S(1)}, u32[]{:S(2)}, u32[]{:S(2)}) collective-permute-start(f32[64,128]{1,0:T(8,128)S(1)} %get-tuple-element.15), channel_id=1, source_target_pairs={{0,16},{16,32},{32,48},{48,64},{64,80},{80,96},{96,112},{112,128},... | collective-permute-start | bytes 98312 | tf_op jit(solution)/shard_map/ppermute | solution.py:248
  25.3 21.8 %collective-permute-start.1 = (bf16[8,64,256]{2,1,0:T(8,128)(2,1)S(1)}, bf16[8,64,256]{2,1,0:T(8,128)(2,1)S(1)}, u32[]{:S(2)}, u32[]{:S(2)}) collective-permute-start(bf16[8,64,256]{2,1,0:T(8,128)(2,1)S(1)} %all-to-all-done.own_ref), channel_id=1, source_target_pairs={{0,1},{1,0},{2,3},{3,2},{4,5},{5,4},{6,7},{7,6},{8,9},{9,8},{10,11... | collective-permute-start | bytes 786440 | tf_op jit(solution)/shard_map/ppermute | solution.py:18
  74.2 84.4 %reduce-scatter.2.cloned.1.call-start = ((), (), s32[]{:S(2)}) async-start(), calls=%async_computation.5 | async-start | bytes 2359296 | tf_op jit(solution)/shard_map/reduce_scatter | solution.py:316
  74.2 8.6 %collective-permute-start.2 = (bf16[2048,256]{1,0:T(8,128)(2,1)S(1)}, bf16[2048,256]{1,0:T(8,128)(2,1)S(1)}, u32[]{:S(2)}, u32[]{:S(2)}) collective-permute-start(bf16[2048,256]{1,0:T(8,128)(2,1)S(1)} %bitcast.14), channel_id=1, source_target_pairs={{0,1},{1,0},{2,3},{3,2},{4,5},{5,4},{6,7},{7,6},{8,9},{9,8},{10,11... | collective-permute-start | bytes 3145736 | tf_op jit(solution)/shard_map/ppermute | solution.py:18
  78.5 4.6 %collective-permute-start.3 = (bf16[2048,256]{1,0:T(8,128)(2,1)S(1)}, bf16[2048,256]{1,0:T(8,128)(2,1)S(1)}, u32[]{:S(2)}, u32[]{:S(2)}) collective-permute-start(bf16[2048,256]{1,0:T(8,128)(2,1)S(1)} %bitcast.20), channel_id=1, source_target_pairs={{0,1},{1,0},{2,3},{3,2},{4,5},{5,4},{6,7},{7,6},{8,9},{9,8},{10,11... | collective-permute-start | bytes 3145736 | tf_op jit(solution)/shard_map/ppermute | solution.py:18
  80.4 5.0 %collective-permute-start.4 = (bf16[256,2048]{1,0:T(8,128)(2,1)}, bf16[256,2048]{1,0:T(8,128)(2,1)}, u32[]{:S(2)}, u32[]{:S(2)}) collective-permute-start(bf16[256,2048]{1,0:T(8,128)(2,1)} %bitcast.21), channel_id=1, source_target_pairs={{0,1},{1,0},{2,3},{3,2},{4,5},{5,4},{6,7},{7,6},{8,9},{9,8},{10,11... | collective-permute-start | bytes 3145736 | tf_op jit(solution)/shard_map/ppermute | solution.py:18
  83.1 1.0 copy-start.4
  114.9 64.3 %copy-start.1 = (s32[256,2]{0,1:T(2,128)S(1)}, s32[256,2]{0,1:T(2,128)}, u32[]{:S(2)}) copy-start(s32[256,2]{0,1:T(2,128)} %param.17) | copy-start | bytes 6148
  114.9 64.3 %copy-start.2 = (f32[256,2]{0,1:T(2,128)S(1)}, f32[256,2]{0,1:T(2,128)}, u32[]{:S(2)}) copy-start(f32[256,2]{0,1:T(2,128)} %param.18) | copy-start | bytes 6148
  180.2 9.0 %collective-permute-start.5 = (f32[256,128]{1,0:T(8,128)S(1)}, f32[256,128]{1,0:T(8,128)S(1)}, u32[]{:S(2)}, u32[]{:S(2)}) collective-permute-start(f32[256,128]{1,0:T(8,128)S(1)} %get-tuple-element.24), channel_id=1, source_target_pairs={{0,1},{1,0},{2,3},{3,2},{4,5},{5,4},{6,7},{7,6},{8,9},{9,8},{10,11... | collective-permute-start | bytes 393224 | tf_op jit(solution)/shard_map/ppermute | solution.py:18
Sparse Core Ops, SparseCore 0:
  74.3 33.1 all-gather.1
  115.1 43.4 reduce-scatter.1

commit v8 on v7

--- a/solution.py
+++ b/solution.py
@@ -34,19 +34,18 @@
     return pltpu.with_memory_space_constraint(value, pltpu.HBM)
 
 
-def gate_kernel(value_ref, gate_ref, out_ref, tail_ref):
-    value, gate = value_ref[...].astype(F32), gate_ref[...].astype(F32)
-    gated = value * (1.0 / (1.0 + jnp.exp(-gate)))
-    out_ref[...] = gated
-    tail_ref[...] = gated[:, gated.shape[1] - tail_ref.shape[1] :]
-
-
 def diagonal(size):
     rows = lax.broadcasted_iota(jnp.int32, (size, size), 0)
     return rows == lax.broadcasted_iota(jnp.int32, (size, size), 1)
 
 
-def pack_kernel(weight_ref, taps_ref, gain_ref, out_ref, columns_ref, rows_ref):
+def first_kernel(
+    value_ref, gate_ref, weight_ref, taps_ref, gain_ref, gated_ref, tail_ref, out_ref, columns_ref, rows_ref
+):
+    value, gate = value_ref[...].astype(F32), gate_ref[...].astype(F32)
+    gated = value * (1.0 / (1.0 + jnp.exp(-gate)))
+    gated_ref[...] = gated
+    tail_ref[...] = gated[:, gated.shape[1] - tail_ref.shape[1] :]
     chips, group, width = out_ref.shape
     for i in range(chips):
         out_ref[i] = weight_ref[:, i * width : (i + 1) * width]
@@ -80,7 +79,9 @@
     out_ref[group:, :] = gain_ref[...]
 
 
-def token_kernel(place_ref, rows_ref, own_ref, other_ref, ids_ref, all_ref, upd_ref, send_ref, rank_ref, res_ref, sem):
+def token_kernel(
+    place_ref, rows_ref, own_ref, other_ref, ids_hbm, all_ref, upd_ref, send_ref, rank_ref, res_ref, ids_ref, sem, ids_sem
+):
     chip, core = place_ref[0], place_ref[1]
     blocks, _, _, tokens = rows_ref.shape
     group = own_ref.shape[1]
@@ -89,6 +90,8 @@
     columns = pl.ds(pl.multiple_of(chip * width, width), width)
     copy = pltpu.make_async_copy(all_ref.at[:, columns], res_ref, sem)
     copy.start()
+    ids_copy = pltpu.make_async_copy(ids_hbm, ids_ref, ids_sem)
+    ids_copy.start()
     both = []
     for which in (core, 1 - core):
         values = rows_ref[:, which, :group].reshape(half, tokens).astype(F32)
@@ -117,6 +120,7 @@
     updated = res_ref[...].astype(F32) + mixed
     mine = width // 2
     upd_ref[...] = jnp.where(core == 0, updated[:, :mine], updated[:, mine:])
+    ids_copy.wait()
     experts, slots = send_ref.shape[:2]
     expert = lax.broadcasted_iota(jnp.int32, (experts, tokens), 0)
     named = (ids_ref[0:1, :] == expert) | (ids_ref[1:2, :] == expert)
@@ -165,10 +169,11 @@
             for copy in ins[1:]:
                 copy.start()
         x = jnp.concatenate([x_ref[k, i] for i in range(chunks)], axis=1)
-        squares = jnp.zeros((part, 1), F32)
+        squares = jnp.zeros((part, width), F32)
         for i in range(chunks):
             piece = x_ref[k, i].astype(F32)
-            squares = squares + jnp.sum(piece * piece, axis=1, keepdims=True)
+            squares = squares + piece * piece
+        squares = jnp.sum(squares, axis=1, keepdims=True)
         scale = lax.rsqrt(squares / (chunks * width) + 1e-06)
         gates = [jnp.dot(x, g[...], preferred_element_type=F32) * scale for g in (g0, g1)]
         hidden = []
@@ -236,28 +241,22 @@
     model = residual.shape[1]
     width = model // chips
 
-    gated, tail = pl.pallas_call(
-        gate_kernel,
-        out_shape=(pltpu.VMEM((group, tokens), F32), pltpu.VMEM((group, 128), F32)),
-        in_specs=[VMEM] * 2,
-        out_specs=(VMEM,) * 2,
-        compiler_params=room(4),
-        name="gate",
-    )(far(conv_value.T), far(conv_gate.T))
-    order = lax.axis_size("sp")
-    head = lax.ppermute(tail, "sp", [(i, i + 1) for i in range(order - 1)])
-    packed, taps, gains = pl.pallas_call(
-        pack_kernel,
+    gated, tail, packed, taps, gains = pl.pallas_call(
+        first_kernel,
         out_shape=(
+            pltpu.VMEM((group, tokens), F32),
+            pltpu.VMEM((group, 128), F32),
             pltpu.VMEM((chips, group, width), BF16),
             pltpu.VMEM((group, taps_count), F32),
             pltpu.VMEM((16, tokens), BF16),
         ),
-        in_specs=[VMEM] * 3,
-        out_specs=(VMEM,) * 3,
+        in_specs=[VMEM] * 5,
+        out_specs=(VMEM,) * 5,
         compiler_params=room(4),
-        name="pack",
-    )(far(out_weight), far(conv_taps), far(conv_gain[None]))
+        name="first",
+    )(*(far(a) for a in (conv_value.T, conv_gate.T, out_weight, conv_taps, conv_gain[None])))
+    order = lax.axis_size("sp")
+    head = lax.ppermute(tail, "sp", [(i, i + 1) for i in range(order - 1)])
     own_out = lax.all_to_all(packed, "y", 0, 0, tiled=True)
     sent = group + gains.shape[0]
     filtered = pl.pallas_call(
@@ -285,9 +284,14 @@
             pltpu.VMEM((experts, slots, width), BF16),
             pltpu.VMEM((experts, tokens), F32),
         ),
-        in_specs=[SMEM] + [VMEM] * 4 + [HBM],
+        in_specs=[SMEM] + [VMEM] * 3 + [HBM] * 2,
         out_specs=(VMEM,) * 3,
-        scratch_shapes=[pltpu.VMEM((tokens, width), BF16), pltpu.SemaphoreType.DMA],
+        scratch_shapes=[
+            pltpu.VMEM((tokens, width), BF16),
+            pltpu.VMEM(ids.shape, jnp.int32),
+            pltpu.SemaphoreType.DMA,
+            pltpu.SemaphoreType.DMA,
+        ],
         compiler_params=room(12),
         name="token",
     )(place, near(rows), near(own_out), near(other_out), far(ids), far(residual))

time: 197 us -> 196 us (level)
  no operation moved by 1% of the time
where the time goes in v8:
time: 196 us
  waiting for transfers between devices  72.2 us (37%)
  blocking collectives  61.7 us (31%)
  starting transfers between devices  32.9 us (17%)
  Pallas kernels  13.9 us (7%)
  between operations  13.5 us (7%)
    reduce_scatter x1, waiting for transfers between devices, local(): summed = lax.psum_scatter(partial, 'y', scatter_dimension=0, tiled=True)  43.2 us
    all_to_all x1, blocking collectives, local(): lax.all_to_all(send, 'sp', 0, 0, tiled=True)  24.2 us
    ppermute x5, starting transfers between devices, twin(): return lax.ppermute(value, 'c', [(0, 1), (1, 0)])  22 us
    all_gather x1, waiting for transfers between devices, local(): full = lax.all_gather(arrived, 'y', axis=0, tiled=True)  21.5 us
    all_to_all x1, blocking collectives, local(): lax.all_to_all(summed.reshape(experts, slots, width), 'sp', 0, 0, tiled=T...  21.1 us
    all_gather x1, blocking collectives, local(): rows = lax.all_gather(filtered, TP, axis=0, tiled=True)  16.3 us
    all_to_all x1, starting transfers between devices, local(): own_out = lax.all_to_all(packed, 'y', 0, 0, tiled=True)  7.64 us
    pallas_call x1, Pallas kernels, local(): pl.pallas_call(expert_kernel, out_shape=pltpu.HBM(full.shape, BF16), in_s...  7.29 us
  transfers between devices with their start and end apart: 9, of which 7 were waited for; matrix products, arithmetic and copies ran while one was open for 0% of the time, Pallas kernels for 1%

profile of v8, /device:TPU:1, one launch (start us, length us, event | category | flops | bytes accessed | tf_op | source)
XLA Modules:
  0.0 196.0 jit_solution(1117024676283701702)
XLA Ops:
  6.5 1.7 first.1
  8.3 7.6 %all-to-all-start = ((bf16[8,64,256]{2,1,0:T(8,128)(2,1)}), bf16[8,64,256]{2,1,0:T(8,128)(2,1)S(1)}, u32[]{:S(2)}, u32[]{:S(2)}) async-start(bf16[8,64,256]{2,1,0:T(8,128)(2,1)} %get-tuple-element.19), calls=%async_computation | async-start | bytes 524288 | tf_op jit(solution)/shard_map/all_to_all | solution.py:260
  16.0 3.2 %collective-permute-start = (f32[64,128]{1,0:T(8,128)S(1)}, f32[64,128]{1,0:T(8,128)S(1)}, u32[]{:S(2)}, u32[]{:S(2)}) collective-permute-start(f32[64,128]{1,0:T(8,128)S(1)} %get-tuple-element.15), channel_id=1, source_target_pairs={{0,16},{16,32},{32,48},{48,64},{64,80},{80,96},{96,112},{112,128},... | collective-permute-start | bytes 98312 | tf_op jit(solution)/shard_map/ppermute | solution.py:259
  19.3 0.9 collective-permute-done.head_ref
  20.2 1.2 filter.1
  21.4 3.9 %all-to-all-done.own_ref = bf16[8,64,256]{2,1,0:T(8,128)(2,1)S(1)} async-done(((bf16[8,64,256]{2,1,0:T(8,128)(2,1)}), bf16[8,64,256]{2,1,0:T(8,128)(2,1)S(1)}, u32[]{:S(2)}, u32[]{:S(2)}) %all-to-all-start) | async-done | bytes 262176 | tf_op jit(solution)/shard_map/all_to_all | solution.py:260
  25.4 5.5 %collective-permute-start.1 = (bf16[8,64,256]{2,1,0:T(8,128)(2,1)S(1)}, bf16[8,64,256]{2,1,0:T(8,128)(2,1)S(1)}, u32[]{:S(2)}, u32[]{:S(2)}) collective-permute-start(bf16[8,64,256]{2,1,0:T(8,128)(2,1)S(1)} %all-to-all-done.own_ref), channel_id=1, source_target_pairs={{0,1},{1,0},{2,3},{3,2},{4,5},{5,4},{6,7},{7,6},{8,9},{9,8},{10,11... | collective-permute-start | bytes 786440 | tf_op jit(solution)/shard_map/ppermute | solution.py:18
  30.8 16.3 %all_gather.6 = bf16[1280,256]{1,0:T(8,128)(2,1)S(1)} all-gather(bf16[80,256]{1,0:T(8,128)(2,1)S(1)} %filter.1), channel_id=1, replica_groups=mesh['sp'=32,'y'=8,'c'=2] {'y','c'}, dimensions={0}, use_global_device_ids=true | all-gather | bytes 696320 | tf_op jit(solution)/shard_map/all_gather | solution.py:270
  47.2 2.7 %token_.1 = (f32[256,128]{1,0:T(8,128)S(1)}, bf16[32,16,256]{2,1,0:T(8,128)(2,1)S(1)}, f32[32,256]{1,0:T(8,128)S(1)}) custom-call(s32[2]{0:T(128)S(1)} %pad_add_fusion.place_ref, bf16[8,2,80,256]{3,2,1,0:T(8,128)(2,1)S(1)} %bitcast.13, bf16[8,64,256]{2,1,0:T(8,128)(2,1)S(1)} %all-to-all-done.own_ref, ...), custom_call_target="tpu_custom_call" | custom-call | tf_op jit(solution)/shard_map/token/pallas_call | solution.py:280
  49.8 24.2 %all_to_all.15 = bf16[32,16,256]{2,1,0:T(8,128)(2,1)} all-to-all(bf16[32,16,256]{2,1,0:T(8,128)(2,1)S(1)} %get-tuple-element.20), channel_id=1, replica_groups=mesh['sp'=32,'y'=8,'c'=2] {'sp'}, dimensions={0} | all-to-all | bytes 524288 | tf_op jit(solution)/shard_map/all_to_all | solution.py:299
  74.2 4.3 %collective-permute-start.2 = (bf16[2048,256]{1,0:T(8,128)(2,1)S(1)}, bf16[2048,256]{1,0:T(8,128)(2,1)S(1)}, u32[]{:S(2)}, u32[]{:S(2)}) collective-permute-start(bf16[2048,256]{1,0:T(8,128)(2,1)S(1)} %bitcast.14), channel_id=1, source_target_pairs={{0,1},{1,0},{2,3},{3,2},{4,5},{5,4},{6,7},{7,6},{8,9},{9,8},{10,11... | collective-permute-start | bytes 3145736 | tf_op jit(solution)/shard_map/ppermute | solution.py:18
  78.4 1.9 collective-permute-start.3
  80.4 2.4 %collective-permute-start.4 = (bf16[256,2048]{1,0:T(8,128)(2,1)}, bf16[256,2048]{1,0:T(8,128)(2,1)}, u32[]{:S(2)}, u32[]{:S(2)}) collective-permute-start(bf16[256,2048]{1,0:T(8,128)(2,1)} %bitcast.21), channel_id=1, source_target_pairs={{0,1},{1,0},{2,3},{3,2},{4,5},{5,4},{6,7},{7,6},{8,9},{9,8},{10,11... | collective-permute-start | bytes 3145736 | tf_op jit(solution)/shard_map/ppermute | solution.py:18
  82.8 0.2 collective-permute-done.3.u1_hbm
  83.0 1.0 copy-done.4
  84.0 1.4 collective-permute-done.4.d1_hbm
  85.4 21.5 %all-gather.2.cloned.1.call-done.x_hbm = bf16[8,512,256]{2,1,0:T(8,128)(2,1)} async-done(((bf16[1,512,256]{2,1,0:T(8,128)(2,1)}), bf16[8,512,256]{2,1,0:T(8,128)(2,1)}) %all-gather.2.cloned.1.call-update) | async-done | bytes 2097168 | tf_op jit(solution)/shard_map/all_gather | solution.py:300
  106.9 7.3 %expert.1 = bf16[8,512,256]{2,1,0:T(8,128)(2,1)} custom-call(bf16[8,512,256]{2,1,0:T(8,128)(2,1)} %all-gather.2.cloned.1.call-done.x_hbm, bf16[2048,256]{1,0:T(8,128)(2,1)S(1)} %bitcast.15, bf16[2048,256]{1,0:T(8,128)(2,1)S(1)} %collective-permute-done.2.g1, bf16[2048,256]{1,0:T(8,128)(2,1)} %bitcast.19, bf16[2048,256]{1,0:T(8,128)(2,1)} %copy-done.4, ...), custom_call_target="tpu_custom_call" | custom-call | tf_op jit(solution)/shard_map/expert/pallas_call | solution.py:302
  114.2 43.2 %reduce-scatter.2.cloned.1.call-done = bf16[1,512,256]{2,1,0:T(8,128)(2,1)} async-done(((bf16[8,512,256]{2,1,0:T(8,128)(2,1)}), bf16[1,512,256]{2,1,0:T(8,128)(2,1)}) %reduce-scatter.2.cloned.1.call-update) | async-done | bytes 262160 | tf_op jit(solution)/shard_map/reduce_scatter | solution.py:320
  157.5 21.1 %all_to_all.16.back_ref = bf16[32,16,256]{2,1,0:T(8,128)(2,1)S(1)} all-to-all(bf16[32,16,256]{2,1,0:T(8,128)(2,1)} %bitcast.24), channel_id=1, replica_groups=mesh['sp'=32,'y'=8,'c'=2] {'sp'}, dimensions={0} | all-to-all | bytes 524288 | tf_op jit(solution)/shard_map/all_to_all | solution.py:321
  178.6 1.0 combine.1
  179.6 7.9 %collective-permute-start.5 = (f32[256,128]{1,0:T(8,128)S(1)}, f32[256,128]{1,0:T(8,128)S(1)}, u32[]{:S(2)}, u32[]{:S(2)}) collective-permute-start(f32[256,128]{1,0:T(8,128)S(1)} %get-tuple-element.24), channel_id=1, source_target_pairs={{0,1},{1,0},{2,3},{3,2},{4,5},{5,4},{6,7},{7,6},{8,9},{9,8},{10,11... | collective-permute-start | bytes 393224 | tf_op jit(solution)/shard_map/ppermute | solution.py:18
  187.5 1.0 collective-permute-done.5
  188.5 0.6 add_convert_fusion
  (16 shorter events, 0.2 us)
Async XLA Ops:
  8.3 17.1 %all-to-all-start = ((bf16[8,64,256]{2,1,0:T(8,128)(2,1)}), bf16[8,64,256]{2,1,0:T(8,128)(2,1)S(1)}, u32[]{:S(2)}, u32[]{:S(2)}) async-start(bf16[8,64,256]{2,1,0:T(8,128)(2,1)} %get-tuple-element.19), calls=%async_computation | async-start | bytes 524288 | tf_op jit(solution)/shard_map/all_to_all | solution.py:260
  15.9 58.2 %copy-start = (bf16[1,2048,256]{2,1,0:T(8,128)(2,1)S(1)}, bf16[1,2048,256]{2,1,0:T(8,128)(2,1)}, u32[]{:S(2)}) copy-start(bf16[1,2048,256]{2,1,0:T(8,128)(2,1)} %param.19) | copy-start | bytes 3145732
  15.9 62.5 %copy-start.3 = (bf16[1,2048,256]{2,1,0:T(8,128)(2,1)S(1)}, bf16[1,2048,256]{2,1,0:T(8,128)(2,1)}, u32[]{:S(2)}) copy-start(bf16[1,2048,256]{2,1,0:T(8,128)(2,1)} %param.20) | copy-start | bytes 3145732
  15.9 91.0 %all-gather.2.cloned.1.call-start = ((), (), s32[]{:S(2)}) async-start(), calls=%async_computation.4 | async-start | bytes 2359296 | tf_op jit(solution)/shard_map/all_gather | solution.py:300
  16.0 4.3 %collective-permute-start = (f32[64,128]{1,0:T(8,128)S(1)}, f32[64,128]{1,0:T(8,128)S(1)}, u32[]{:S(2)}, u32[]{:S(2)}) collective-permute-start(f32[64,128]{1,0:T(8,128)S(1)} %get-tuple-element.15), channel_id=1, source_target_pairs={{0,16},{16,32},{32,48},{48,64},{64,80},{80,96},{96,112},{112,128},... | collective-permute-start | bytes 98312 | tf_op jit(solution)/shard_map/ppermute | solution.py:259
  25.4 21.8 %collective-permute-start.1 = (bf16[8,64,256]{2,1,0:T(8,128)(2,1)S(1)}, bf16[8,64,256]{2,1,0:T(8,128)(2,1)S(1)}, u32[]{:S(2)}, u32[]{:S(2)}) collective-permute-start(bf16[8,64,256]{2,1,0:T(8,128)(2,1)S(1)} %all-to-all-done.own_ref), channel_id=1, source_target_pairs={{0,1},{1,0},{2,3},{3,2},{4,5},{5,4},{6,7},{7,6},{8,9},{9,8},{10,11... | collective-permute-start | bytes 786440 | tf_op jit(solution)/shard_map/ppermute | solution.py:18
  74.1 83.4 %reduce-scatter.2.cloned.1.call-start = ((), (), s32[]{:S(2)}) async-start(), calls=%async_computation.5 | async-start | bytes 2359296 | tf_op jit(solution)/shard_map/reduce_scatter | solution.py:320
  74.2 8.6 %collective-permute-start.2 = (bf16[2048,256]{1,0:T(8,128)(2,1)S(1)}, bf16[2048,256]{1,0:T(8,128)(2,1)S(1)}, u32[]{:S(2)}, u32[]{:S(2)}) collective-permute-start(bf16[2048,256]{1,0:T(8,128)(2,1)S(1)} %bitcast.14), channel_id=1, source_target_pairs={{0,1},{1,0},{2,3},{3,2},{4,5},{5,4},{6,7},{7,6},{8,9},{9,8},{10,11... | collective-permute-start | bytes 3145736 | tf_op jit(solution)/shard_map/ppermute | solution.py:18
  78.4 4.6 %collective-permute-start.3 = (bf16[2048,256]{1,0:T(8,128)(2,1)S(1)}, bf16[2048,256]{1,0:T(8,128)(2,1)S(1)}, u32[]{:S(2)}, u32[]{:S(2)}) collective-permute-start(bf16[2048,256]{1,0:T(8,128)(2,1)S(1)} %bitcast.20), channel_id=1, source_target_pairs={{0,1},{1,0},{2,3},{3,2},{4,5},{5,4},{6,7},{7,6},{8,9},{9,8},{10,11... | collective-permute-start | bytes 3145736 | tf_op jit(solution)/shard_map/ppermute | solution.py:18
  80.4 5.0 %collective-permute-start.4 = (bf16[256,2048]{1,0:T(8,128)(2,1)}, bf16[256,2048]{1,0:T(8,128)(2,1)}, u32[]{:S(2)}, u32[]{:S(2)}) collective-permute-start(bf16[256,2048]{1,0:T(8,128)(2,1)} %bitcast.21), channel_id=1, source_target_pairs={{0,1},{1,0},{2,3},{3,2},{4,5},{5,4},{6,7},{7,6},{8,9},{9,8},{10,11... | collective-permute-start | bytes 3145736 | tf_op jit(solution)/shard_map/ppermute | solution.py:18
  83.0 1.0 copy-start.4
  114.2 64.4 %copy-start.1 = (s32[256,2]{0,1:T(2,128)S(1)}, s32[256,2]{0,1:T(2,128)}, u32[]{:S(2)}) copy-start(s32[256,2]{0,1:T(2,128)} %param.17) | copy-start | bytes 6148
  114.2 64.4 %copy-start.2 = (f32[256,2]{0,1:T(2,128)S(1)}, f32[256,2]{0,1:T(2,128)}, u32[]{:S(2)}) copy-start(f32[256,2]{0,1:T(2,128)} %param.18) | copy-start | bytes 6148
  179.6 8.9 %collective-permute-start.5 = (f32[256,128]{1,0:T(8,128)S(1)}, f32[256,128]{1,0:T(8,128)S(1)}, u32[]{:S(2)}, u32[]{:S(2)}) collective-permute-start(f32[256,128]{1,0:T(8,128)S(1)} %get-tuple-element.24), channel_id=1, source_target_pairs={{0,1},{1,0},{2,3},{3,2},{4,5},{5,4},{6,7},{7,6},{8,9},{9,8},{10,11... | collective-permute-start | bytes 393224 | tf_op jit(solution)/shard_map/ppermute | solution.py:18
Sparse Core Ops, SparseCore 0:
  74.2 32.6 all-gather.1
  114.4 43.0 reduce-scatter.1

commit v9 on v8

--- a/solution.py
+++ b/solution.py
@@ -190,9 +190,11 @@
             columns = slice(i * width, (i + 1) * width)
             piece = jnp.dot(hidden, down_ref[:, columns], preferred_element_type=F32)
             out_ref[k, i] = piece.astype(BF16)
-        out = pltpu.make_async_copy(out_ref.at[k], out_hbm.at[:, pl.ds(k * part, part)], out_sem.at[k])
-        out.start()
-        outs.append(out)
+            out = pltpu.make_async_copy(
+                out_ref.at[k, i], out_hbm.at[i, pl.ds(k * part, part)], out_sem.at[k, i]
+            )
+            out.start()
+            outs.append(out)
     for out in outs:
         out.wait()
 
@@ -312,7 +314,7 @@
             pltpu.SemaphoreType.DMA((parts,)),
             pltpu.SemaphoreType.DMA((2,)),
             pltpu.SemaphoreType.DMA((2,)),
-            pltpu.SemaphoreType.DMA((parts,)),
+            pltpu.SemaphoreType.DMA((parts, chips)),
         ],
         compiler_params=room(32),
         name="expert",

time: 196 us -> 196 us (level)
  no operation moved by 1% of the time
where the time goes in v9:
time: 196 us
  waiting for transfers between devices  72.7 us (37%)
  blocking collectives  61.2 us (31%)
  starting transfers between devices  32.9 us (17%)
  Pallas kernels  13.8 us (7%)
  between operations  13.5 us (7%)
    reduce_scatter x1, waiting for transfers between devices, local(): summed = lax.psum_scatter(partial, 'y', scatter_dimension=0, tiled=True)  43.7 us
    all_to_all x1, blocking collectives, local(): lax.all_to_all(send, 'sp', 0, 0, tiled=True)  24.2 us
    ppermute x5, starting transfers between devices, twin(): return lax.ppermute(value, 'c', [(0, 1), (1, 0)])  22 us
    all_gather x1, waiting for transfers between devices, local(): full = lax.all_gather(arrived, 'y', axis=0, tiled=True)  21.5 us
    all_to_all x1, blocking collectives, local(): lax.all_to_all(summed.reshape(experts, slots, width), 'sp', 0, 0, tiled=T...  20.6 us
    all_gather x1, blocking collectives, local(): rows = lax.all_gather(filtered, TP, axis=0, tiled=True)  16.3 us
    all_to_all x1, starting transfers between devices, local(): own_out = lax.all_to_all(packed, 'y', 0, 0, tiled=True)  7.64 us
    pallas_call x1, Pallas kernels, local(): pl.pallas_call(expert_kernel, out_shape=pltpu.HBM(full.shape, BF16), in_s...  7.17 us
  transfers between devices with their start and end apart: 9, of which 7 were waited for; matrix products, arithmetic and copies ran while one was open for 0% of the time, Pallas kernels for 1%

profile of v9, /device:TPU:1, one launch (start us, length us, event | category | flops | bytes accessed | tf_op | source)
XLA Modules:
  0.0 195.8 jit_solution(6181322227112998120)
XLA Ops:
  6.5 1.7 first.1
  8.3 7.6 %all-to-all-start = ((bf16[8,64,256]{2,1,0:T(8,128)(2,1)}), bf16[8,64,256]{2,1,0:T(8,128)(2,1)S(1)}, u32[]{:S(2)}, u32[]{:S(2)}) async-start(bf16[8,64,256]{2,1,0:T(8,128)(2,1)} %get-tuple-element.19), calls=%async_computation | async-start | bytes 524288 | tf_op jit(solution)/shard_map/all_to_all | solution.py:262
  16.0 3.2 %collective-permute-start = (f32[64,128]{1,0:T(8,128)S(1)}, f32[64,128]{1,0:T(8,128)S(1)}, u32[]{:S(2)}, u32[]{:S(2)}) collective-permute-start(f32[64,128]{1,0:T(8,128)S(1)} %get-tuple-element.15), channel_id=1, source_target_pairs={{0,16},{16,32},{32,48},{48,64},{64,80},{80,96},{96,112},{112,128},... | collective-permute-start | bytes 98312 | tf_op jit(solution)/shard_map/ppermute | solution.py:261
  19.3 0.9 collective-permute-done.head_ref
  20.2 1.2 filter.1
  21.4 3.9 %all-to-all-done.own_ref = bf16[8,64,256]{2,1,0:T(8,128)(2,1)S(1)} async-done(((bf16[8,64,256]{2,1,0:T(8,128)(2,1)}), bf16[8,64,256]{2,1,0:T(8,128)(2,1)S(1)}, u32[]{:S(2)}, u32[]{:S(2)}) %all-to-all-start) | async-done | bytes 262176 | tf_op jit(solution)/shard_map/all_to_all | solution.py:262
  25.4 5.5 %collective-permute-start.1 = (bf16[8,64,256]{2,1,0:T(8,128)(2,1)S(1)}, bf16[8,64,256]{2,1,0:T(8,128)(2,1)S(1)}, u32[]{:S(2)}, u32[]{:S(2)}) collective-permute-start(bf16[8,64,256]{2,1,0:T(8,128)(2,1)S(1)} %all-to-all-done.own_ref), channel_id=1, source_target_pairs={{0,1},{1,0},{2,3},{3,2},{4,5},{5,4},{6,7},{7,6},{8,9},{9,8},{10,11... | collective-permute-start | bytes 786440 | tf_op jit(solution)/shard_map/ppermute | solution.py:18
  30.8 16.3 %all_gather.6 = bf16[1280,256]{1,0:T(8,128)(2,1)S(1)} all-gather(bf16[80,256]{1,0:T(8,128)(2,1)S(1)} %filter.1), channel_id=1, replica_groups=mesh['sp'=32,'y'=8,'c'=2] {'y','c'}, dimensions={0}, use_global_device_ids=true | all-gather | bytes 696320 | tf_op jit(solution)/shard_map/all_gather | solution.py:272
  47.2 2.7 %token_.1 = (f32[256,128]{1,0:T(8,128)S(1)}, bf16[32,16,256]{2,1,0:T(8,128)(2,1)S(1)}, f32[32,256]{1,0:T(8,128)S(1)}) custom-call(s32[2]{0:T(128)S(1)} %pad_add_fusion.place_ref, bf16[8,2,80,256]{3,2,1,0:T(8,128)(2,1)S(1)} %bitcast.13, bf16[8,64,256]{2,1,0:T(8,128)(2,1)S(1)} %all-to-all-done.own_ref, ...), custom_call_target="tpu_custom_call" | custom-call | tf_op jit(solution)/shard_map/token/pallas_call | solution.py:282
  49.8 24.2 %all_to_all.15 = bf16[32,16,256]{2,1,0:T(8,128)(2,1)} all-to-all(bf16[32,16,256]{2,1,0:T(8,128)(2,1)S(1)} %get-tuple-element.20), channel_id=1, replica_groups=mesh['sp'=32,'y'=8,'c'=2] {'sp'}, dimensions={0} | all-to-all | bytes 524288 | tf_op jit(solution)/shard_map/all_to_all | solution.py:301
  74.2 4.3 %collective-permute-start.2 = (bf16[2048,256]{1,0:T(8,128)(2,1)S(1)}, bf16[2048,256]{1,0:T(8,128)(2,1)S(1)}, u32[]{:S(2)}, u32[]{:S(2)}) collective-permute-start(bf16[2048,256]{1,0:T(8,128)(2,1)S(1)} %bitcast.14), channel_id=1, source_target_pairs={{0,1},{1,0},{2,3},{3,2},{4,5},{5,4},{6,7},{7,6},{8,9},{9,8},{10,11... | collective-permute-start | bytes 3145736 | tf_op jit(solution)/shard_map/ppermute | solution.py:18
  78.4 1.9 collective-permute-start.3
  80.4 2.4 %collective-permute-start.4 = (bf16[256,2048]{1,0:T(8,128)(2,1)}, bf16[256,2048]{1,0:T(8,128)(2,1)}, u32[]{:S(2)}, u32[]{:S(2)}) collective-permute-start(bf16[256,2048]{1,0:T(8,128)(2,1)} %bitcast.21), channel_id=1, source_target_pairs={{0,1},{1,0},{2,3},{3,2},{4,5},{5,4},{6,7},{7,6},{8,9},{9,8},{10,11... | collective-permute-start | bytes 3145736 | tf_op jit(solution)/shard_map/ppermute | solution.py:18
  82.8 0.2 collective-permute-done.3.u1_hbm
  83.0 1.0 copy-done.4
  84.0 1.4 collective-permute-done.4.d1_hbm
  85.4 21.5 %all-gather.2.cloned.1.call-done.x_hbm = bf16[8,512,256]{2,1,0:T(8,128)(2,1)} async-done(((bf16[1,512,256]{2,1,0:T(8,128)(2,1)}), bf16[8,512,256]{2,1,0:T(8,128)(2,1)}) %all-gather.2.cloned.1.call-update) | async-done | bytes 2097168 | tf_op jit(solution)/shard_map/all_gather | solution.py:302
  106.9 7.2 %expert.1 = bf16[8,512,256]{2,1,0:T(8,128)(2,1)} custom-call(bf16[8,512,256]{2,1,0:T(8,128)(2,1)} %all-gather.2.cloned.1.call-done.x_hbm, bf16[2048,256]{1,0:T(8,128)(2,1)S(1)} %bitcast.15, bf16[2048,256]{1,0:T(8,128)(2,1)S(1)} %collective-permute-done.2.g1, bf16[2048,256]{1,0:T(8,128)(2,1)} %bitcast.19, bf16[2048,256]{1,0:T(8,128)(2,1)} %copy-done.4, ...), custom_call_target="tpu_custom_call" | custom-call | tf_op jit(solution)/shard_map/expert/pallas_call | solution.py:304
  114.1 43.7 %reduce-scatter.2.cloned.1.call-done = bf16[1,512,256]{2,1,0:T(8,128)(2,1)} async-done(((bf16[8,512,256]{2,1,0:T(8,128)(2,1)}), bf16[1,512,256]{2,1,0:T(8,128)(2,1)}) %reduce-scatter.2.cloned.1.call-update) | async-done | bytes 262160 | tf_op jit(solution)/shard_map/reduce_scatter | solution.py:322
  157.8 20.6 %all_to_all.16.back_ref = bf16[32,16,256]{2,1,0:T(8,128)(2,1)S(1)} all-to-all(bf16[32,16,256]{2,1,0:T(8,128)(2,1)} %bitcast.24), channel_id=1, replica_groups=mesh['sp'=32,'y'=8,'c'=2] {'sp'}, dimensions={0} | all-to-all | bytes 524288 | tf_op jit(solution)/shard_map/all_to_all | solution.py:323
  178.5 1.0 combine.1
  179.5 7.9 %collective-permute-start.5 = (f32[256,128]{1,0:T(8,128)S(1)}, f32[256,128]{1,0:T(8,128)S(1)}, u32[]{:S(2)}, u32[]{:S(2)}) collective-permute-start(f32[256,128]{1,0:T(8,128)S(1)} %get-tuple-element.24), channel_id=1, source_target_pairs={{0,1},{1,0},{2,3},{3,2},{4,5},{5,4},{6,7},{7,6},{8,9},{9,8},{10,11... | collective-permute-start | bytes 393224 | tf_op jit(solution)/shard_map/ppermute | solution.py:18
  187.4 1.0 collective-permute-done.5
  188.4 0.6 add_convert_fusion
  (16 shorter events, 0.2 us)
Async XLA Ops:
  8.3 17.1 %all-to-all-start = ((bf16[8,64,256]{2,1,0:T(8,128)(2,1)}), bf16[8,64,256]{2,1,0:T(8,128)(2,1)S(1)}, u32[]{:S(2)}, u32[]{:S(2)}) async-start(bf16[8,64,256]{2,1,0:T(8,128)(2,1)} %get-tuple-element.19), calls=%async_computation | async-start | bytes 524288 | tf_op jit(solution)/shard_map/all_to_all | solution.py:262
  15.9 58.2 %copy-start = (bf16[1,2048,256]{2,1,0:T(8,128)(2,1)S(1)}, bf16[1,2048,256]{2,1,0:T(8,128)(2,1)}, u32[]{:S(2)}) copy-start(bf16[1,2048,256]{2,1,0:T(8,128)(2,1)} %param.19) | copy-start | bytes 3145732
  15.9 62.5 %copy-start.3 = (bf16[1,2048,256]{2,1,0:T(8,128)(2,1)S(1)}, bf16[1,2048,256]{2,1,0:T(8,128)(2,1)}, u32[]{:S(2)}) copy-start(bf16[1,2048,256]{2,1,0:T(8,128)(2,1)} %param.20) | copy-start | bytes 3145732
  15.9 91.0 %all-gather.2.cloned.1.call-start = ((), (), s32[]{:S(2)}) async-start(), calls=%async_computation.4 | async-start | bytes 2359296 | tf_op jit(solution)/shard_map/all_gather | solution.py:302
  16.0 4.3 %collective-permute-start = (f32[64,128]{1,0:T(8,128)S(1)}, f32[64,128]{1,0:T(8,128)S(1)}, u32[]{:S(2)}, u32[]{:S(2)}) collective-permute-start(f32[64,128]{1,0:T(8,128)S(1)} %get-tuple-element.15), channel_id=1, source_target_pairs={{0,16},{16,32},{32,48},{48,64},{64,80},{80,96},{96,112},{112,128},... | collective-permute-start | bytes 98312 | tf_op jit(solution)/shard_map/ppermute | solution.py:261
  25.4 21.8 %collective-permute-start.1 = (bf16[8,64,256]{2,1,0:T(8,128)(2,1)S(1)}, bf16[8,64,256]{2,1,0:T(8,128)(2,1)S(1)}, u32[]{:S(2)}, u32[]{:S(2)}) collective-permute-start(bf16[8,64,256]{2,1,0:T(8,128)(2,1)S(1)} %all-to-all-done.own_ref), channel_id=1, source_target_pairs={{0,1},{1,0},{2,3},{3,2},{4,5},{5,4},{6,7},{7,6},{8,9},{9,8},{10,11... | collective-permute-start | bytes 786440 | tf_op jit(solution)/shard_map/ppermute | solution.py:18
  74.1 83.7 %reduce-scatter.2.cloned.1.call-start = ((), (), s32[]{:S(2)}) async-start(), calls=%async_computation.5 | async-start | bytes 2359296 | tf_op jit(solution)/shard_map/reduce_scatter | solution.py:322
  74.2 8.6 %collective-permute-start.2 = (bf16[2048,256]{1,0:T(8,128)(2,1)S(1)}, bf16[2048,256]{1,0:T(8,128)(2,1)S(1)}, u32[]{:S(2)}, u32[]{:S(2)}) collective-permute-start(bf16[2048,256]{1,0:T(8,128)(2,1)S(1)} %bitcast.14), channel_id=1, source_target_pairs={{0,1},{1,0},{2,3},{3,2},{4,5},{5,4},{6,7},{7,6},{8,9},{9,8},{10,11... | collective-permute-start | bytes 3145736 | tf_op jit(solution)/shard_map/ppermute | solution.py:18
  78.4 4.6 %collective-permute-start.3 = (bf16[2048,256]{1,0:T(8,128)(2,1)S(1)}, bf16[2048,256]{1,0:T(8,128)(2,1)S(1)}, u32[]{:S(2)}, u32[]{:S(2)}) collective-permute-start(bf16[2048,256]{1,0:T(8,128)(2,1)S(1)} %bitcast.20), channel_id=1, source_target_pairs={{0,1},{1,0},{2,3},{3,2},{4,5},{5,4},{6,7},{7,6},{8,9},{9,8},{10,11... | collective-permute-start | bytes 3145736 | tf_op jit(solution)/shard_map/ppermute | solution.py:18
  80.4 5.0 %collective-permute-start.4 = (bf16[256,2048]{1,0:T(8,128)(2,1)}, bf16[256,2048]{1,0:T(8,128)(2,1)}, u32[]{:S(2)}, u32[]{:S(2)}) collective-permute-start(bf16[256,2048]{1,0:T(8,128)(2,1)} %bitcast.21), channel_id=1, source_target_pairs={{0,1},{1,0},{2,3},{3,2},{4,5},{5,4},{6,7},{7,6},{8,9},{9,8},{10,11... | collective-permute-start | bytes 3145736 | tf_op jit(solution)/shard_map/ppermute | solution.py:18
  83.0 1.0 copy-start.4
  114.1 64.4 %copy-start.1 = (s32[256,2]{0,1:T(2,128)S(1)}, s32[256,2]{0,1:T(2,128)}, u32[]{:S(2)}) copy-start(s32[256,2]{0,1:T(2,128)} %param.17) | copy-start | bytes 6148
  114.1 64.4 %copy-start.2 = (f32[256,2]{0,1:T(2,128)S(1)}, f32[256,2]{0,1:T(2,128)}, u32[]{:S(2)}) copy-start(f32[256,2]{0,1:T(2,128)} %param.18) | copy-start | bytes 6148
  179.5 8.9 %collective-permute-start.5 = (f32[256,128]{1,0:T(8,128)S(1)}, f32[256,128]{1,0:T(8,128)S(1)}, u32[]{:S(2)}, u32[]{:S(2)}) collective-permute-start(f32[256,128]{1,0:T(8,128)S(1)} %get-tuple-element.24), channel_id=1, source_target_pairs={{0,1},{1,0},{2,3},{3,2},{4,5},{5,4},{6,7},{7,6},{8,9},{9,8},{10,11... | collective-permute-start | bytes 393224 | tf_op jit(solution)/shard_map/ppermute | solution.py:18
Sparse Core Ops, SparseCore 0:
  74.2 32.6 all-gather.1
  114.2 43.5 reduce-scatter.1

commit v10 on v9

--- a/solution.py
+++ b/solution.py
@@ -79,19 +79,37 @@
     out_ref[group:, :] = gain_ref[...]
 
 
-def token_kernel(
-    place_ref, rows_ref, own_ref, other_ref, ids_hbm, all_ref, upd_ref, send_ref, rank_ref, res_ref, ids_ref, sem, ids_sem
-):
+def plan_kernel(place_ref, ids_ref, all_ref, pick_ref, rank_ref, res_ref, sem):
     chip, core = place_ref[0], place_ref[1]
+    width, tokens = res_ref.shape[1], rank_ref.shape[1]
+    columns = pl.ds(pl.multiple_of(chip * width, width), width)
+    copy = pltpu.make_async_copy(all_ref.at[:, columns], res_ref, sem)
+    copy.start()
+    experts = rank_ref.shape[0]
+    slots = pick_ref.shape[0] // experts
+    expert = lax.broadcasted_iota(jnp.int32, (experts, tokens), 0)
+    named = (ids_ref[0:1, :] == expert) | (ids_ref[1:2, :] == expert)
+    before = lax.broadcasted_iota(jnp.int32, (tokens, tokens), 0)
+    after = lax.broadcasted_iota(jnp.int32, (tokens, tokens), 1)
+    earlier = jnp.dot(
+        named.astype(F32).astype(BF16),
+        (before < after).astype(F32).astype(BF16),
+        preferred_element_type=F32,
+    )
+    rank = jnp.where(named, earlier, -1.0)
+    rank_ref[...] = rank
+    slot = lax.broadcasted_iota(jnp.int32, (experts, slots, tokens), 1) + core * slots
+    pick = (rank[:, None, :] == slot.astype(F32)).astype(F32).astype(BF16)
+    pick_ref[...] = pick.reshape(experts * slots, tokens)
+    copy.wait()
+
+
+def token_kernel(place_ref, rows_ref, own_ref, other_ref, pick_ref, res_ref, upd_ref, send_ref):
+    core = place_ref[1]
     blocks, _, _, tokens = rows_ref.shape
     group = own_ref.shape[1]
     half = blocks * group
     width = res_ref.shape[1]
-    columns = pl.ds(pl.multiple_of(chip * width, width), width)
-    copy = pltpu.make_async_copy(all_ref.at[:, columns], res_ref, sem)
-    copy.start()
-    ids_copy = pltpu.make_async_copy(ids_hbm, ids_ref, ids_sem)
-    ids_copy.start()
     both = []
     for which in (core, 1 - core):
         values = rows_ref[:, which, :group].reshape(half, tokens).astype(F32)
@@ -116,27 +134,12 @@
         mixed = mixed + lax.dot_general(
             activated, weight, across(0, 0), preferred_element_type=F32
         )
-    copy.wait()
     updated = res_ref[...].astype(F32) + mixed
     mine = width // 2
     upd_ref[...] = jnp.where(core == 0, updated[:, :mine], updated[:, mine:])
-    ids_copy.wait()
     experts, slots = send_ref.shape[:2]
-    expert = lax.broadcasted_iota(jnp.int32, (experts, tokens), 0)
-    named = (ids_ref[0:1, :] == expert) | (ids_ref[1:2, :] == expert)
-    before = lax.broadcasted_iota(jnp.int32, (tokens, tokens), 0)
-    after = lax.broadcasted_iota(jnp.int32, (tokens, tokens), 1)
-    earlier = jnp.dot(
-        named.astype(F32).astype(BF16),
-        (before < after).astype(F32).astype(BF16),
-        preferred_element_type=F32,
-    )
-    rank = jnp.where(named, earlier, -1.0)
-    rank_ref[...] = rank
-    slot = lax.broadcasted_iota(jnp.int32, (experts, slots, tokens), 1) + core * slots
-    pick = (rank[:, None, :] == slot.astype(F32)).astype(F32).astype(BF16)
     sent = jnp.dot(
-        pick.reshape(experts * slots, tokens), updated.astype(BF16), preferred_element_type=F32
+        pick_ref[...], updated.astype(BF16), preferred_element_type=F32
     )
     send_ref[...] = sent.astype(BF16).reshape(experts, slots, width)
 
@@ -257,6 +260,22 @@
         compiler_params=room(4),
         name="first",
     )(*(far(a) for a in (conv_value.T, conv_gate.T, out_weight, conv_taps, conv_gain[None])))
+    ids, weights = route_ids.T, route_weight.T
+    slots = 2 * tokens * route_ids.shape[1] // experts // 2
+    mine = width // 2
+    pick, rank, res = pl.pallas_call(
+        plan_kernel,
+        out_shape=(
+            pltpu.VMEM((experts * slots, tokens), BF16),
+            pltpu.VMEM((experts, tokens), F32),
+            pltpu.VMEM((tokens, width), BF16),
+        ),
+        in_specs=[SMEM, VMEM, HBM],
+        out_specs=(VMEM,) * 3,
+        scratch_shapes=[pltpu.SemaphoreType.DMA],
+        compiler_params=room(8),
+        name="slots",
+    )(place, far(ids), far(residual))
     order = lax.axis_size("sp")
     head = lax.ppermute(tail, "sp", [(i, i + 1) for i in range(order - 1)])
     own_out = lax.all_to_all(packed, "y", 0, 0, tiled=True)
@@ -276,27 +295,17 @@
     ups = (expert_up[0], twin(expert_up[0]))
     downs = (expert_down[0], twin(expert_down[0]))
 
-    ids, weights = route_ids.T, route_weight.T
-    slots = 2 * tokens * route_ids.shape[1] // experts // 2
-    mine = width // 2
-    updated, send, rank = pl.pallas_call(
+    updated, send = pl.pallas_call(
         token_kernel,
         out_shape=(
             pltpu.VMEM((tokens, mine), F32),
             pltpu.VMEM((experts, slots, width), BF16),
-            pltpu.VMEM((experts, tokens), F32),
         ),
-        in_specs=[SMEM] + [VMEM] * 3 + [HBM] * 2,
-        out_specs=(VMEM,) * 3,
-        scratch_shapes=[
-            pltpu.VMEM((tokens, width), BF16),
-            pltpu.VMEM(ids.shape, jnp.int32),
-            pltpu.SemaphoreType.DMA,
-            pltpu.SemaphoreType.DMA,
-        ],
+        in_specs=[SMEM] + [VMEM] * 5,
+        out_specs=(VMEM,) * 2,
         compiler_params=room(12),
         name="token",
-    )(place, near(rows), near(own_out), near(other_out), far(ids), far(residual))
+    )(place, near(rows), near(own_out), near(other_out), near(pick), near(res))
 
     arrived = lax.all_to_all(send, "sp", 0, 0, tiled=True).reshape(1, experts * slots, width)
     full = lax.all_gather(arrived, "y", axis=0, tiled=True)

time: 196 us -> 196 us (level)
  transfers between devices with their start and end apart: 9 -> 9, of which waited for: 7 -> 6; matrix products, arithmetic and copies ran while one was open for 0% -> 0% of each run, Pallas kernels for 1% -> 2%
where the time goes in v10:
time: 196 us; the launch traced here: 195 us
  waiting for transfers between devices  70.8 us (36%)
  blocking collectives  60.9 us (31%)
  starting transfers between devices  33.5 us (17%)
  Pallas kernels  14.7 us (8%)
  between operations  13.6 us (7%)
    reduce_scatter x1, waiting for transfers between devices, local(): summed = lax.psum_scatter(partial, 'y', scatter_dimension=0, tiled=True)  43.5 us
    all_to_all x1, blocking collectives, local(): lax.all_to_all(send, 'sp', 0, 0, tiled=True)  24.2 us
    ppermute x5, starting transfers between devices, twin(): return lax.ppermute(value, 'c', [(0, 1), (1, 0)])  22.7 us
    all_gather x1, waiting for transfers between devices, local(): full = lax.all_gather(arrived, 'y', axis=0, tiled=True)  21.5 us
    all_to_all x1, blocking collectives, local(): lax.all_to_all(summed.reshape(experts, slots, width), 'sp', 0, 0, tiled=T...  20.4 us
    all_gather x1, blocking collectives, local(): rows = lax.all_gather(filtered, TP, axis=0, tiled=True)  16.3 us
    all_to_all x1, starting transfers between devices, local(): own_out = lax.all_to_all(packed, 'y', 0, 0, tiled=True)  7.64 us
    pallas_call x1, Pallas kernels, local(): pl.pallas_call(expert_kernel, out_shape=pltpu.HBM(full.shape, BF16), in_s...  7.23 us
  transfers between devices with their start and end apart: 9, of which 6 were waited for; matrix products, arithmetic and copies ran while one was open for 0% of the time, Pallas kernels for 2%

profile of v10, /device:TPU:1, one launch (start us, length us, event | category | flops | bytes accessed | tf_op | source)
XLA Modules:
  0.0 195.3 jit_solution(10067336042881530879)
XLA Ops:
  6.5 1.8 first.1
  8.3 7.6 %all-to-all-start = ((bf16[8,64,256]{2,1,0:T(8,128)(2,1)}), bf16[8,64,256]{2,1,0:T(8,128)(2,1)S(1)}, u32[]{:S(2)}, u32[]{:S(2)}) async-start(bf16[8,64,256]{2,1,0:T(8,128)(2,1)} %get-tuple-element.21), calls=%async_computation | async-start | bytes 524288 | tf_op jit(solution)/shard_map/all_to_all | solution.py:281
  16.0 3.1 %collective-permute-start = (f32[64,128]{1,0:T(8,128)S(1)}, f32[64,128]{1,0:T(8,128)S(1)}, u32[]{:S(2)}, u32[]{:S(2)}) collective-permute-start(f32[64,128]{1,0:T(8,128)S(1)} %get-tuple-element.17), channel_id=1, source_target_pairs={{0,16},{16,32},{32,48},{48,64},{64,80},{80,96},{96,112},{112,128},... | collective-permute-start | bytes 98312 | tf_op jit(solution)/shard_map/ppermute | solution.py:280
  19.2 1.8 slots.1
  21.0 1.2 filter.1
  22.2 3.2 %all-to-all-done.own_ref = bf16[8,64,256]{2,1,0:T(8,128)(2,1)S(1)} async-done(((bf16[8,64,256]{2,1,0:T(8,128)(2,1)}), bf16[8,64,256]{2,1,0:T(8,128)(2,1)S(1)}, u32[]{:S(2)}, u32[]{:S(2)}) %all-to-all-start) | async-done | bytes 262176 | tf_op jit(solution)/shard_map/all_to_all | solution.py:281
  25.4 5.5 %collective-permute-start.1 = (bf16[8,64,256]{2,1,0:T(8,128)(2,1)S(1)}, bf16[8,64,256]{2,1,0:T(8,128)(2,1)S(1)}, u32[]{:S(2)}, u32[]{:S(2)}) collective-permute-start(bf16[8,64,256]{2,1,0:T(8,128)(2,1)S(1)} %all-to-all-done.own_ref), channel_id=1, source_target_pairs={{0,1},{1,0},{2,3},{3,2},{4,5},{5,4},{6,7},{7,6},{8,9},{9,8},{10,11... | collective-permute-start | bytes 786440 | tf_op jit(solution)/shard_map/ppermute | solution.py:18
  30.8 16.3 %all_gather.6 = bf16[1280,256]{1,0:T(8,128)(2,1)S(1)} all-gather(bf16[80,256]{1,0:T(8,128)(2,1)S(1)} %filter.1), channel_id=1, replica_groups=mesh['sp'=32,'y'=8,'c'=2] {'y','c'}, dimensions={0}, use_global_device_ids=true | all-gather | bytes 696320 | tf_op jit(solution)/shard_map/all_gather | solution.py:291
  47.2 1.8 token_.1
  49.0 24.2 %all_to_all.15 = bf16[32,16,256]{2,1,0:T(8,128)(2,1)} all-to-all(bf16[32,16,256]{2,1,0:T(8,128)(2,1)S(1)} %get-tuple-element.24), channel_id=1, replica_groups=mesh['sp'=32,'y'=8,'c'=2] {'sp'}, dimensions={0} | all-to-all | bytes 524288 | tf_op jit(solution)/shard_map/all_to_all | solution.py:310
  73.3 4.3 %collective-permute-start.2 = (bf16[2048,256]{1,0:T(8,128)(2,1)S(1)}, bf16[2048,256]{1,0:T(8,128)(2,1)S(1)}, u32[]{:S(2)}, u32[]{:S(2)}) collective-permute-start(bf16[2048,256]{1,0:T(8,128)(2,1)S(1)} %bitcast.14), channel_id=1, source_target_pairs={{0,1},{1,0},{2,3},{3,2},{4,5},{5,4},{6,7},{7,6},{8,9},{9,8},{10,11... | collective-permute-start | bytes 3145736 | tf_op jit(solution)/shard_map/ppermute | solution.py:18
  77.5 1.9 collective-permute-start.3
  79.5 2.4 %collective-permute-start.4 = (bf16[256,2048]{1,0:T(8,128)(2,1)}, bf16[256,2048]{1,0:T(8,128)(2,1)}, u32[]{:S(2)}, u32[]{:S(2)}) collective-permute-start(bf16[256,2048]{1,0:T(8,128)(2,1)} %bitcast.21), channel_id=1, source_target_pairs={{0,1},{1,0},{2,3},{3,2},{4,5},{5,4},{6,7},{7,6},{8,9},{9,8},{10,11... | collective-permute-start | bytes 3145736 | tf_op jit(solution)/shard_map/ppermute | solution.py:18
  81.9 0.2 collective-permute-done.3.u1_hbm
  82.1 1.0 copy-done.4
  83.1 1.4 collective-permute-done.4.d1_hbm
  84.5 21.5 %all-gather.2.cloned.1.call-done.x_hbm = bf16[8,512,256]{2,1,0:T(8,128)(2,1)} async-done(((bf16[1,512,256]{2,1,0:T(8,128)(2,1)}), bf16[8,512,256]{2,1,0:T(8,128)(2,1)}) %all-gather.2.cloned.1.call-update) | async-done | bytes 2097168 | tf_op jit(solution)/shard_map/all_gather | solution.py:311
  106.0 7.2 %expert.1 = bf16[8,512,256]{2,1,0:T(8,128)(2,1)} custom-call(bf16[8,512,256]{2,1,0:T(8,128)(2,1)} %all-gather.2.cloned.1.call-done.x_hbm, bf16[2048,256]{1,0:T(8,128)(2,1)S(1)} %bitcast.15, bf16[2048,256]{1,0:T(8,128)(2,1)S(1)} %collective-permute-done.2.g1, bf16[2048,256]{1,0:T(8,128)(2,1)} %bitcast.19, bf16[2048,256]{1,0:T(8,128)(2,1)} %copy-done.4, ...), custom_call_target="tpu_custom_call" | custom-call | tf_op jit(solution)/shard_map/expert/pallas_call | solution.py:313
  113.3 43.5 %reduce-scatter.2.cloned.1.call-done = bf16[1,512,256]{2,1,0:T(8,128)(2,1)} async-done(((bf16[8,512,256]{2,1,0:T(8,128)(2,1)}), bf16[1,512,256]{2,1,0:T(8,128)(2,1)}) %reduce-scatter.2.cloned.1.call-update) | async-done | bytes 262160 | tf_op jit(solution)/shard_map/reduce_scatter | solution.py:331
  156.8 20.4 %all_to_all.16.back_ref = bf16[32,16,256]{2,1,0:T(8,128)(2,1)S(1)} all-to-all(bf16[32,16,256]{2,1,0:T(8,128)(2,1)} %bitcast.24), channel_id=1, replica_groups=mesh['sp'=32,'y'=8,'c'=2] {'sp'}, dimensions={0} | all-to-all | bytes 524288 | tf_op jit(solution)/shard_map/all_to_all | solution.py:332
  177.2 1.0 combine.1
  178.2 8.6 %collective-permute-start.5 = (f32[256,128]{1,0:T(8,128)S(1)}, f32[256,128]{1,0:T(8,128)S(1)}, u32[]{:S(2)}, u32[]{:S(2)}) collective-permute-start(f32[256,128]{1,0:T(8,128)S(1)} %get-tuple-element.28), channel_id=1, source_target_pairs={{0,1},{1,0},{2,3},{3,2},{4,5},{5,4},{6,7},{7,6},{8,9},{9,8},{10,11... | collective-permute-start | bytes 393224 | tf_op jit(solution)/shard_map/ppermute | solution.py:18
  186.8 1.0 collective-permute-done.5
  187.8 0.6 add_convert_fusion
  (17 shorter events, 0.2 us)
Async XLA Ops:
  8.3 17.1 %all-to-all-start = ((bf16[8,64,256]{2,1,0:T(8,128)(2,1)}), bf16[8,64,256]{2,1,0:T(8,128)(2,1)S(1)}, u32[]{:S(2)}, u32[]{:S(2)}) async-start(bf16[8,64,256]{2,1,0:T(8,128)(2,1)} %get-tuple-element.21), calls=%async_computation | async-start | bytes 524288 | tf_op jit(solution)/shard_map/all_to_all | solution.py:281
  15.9 90.1 %all-gather.2.cloned.1.call-start = ((), (), s32[]{:S(2)}) async-start(), calls=%async_computation.4 | async-start | bytes 2359296 | tf_op jit(solution)/shard_map/all_gather | solution.py:311
  16.0 5.0 %collective-permute-start = (f32[64,128]{1,0:T(8,128)S(1)}, f32[64,128]{1,0:T(8,128)S(1)}, u32[]{:S(2)}, u32[]{:S(2)}) collective-permute-start(f32[64,128]{1,0:T(8,128)S(1)} %get-tuple-element.17), channel_id=1, source_target_pairs={{0,16},{16,32},{32,48},{48,64},{64,80},{80,96},{96,112},{112,128},... | collective-permute-start | bytes 98312 | tf_op jit(solution)/shard_map/ppermute | solution.py:280
  19.2 54.1 %copy-start = (bf16[1,2048,256]{2,1,0:T(8,128)(2,1)S(1)}, bf16[1,2048,256]{2,1,0:T(8,128)(2,1)}, u32[]{:S(2)}) copy-start(bf16[1,2048,256]{2,1,0:T(8,128)(2,1)} %param.19) | copy-start | bytes 3145732
  19.2 58.4 %copy-start.3 = (bf16[1,2048,256]{2,1,0:T(8,128)(2,1)S(1)}, bf16[1,2048,256]{2,1,0:T(8,128)(2,1)}, u32[]{:S(2)}) copy-start(bf16[1,2048,256]{2,1,0:T(8,128)(2,1)} %param.20) | copy-start | bytes 3145732
  25.4 21.8 %collective-permute-start.1 = (bf16[8,64,256]{2,1,0:T(8,128)(2,1)S(1)}, bf16[8,64,256]{2,1,0:T(8,128)(2,1)S(1)}, u32[]{:S(2)}, u32[]{:S(2)}) collective-permute-start(bf16[8,64,256]{2,1,0:T(8,128)(2,1)S(1)} %all-to-all-done.own_ref), channel_id=1, source_target_pairs={{0,1},{1,0},{2,3},{3,2},{4,5},{5,4},{6,7},{7,6},{8,9},{9,8},{10,11... | collective-permute-start | bytes 786440 | tf_op jit(solution)/shard_map/ppermute | solution.py:18
  73.2 83.6 %reduce-scatter.2.cloned.1.call-start = ((), (), s32[]{:S(2)}) async-start(), calls=%async_computation.5 | async-start | bytes 2359296 | tf_op jit(solution)/shard_map/reduce_scatter | solution.py:331
  73.3 8.6 %collective-permute-start.2 = (bf16[2048,256]{1,0:T(8,128)(2,1)S(1)}, bf16[2048,256]{1,0:T(8,128)(2,1)S(1)}, u32[]{:S(2)}, u32[]{:S(2)}) collective-permute-start(bf16[2048,256]{1,0:T(8,128)(2,1)S(1)} %bitcast.14), channel_id=1, source_target_pairs={{0,1},{1,0},{2,3},{3,2},{4,5},{5,4},{6,7},{7,6},{8,9},{9,8},{10,11... | collective-permute-start | bytes 3145736 | tf_op jit(solution)/shard_map/ppermute | solution.py:18
  77.5 4.6 %collective-permute-start.3 = (bf16[2048,256]{1,0:T(8,128)(2,1)S(1)}, bf16[2048,256]{1,0:T(8,128)(2,1)S(1)}, u32[]{:S(2)}, u32[]{:S(2)}) collective-permute-start(bf16[2048,256]{1,0:T(8,128)(2,1)S(1)} %bitcast.20), channel_id=1, source_target_pairs={{0,1},{1,0},{2,3},{3,2},{4,5},{5,4},{6,7},{7,6},{8,9},{9,8},{10,11... | collective-permute-start | bytes 3145736 | tf_op jit(solution)/shard_map/ppermute | solution.py:18
  79.5 5.0 %collective-permute-start.4 = (bf16[256,2048]{1,0:T(8,128)(2,1)}, bf16[256,2048]{1,0:T(8,128)(2,1)}, u32[]{:S(2)}, u32[]{:S(2)}) collective-permute-start(bf16[256,2048]{1,0:T(8,128)(2,1)} %bitcast.21), channel_id=1, source_target_pairs={{0,1},{1,0},{2,3},{3,2},{4,5},{5,4},{6,7},{7,6},{8,9},{9,8},{10,11... | collective-permute-start | bytes 3145736 | tf_op jit(solution)/shard_map/ppermute | solution.py:18
  82.1 1.0 copy-start.4
  113.3 63.9 %copy-start.1 = (s32[256,2]{0,1:T(2,128)S(1)}, s32[256,2]{0,1:T(2,128)}, u32[]{:S(2)}) copy-start(s32[256,2]{0,1:T(2,128)} %param.17) | copy-start | bytes 6148
  113.3 63.9 %copy-start.2 = (f32[256,2]{0,1:T(2,128)S(1)}, f32[256,2]{0,1:T(2,128)}, u32[]{:S(2)}) copy-start(f32[256,2]{0,1:T(2,128)} %param.18) | copy-start | bytes 6148
  178.2 9.6 %collective-permute-start.5 = (f32[256,128]{1,0:T(8,128)S(1)}, f32[256,128]{1,0:T(8,128)S(1)}, u32[]{:S(2)}, u32[]{:S(2)}) collective-permute-start(f32[256,128]{1,0:T(8,128)S(1)} %get-tuple-element.28), channel_id=1, source_target_pairs={{0,1},{1,0},{2,3},{3,2},{4,5},{5,4},{6,7},{7,6},{8,9},{9,8},{10,11... | collective-permute-start | bytes 393224 | tf_op jit(solution)/shard_map/ppermute | solution.py:18
Sparse Core Ops, SparseCore 0:
  73.3 32.6 all-gather.1
  113.4 43.3 reduce-scatter.1
